TPU v7x, 32 devices: a whole 2x2x4 slice. The times are simulated.
32 devices in a mesh: fs: 4 (over z), tp: 8 (over y, x, core).
Axes of the slice: x: 2, y: 2, z: 4, core: 2. Of those that a mesh axis runs over, the one named last changes fastest.
Arguments:
- tokens: bfloat16 [768, 2304], P('fs'), may hold values from -6 to 6
- gate_train: float32 [8, 2304, 2304], P(None, 'fs', 'tp'), may hold values from -0.125 to 0.125
- up_train: float32 [8, 2304, 2304], P(None, 'fs', 'tp'), may hold values from -0.125 to 0.125
- down_train: float32 [8, 2304, 2304], P(None, 'fs', 'tp'), may hold values from -0.125 to 0.125
- gain: float32 [2304], P('fs'), may hold values from 0.1 to 1.9
- routes: int32 [768, 2], P('fs'), may hold values from 0 to 7, all different within a row; in each aligned block of 192 rows (0 to 191, 192 to 383, ...) at most 72 rows name the same one
- route_weights: float32 [768, 2], P('fs'), may hold values from 0.1 to 1
Outputs:
- gate_new: bfloat16 [8, 2304, 2304], P('tp')
- up_new: bfloat16 [8, 2304, 2304], P('tp')
- down_new: bfloat16 [8, 2304, 2304], P('tp')
- mixed: bfloat16 [768, 2304], P('fs', 'tp')
Inputs may be any that keep to these rules, and one draw needn't show every extreme that they name: `routes`: each row names two different experts; in each aligned block of 192 rows at most 72 rows name one expert, a bound that some block reaches.
All inputs are finite; a program needn't handle non-finite values.
Results may differ from a plain program's by a relative error of at most 0.0095.
Values may be sent and summed in bfloat16 or wider, within the bound.
A program may use at most 128 MiB of HBM per device.

v0:
```python
import jax
import jax.numpy as jnp
from jax import lax
from jax.experimental import pallas as pl
from jax.experimental.pallas import tpu as pltpu
from jax.sharding import PartitionSpec as P

CAP = 72


norm_eps = 1e-06


def arrange(matrix, tp_count):
    experts, row_count, col_count = matrix.shape
    slices = tp_count // experts
    piece_width = col_count // slices
    shaped = matrix.reshape(experts, row_count, slices, piece_width)
    return shaped.transpose(0, 2, 3, 1).reshape(tp_count, piece_width, row_count)


def block_of(*counts):
    for size in (256, 128):
        if all(count % size == 0 for count in counts):
            return size
    return None


def flip(wide, total_rows, first_row, base=None):
    features, rows = wide.shape
    size = block_of(rows, first_row, total_rows) or rows
    first = first_row // size

    def kernel(*refs):
        refs[-1][...] = refs[0][...].T

    in_specs = [pl.BlockSpec((features, size), lambda i: (0, i))]
    operands = [wide]
    aliases = {}
    if base is not None:
        in_specs.append(pl.BlockSpec(memory_space=pl.ANY))
        operands.append(base)
        aliases = {1: 0}
    return pl.pallas_call(
        kernel,
        grid=(rows // size,),
        in_specs=in_specs,
        out_specs=pl.BlockSpec((size, features), lambda i: (first + i, 0)),
        out_shape=jax.ShapeDtypeStruct((total_rows, features), wide.dtype),
        input_output_aliases=aliases,
        cost_estimate=pl.CostEstimate(
            flops=0, bytes_accessed=4 * features * rows, transcendentals=0
        ),
    )(*operands)


def columns(wide, first, count, *others):
    size = block_of(first, count, *others)
    if size is None:
        return lax.slice_in_dim(wide, first, first + count, axis=1), count, 0
    return wide, size, first // size


def flip_product(wide, first, rows, chosen):
    features = wide.shape[0]
    wide, size, start = columns(wide, first, rows)
    slots = chosen.shape[0]

    def kernel(wide_ref, chosen_ref, rows_ref, product_ref):
        value = wide_ref[...]
        rows_ref[...] = value.T
        product_ref[...] = jnp.dot(chosen_ref[...], value, preferred_element_type=jnp.float32)

    return pl.pallas_call(
        kernel,
        grid=(rows // size,),
        in_specs=[
            pl.BlockSpec((features, size), lambda i: (0, start + i)),
            pl.BlockSpec((slots, features), lambda i: (0, 0)),
        ],
        out_specs=[
            pl.BlockSpec((size, features), lambda i: (i, 0)),
            pl.BlockSpec((slots, size), lambda i: (0, i)),
        ],
        out_shape=[
            jax.ShapeDtypeStruct((rows, features), wide.dtype),
            jax.ShapeDtypeStruct((slots, rows), jnp.float32),
        ],
        cost_estimate=pl.CostEstimate(
            flops=2 * slots * features * rows,
            bytes_accessed=4 * features * rows,
            transcendentals=0,
        ),
    )(wide, chosen)


def spread(train, gain):
    experts, features, count = train.shape
    rows = experts * count
    size = block_of(rows) or rows

    def kernel(train_ref, gain_ref, out_ref):
        out_ref[...] = (train_ref[...] * gain_ref[...]).astype(jnp.bfloat16).T

    return pl.pallas_call(
        kernel,
        grid=(rows // size,),
        in_specs=[
            pl.BlockSpec((size, features), lambda i: (i, 0)),
            pl.BlockSpec((1, features), lambda i: (0, 0)),
        ],
        out_specs=pl.BlockSpec((features, size), lambda i: (0, i)),
        out_shape=jax.ShapeDtypeStruct((features, rows), jnp.bfloat16),
        cost_estimate=pl.CostEstimate(
            flops=train.size, bytes_accessed=6 * train.size, transcendentals=0
        ),
    )(train.transpose(0, 2, 1).reshape(rows, features), gain[None, :])


def flip_dot(wide, first, total_rows, hidden):
    features = wide.shape[0]
    slots, rows = hidden.shape
    wide, size, start = columns(wide, first, rows, total_rows)

    def kernel(wide_ref, hidden_ref, rows_ref, total_ref):
        turned = wide_ref[...].T
        rows_ref[...] = turned

        @pl.when(pl.program_id(0) == 0)
        def _():
            total_ref[...] = jnp.zeros_like(total_ref)

        total_ref[...] += jnp.dot(hidden_ref[...], turned, preferred_element_type=jnp.float32)

    return pl.pallas_call(
        kernel,
        grid=(rows // size,),
        in_specs=[
            pl.BlockSpec((features, size), lambda i: (0, start + i)),
            pl.BlockSpec((slots, size), lambda i: (0, i)),
        ],
        out_specs=[
            pl.BlockSpec((size, features), lambda i: (i, 0)),
            pl.BlockSpec((slots, features), lambda i: (0, 0)),
        ],
        out_shape=[
            jax.ShapeDtypeStruct((total_rows, features), wide.dtype),
            jax.ShapeDtypeStruct((slots, features), jnp.float32),
        ],
        cost_estimate=pl.CostEstimate(
            flops=2 * slots * features * rows,
            bytes_accessed=4 * features * rows,
            transcendentals=0,
        ),
    )(wide, hidden)


def keep_dot(weights, chosen):
    rows, features = weights.shape
    size = block_of(rows) or rows
    slots = chosen.shape[0]

    def kernel(weights_ref, chosen_ref, rows_ref, product_ref):
        rows_ref[...] = weights_ref[...]
        product_ref[...] = lax.dot_general(
            chosen_ref[...],
            weights_ref[...],
            (((1,), (1,)), ((), ())),
            preferred_element_type=jnp.float32,
        )

    return pl.pallas_call(
        kernel,
        grid=(rows // size,),
        in_specs=[
            pl.BlockSpec((size, features), lambda i: (i, 0)),
            pl.BlockSpec((slots, features), lambda i: (0, 0)),
        ],
        out_specs=[
            pl.BlockSpec((size, features), lambda i: (i, 0)),
            pl.BlockSpec((slots, size), lambda i: (0, i)),
        ],
        out_shape=[
            jax.ShapeDtypeStruct((rows, features), weights.dtype),
            jax.ShapeDtypeStruct((slots, rows), jnp.float32),
        ],
        cost_estimate=pl.CostEstimate(
            flops=2 * slots * features * rows,
            bytes_accessed=4 * features * rows,
            transcendentals=0,
        ),
    )(weights, chosen)


def after(value, *others):
    def kernel(*refs):
        pass

    return pl.pallas_call(
        kernel,
        in_specs=[pl.BlockSpec(memory_space=pl.ANY)] * (1 + len(others)),
        out_specs=pl.BlockSpec(memory_space=pl.ANY),
        out_shape=jax.ShapeDtypeStruct(value.shape, value.dtype),
        input_output_aliases={0: 0},
    )(value, *others)


def shards(tokens, gate_train, up_train, down_train, gain, routes, route_weights):
    tp_count = lax.axis_size("tp")
    experts = gate_train.shape[0]
    slices = tp_count // experts
    gain_column = gain[None, :, None]
    up_round = (up_train * gain_column).astype(jnp.bfloat16)
    down_round = down_train.astype(jnp.bfloat16)

    def exchange(matrix):
        return lax.all_to_all(matrix, "tp", split_axis=0, concat_axis=1, tiled=True)

    gate_all = lax.all_gather(spread(gate_train, gain), "fs", axis=0, tiled=True)
    features = gate_all.shape[0]

    up_moved = exchange(arrange(up_round, tp_count))[0].T
    down_moved = exchange(arrange(down_round, tp_count))[0].T
    units = down_moved.shape[1]
    size = block_of(units) or units
    main = units - size if units > size else units
    both_wide = lax.all_gather(
        jnp.concatenate([up_moved, down_moved[:, :main]], axis=1), "fs", axis=0, tiled=True
    )

    tokens_wide = tokens.astype(jnp.float32)
    normed = (
        tokens_wide
        * lax.rsqrt(jnp.mean(tokens_wide * tokens_wide, axis=1, keepdims=True) + norm_eps)
    ).astype(jnp.bfloat16)
    expert = lax.axis_index("tp") // slices
    matches = routes == expert
    member = jnp.any(matches, axis=1)
    slot_index = jnp.cumsum(member.astype(jnp.int32)) - 1
    marked = jnp.where(member, slot_index, -1)
    picker = (marked[None, :] == jnp.arange(CAP, dtype=jnp.int32)[:, None]).astype(jnp.bfloat16)
    chosen = jnp.dot(picker, normed, preferred_element_type=jnp.float32).astype(jnp.bfloat16)
    contract_last = (((1,), (1,)), ((), ()))

    gate_moved = exchange(gate_all.reshape(features, tp_count, -1).transpose(1, 2, 0))
    gate_new, gate_pre = keep_dot(gate_moved[0], chosen)
    up_new, up_pre = flip_product(both_wide, 0, units, chosen)
    hidden = (jax.nn.silu(gate_pre) * up_pre).astype(jnp.bfloat16)
    down_new, partial_value = flip_dot(both_wide, units, units, hidden[:, :main])
    if main < units:
        rest_moved = after(down_moved[:, main:], gate_new)
        rest_wide = lax.all_gather(rest_moved, "fs", axis=0, tiled=True)
        partial_value = partial_value + lax.dot_general(
            hidden[:, main:], rest_wide, contract_last, preferred_element_type=jnp.float32
        )
        down_new = flip(rest_wide, units, main, down_new)
    partial_value = partial_value.astype(jnp.bfloat16)

    labels = jnp.arange(experts, dtype=jnp.int32)
    member_all = jnp.any(routes[:, :, None] == labels[None, None, :], axis=1)
    slots_all = jnp.cumsum(member_all.astype(jnp.int32), axis=0) - 1
    slot_pair = jnp.take_along_axis(slots_all, routes, axis=1)
    flat_index = slot_pair * experts + routes
    received = lax.all_to_all(
        partial_value.reshape(CAP, tp_count, -1), "tp", split_axis=1, concat_axis=1, tiled=True
    )
    summed = jnp.sum(received.reshape(CAP, experts, slices, -1).astype(jnp.float32), axis=2)
    summed = summed.reshape(CAP * experts, -1)
    picked = jnp.take(summed, flat_index, axis=0)
    mixed = jnp.sum(route_weights[:, :, None] * picked, axis=1)
    return (gate_new[None], up_new[None], down_new[None], mixed.astype(jnp.bfloat16))


def solution(mesh):
    in_specs = (
        P("fs", None),
        P(None, "fs", "tp"),
        P(None, "fs", "tp"),
        P(None, "fs", "tp"),
        P("fs"),
        P("fs", None),
        P("fs", None),
    )
    out_specs = (P("tp", None, None), P("tp", None, None), P("tp", None, None), P("fs", "tp"))
    return jax.shard_map(shards, mesh=mesh, in_specs=in_specs, out_specs=out_specs, check_vma=False)
```

profile of v0, /device:TPU:0, one launch (start us, length us, event | category | flops | bytes accessed | tf_op | source)
XLA Modules:
  0.0 604.5 jit_solution(15822619317554677456)
XLA Ops:
  8.5 7.6 %shard_map.102 = bf16[576,2304]{1,0:T(8,128)(2,1)} custom-call(f32[2304,576]{1,0:T(8,128)} %bitcast.53, f32[1,576]{1,0:T(1,128)} %broadcast_in_dim.37.gain_ref), custom_call_target="tpu_custom_call" | custom-call | flops 1327104 | bytes 7962624 | tf_op jit(solution)/shard_map/pallas_call | solution.py:105
  16.1 4.6 convert_bitcast_fusion
  20.7 5.3 all-to-all-start.2
  26.0 5.7 fusion.1
  31.7 30.0 %all-to-all-done.2 = bf16[8,288,576]{2,1,0:T(8,128)(2,1)S(1)} async-done(((bf16[8,288,576]{2,1,0:T(8,128)(2,1)}), bf16[8,288,576]{2,1,0:T(8,128)(2,1)S(1)}, u32[]{:S(2)}, u32[]{:S(2)}) %all-to-all-start.2) | async-done | bytes 2654240 | tf_op jit(solution)/shard_map/all_to_all | solution.py:217
  61.8 4.4 all-to-all-start.1
  66.2 3.5 copy.72
  69.7 3.4 slice.45
  73.1 28.8 %all-to-all-done.1 = bf16[8,288,576]{2,1,0:T(8,128)(2,1)} async-done(((bf16[8,288,576]{2,1,0:T(8,128)(2,1)}), bf16[8,288,576]{2,1,0:T(8,128)(2,1)}, u32[]{:S(2)}, u32[]{:S(2)}) %all-to-all-start.1) | async-done | bytes 2654240 | tf_op jit(solution)/shard_map/all_to_all | solution.py:217
  101.9 3.4 copy.71
  105.4 4.3 pad_maximum_fusion
  109.7 95.3 %all-gather.4.cloned.1.call-done = bf16[2304,2304]{1,0:T(8,128)(2,1)} async-done(((bf16[576,2304]{1,0:T(8,128)(2,1)}), bf16[2304,2304]{1,0:T(8,128)(2,1)}) %all-gather.4.cloned.1.call-update) | async-done | bytes 10616848 | tf_op jit(solution)/shard_map/all_gather | solution.py:219
  205.0 15.6 %copy.70 = bf16[2304,2304]{0,1:T(8,128)(2,1)} copy(bf16[2304,2304]{1,0:T(8,128)(2,1)} %all-gather.4.cloned.1.call-done) | data formatting | bytes 21233664 | tf_op jit(solution)/shard_map/all_gather | solution.py:219
  220.6 5.4 all-to-all-start
  227.4 2.7 gather_fusion.1
  234.0 110.0 %all-to-all-done = bf16[8,288,2304]{2,1,0:T(8,128)(2,1)} async-done(((bf16[8,288,2304]{2,1,0:T(8,128)(2,1)}), bf16[8,288,2304]{2,1,0:T(8,128)(2,1)}, u32[]{:S(2)}, u32[]{:S(2)}) %all-to-all-start) | async-done | bytes 10616864 | tf_op jit(solution)/shard_map/all_to_all | solution.py:217
  344.0 13.4 %shard_map.103 = (bf16[2304,2304]{1,0:T(8,128)(2,1)}, f32[72,2304]{1,0:T(8,128)}) custom-call(bf16[2304,2304]{1,0:T(8,128)(2,1)} %bitcast.4.weights_ref, bf16[72,2304]{1,0:T(8,128)(2,1)} %convolution_convert_fusion.chosen_ref), custom_call_target="tpu_custom_call" | custom-call | flops 764411904 | bytes 21233664 | tf_op jit(solution)/shard_map/pallas_call | solution.py:172
  357.5 189.8 %all-gather.6.cloned.1.call-done.wide_ref = bf16[2304,4352]{1,0:T(8,128)(2,1)} async-done(((bf16[576,4352]{1,0:T(8,128)(2,1)}), bf16[2304,4352]{1,0:T(8,128)(2,1)}) %all-gather.6.cloned.1.call-update) | async-done | bytes 20054032 | tf_op jit(solution)/shard_map/all_gather | solution.py:227
  547.2 13.1 %shard_map.104 = (bf16[2304,2304]{1,0:T(8,128)(2,1)}, f32[72,2304]{1,0:T(8,128)}) custom-call(bf16[2304,4352]{1,0:T(8,128)(2,1)} %all-gather.6.cloned.1.call-done.wide_ref, bf16[72,2304]{1,0:T(8,128)(2,1)} %convolution_convert_fusion.chosen_ref), custom_call_target="tpu_custom_call" | custom-call | flops 764411904 | bytes 21233664 | tf_op jit(solution)/shard_map/pallas_call | solution.py:74
  562.3 10.3 %shard_map.106 = (bf16[2304,2304]{1,0:T(8,128)(2,1)}, f32[72,2304]{1,0:T(8,128)}) custom-call(bf16[2304,4352]{1,0:T(8,128)(2,1)} %all-gather.6.cloned.1.call-done.wide_ref, bf16[72,2048]{1,0:T(8,128)(2,1)} %slice.47.hidden_ref), custom_call_target="tpu_custom_call" | custom-call | flops 679477248 | bytes 18874368 | tf_op jit(solution)/shard_map/pallas_call | solution.py:135
  572.6 5.2 all-gather.8.cloned.1.call-done.refs_0_
  581.3 3.7 all-to-all-start.3
  585.5 2.6 shard_map.107
  588.1 5.6 all-to-all-done.3
  (57 shorter events, 16.8 us)
Async XLA Ops:
  7.2 197.9 %all-gather.4.cloned.1.call-start = ((), (), s32[]{:S(2)}) async-start(), calls=%async_computation.4 | async-start | bytes 13271040 | tf_op jit(solution)/shard_map/all_gather | solution.py:219
  20.7 5.3 copy-start.3
  20.7 41.1 %all-to-all-start.2 = ((bf16[8,288,576]{2,1,0:T(8,128)(2,1)}), bf16[8,288,576]{2,1,0:T(8,128)(2,1)S(1)}, u32[]{:S(2)}, u32[]{:S(2)}) async-start(bf16[8,288,576]{2,1,0:T(8,128)(2,1)} %convert_bitcast_fusion), calls=%async_computation.2 | async-start | bytes 5898240 | tf_op jit(solution)/shard_map/all_to_all | solution.py:217
  61.8 40.2 %all-to-all-start.1 = ((bf16[8,288,576]{2,1,0:T(8,128)(2,1)}), bf16[8,288,576]{2,1,0:T(8,128)(2,1)}, u32[]{:S(2)}, u32[]{:S(2)}) async-start(bf16[8,288,576]{2,1,0:T(8,128)(2,1)} %fusion.1), calls=%async_computation.1 | async-start | bytes 5898240 | tf_op jit(solution)/shard_map/all_to_all | solution.py:217
  66.2 481.0 %all-gather.6.cloned.1.call-start = ((), (), s32[]{:S(2)}) async-start(), calls=%async_computation.5 | async-start | bytes 25067520 | tf_op jit(solution)/shard_map/all_gather | solution.py:227
  220.6 5.5 copy-start.2
  220.6 123.4 %all-to-all-start = ((bf16[8,288,2304]{2,1,0:T(8,128)(2,1)}), bf16[8,288,2304]{2,1,0:T(8,128)(2,1)}, u32[]{:S(2)}, u32[]{:S(2)}) async-start(bf16[8,288,2304]{2,1,0:T(8,128)(2,1)} %bitcast.45), calls=%async_computation | async-start | bytes 21233664 | tf_op jit(solution)/shard_map/all_to_all | solution.py:217
  226.1 351.7 %all-gather.8.cloned.1.call-start = ((), (), s32[]{:S(2)}) async-start(), calls=%async_computation.6 | async-start | bytes 1474560 | tf_op jit(solution)/shard_map/all_gather | solution.py:252
  227.4 3.5 copy-start
  357.5 202.8 %copy-start.1 = (f32[72,2304]{1,0:T(8,128)S(1)}, f32[72,2304]{1,0:T(8,128)}, u32[]{:S(2)}) copy-start(f32[72,2304]{1,0:T(8,128)} %get-tuple-element.12) | copy-start | bytes 1990660
  562.3 23.0 %copy-start.4 = (f32[192,2]{0,1:T(2,128)S(1)}, f32[192,2]{0,1:T(2,128)}, u32[]{:S(2)}) copy-start(f32[192,2]{0,1:T(2,128)} %param.13) | copy-start | bytes 4612
  581.3 12.5 %all-to-all-start.3 = ((bf16[72,8,288]{2,0,1:T(8,128)(2,1)}), bf16[72,8,288]{2,0,1:T(8,128)(2,1)S(1)}, u32[]{:S(2)}, u32[]{:S(2)}) async-start(bf16[72,8,288]{2,0,1:T(8,128)(2,1)} %copy.77), calls=%async_computation.3 | async-start | bytes 884736 | tf_op jit(solution)/shard_map/all_to_all | solution.py:264
Sparse Core Ops, SparseCore 0:
  16.2 188.7 all-gather.3
  207.2 340.0 all-gather.5
  548.8 28.9 all-gather.7
where the time goes:
time: 607 us; the launch traced here: 604 us
  waiting for transfers between devices  465 us (77%)
  Pallas kernels  47.1 us (8%)
  local copies, waits for them, and re-layouts  37.4 us (6%)
  other arithmetic  19.3 us (3%)
  starting transfers between devices  19 us (3%)
  between operations  13.9 us (2%)
    all_gather x1, waiting for transfers between devices, shards(): lax.all_gather(jnp.concatenate([up_moved, down_moved[:, :main]], axis=1),...  190 us
    all_to_all x3, waiting for transfers between devices, exchange(): return lax.all_to_all(matrix, 'tp', split_axis=0, concat_axis=1, tiled=True)  169 us
    all_gather x1, waiting for transfers between devices, shards(): lax.all_gather(spread(gate_train, gain), 'fs', axis=0, tiled=True)  95.3 us
    all_gather x1, local copies, waits for them, and re-layouts, shards(): lax.all_gather(spread(gate_train, gain), 'fs', axis=0, tiled=True)  15.6 us
    all_to_all x3, starting transfers between devices, exchange(): return lax.all_to_all(matrix, 'tp', split_axis=0, concat_axis=1, tiled=True)  15.2 us
    pallas_call x1, Pallas kernels, keep_dot(): pl.pallas_call(kernel, grid=(rows // size,), in_specs=[pl.BlockSpec((size...  13.4 us
    pallas_call x1, Pallas kernels, flip_product(): pl.pallas_call(kernel, grid=(rows // size,), in_specs=[pl.BlockSpec((feat...  13.1 us
  transfers between devices with their start and end apart: 7, of which 7 were waited for; matrix products, arithmetic and copies ran while one was open for 8% of the time, Pallas kernels for 7%

commit v1 on v0

--- a/solution.py
+++ b/solution.py
@@ -271,7 +271,412 @@
     return (gate_new[None], up_new[None], down_new[None], mixed.astype(jnp.bfloat16))
 
 
+def fits(mesh_sizes, train):
+    count, tp_count = mesh_sizes
+    experts, features, units = train.shape
+    return (
+        experts == tp_count
+        and tp_count & (tp_count - 1) == 0
+        and count >= 4
+        and count % 2 == 0
+        and features % 128 == 64
+        and units % 32 == 0
+    )
+
+
+def main_start(block, features):
+    return block * features + (64 if block % 2 else 0)
+
+
+def prepare(gate, up, down, gain):
+    experts, units, features = gate.shape
+    wide, half = features - 64, units // 2
+    mats = (gate, up, down)
+
+    def kernel(odd_ref, gate_ref, up_ref, down_ref, gain_ref, main_ref, rest_ref):
+        def write(odd):
+            for m, ref in enumerate((gate_ref, up_ref, down_ref)):
+                value = ref[0]
+                if m < 2:
+                    value = value * gain_ref[...]
+                value = value.astype(jnp.bfloat16)
+                if odd:
+                    main, rest = value[:, 64:], value[:, :64]
+                else:
+                    main, rest = value[:, :wide], value[:, wide:]
+                main_ref[m, 0] = main
+                rest_ref[m, 0] = jnp.concatenate([rest[:half], rest[half:]], axis=1)
+
+        @pl.when(odd_ref[0] == 0)
+        def _():
+            write(False)
+
+        @pl.when(odd_ref[0] == 1)
+        def _():
+            write(True)
+
+    odd = (lax.axis_index("fs") % 2).astype(jnp.int32).reshape(1)
+    block = pl.BlockSpec((1, units, features), lambda i, s: (i, 0, 0))
+    return pl.pallas_call(
+        kernel,
+        grid_spec=pltpu.PrefetchScalarGridSpec(
+            num_scalar_prefetch=1,
+            grid=(experts,),
+            in_specs=[block, block, block, pl.BlockSpec((1, features), lambda i, s: (0, 0))],
+            out_specs=[
+                pl.BlockSpec((len(mats), 1, units, wide), lambda i, s: (0, i, 0, 0)),
+                pl.BlockSpec((len(mats), 1, half, 128), lambda i, s: (0, i, 0, 0)),
+            ],
+        ),
+        out_shape=[
+            jax.ShapeDtypeStruct((len(mats), experts, units, wide), jnp.bfloat16),
+            jax.ShapeDtypeStruct((len(mats), experts, half, 128), jnp.bfloat16),
+        ],
+        cost_estimate=pl.CostEstimate(
+            flops=3 * gate.size, bytes_accessed=18 * gate.size, transcendentals=0
+        ),
+    )(odd, gate, up, down, gain)
+
+
+def gather(own_main, own_rest, count):
+    mats, tp_count, units, wide = own_main.shape
+    half = own_rest.shape[2]
+    pieces = mats * tp_count
+    bits = tp_count.bit_length() - 1
+
+    def kernel(
+        own_main, own_rest, main, rest, hold, hold_rest, load_sem, keep_sem, plane_send, plane_recv,
+        plane_rest_send, plane_rest_recv, line_send, line_recv, line_rest_send, line_rest_recv,
+    ):
+        z = lax.axis_index("fs")
+        t = lax.axis_index("tp")
+
+        def peer(p):
+            total = 0
+            for b in range(bits):
+                mine, other = (t // (1 << b)) % 2, (p // (1 << b)) % 2
+                total = total + (mine + other - 2 * mine * other) * (1 << b)
+            return total
+
+        def plane(m, p):
+            e = peer(p)
+            return pltpu.make_async_remote_copy(
+                own_main.at[m, e], main.at[z, m, t], plane_send.at[m, p], plane_recv.at[m, p],
+                device_id={"fs": z, "tp": e}, device_id_type=pl.DeviceIdType.MESH,
+            )
+
+        def plane_rest(m, p):
+            e = peer(p)
+            return pltpu.make_async_remote_copy(
+                own_rest.at[m, e], rest.at[z, m, t], plane_rest_send.at[m, p], plane_rest_recv.at[m, p],
+                device_id={"fs": z, "tp": e}, device_id_type=pl.DeviceIdType.MESH,
+            )
+
+        def line(way, step, i):
+            block = z + step if way == 0 else z - step
+            target = z - 1 if way == 0 else z + 1
+            m, e = i // tp_count, peer(i % tp_count)
+            return pltpu.make_async_remote_copy(
+                main.at[block, m, e], main.at[block, m, e], line_send.at[way, step], line_recv.at[way, step, i],
+                device_id={"fs": target, "tp": t}, device_id_type=pl.DeviceIdType.MESH,
+            )
+
+        def line_rest(way, step, m):
+            block = z + step if way == 0 else z - step
+            target = z - 1 if way == 0 else z + 1
+            return pltpu.make_async_remote_copy(
+                rest.at[block, m], rest.at[block, m], line_rest_send.at[way, step, m], line_rest_recv.at[way, step, m],
+                device_id={"fs": target, "tp": t}, device_id_type=pl.DeviceIdType.MESH,
+            )
+
+        for m in range(mats):
+            pltpu.make_async_copy(own_main.at[m, t], hold.at[m], load_sem.at[0, m]).start()
+            pltpu.make_async_copy(own_rest.at[m, t], hold_rest.at[m], load_sem.at[1, m]).start()
+
+        for m in range(mats):
+            @pl.loop(1, tp_count)
+            def _(p, m=m):
+                plane(m, p).start()
+                plane_rest(m, p).start()
+
+        for m in range(mats):
+            pltpu.make_async_copy(own_main.at[m, t], hold.at[m], load_sem.at[0, m]).wait()
+            pltpu.make_async_copy(hold.at[m], main.at[z, m, t], keep_sem.at[0, m]).start()
+            pltpu.make_async_copy(own_rest.at[m, t], hold_rest.at[m], load_sem.at[1, m]).wait()
+            pltpu.make_async_copy(hold_rest.at[m], rest.at[z, m, t], keep_sem.at[1, m]).start()
+
+        def has(way, step):
+            return z + step <= count - 1 if way == 0 else z - step >= 0
+
+        def sends(way):
+            return z >= 1 if way == 0 else z <= count - 2
+
+        late = pieces - tp_count
+        for step in range(count):
+            for m in range(mats):
+                final = step == count - 1
+                last = final and m == mats - 1
+                skip = step == count - 2 and m == mats - 1
+                if step == 0:
+                    pltpu.make_async_copy(hold.at[m], main.at[z, m, t], keep_sem.at[0, m]).wait()
+                    pltpu.make_async_copy(hold_rest.at[m], rest.at[z, m, t], keep_sem.at[1, m]).wait()
+
+                @pl.loop(0, tp_count)
+                def _(p, step=step, m=m, last=last, skip=skip, final=final):
+                    i = m * tp_count + p
+                    if step == 0:
+                        @pl.when(p >= 1)
+                        def _():
+                            plane(m, p).wait_recv()
+                    for way in range(2):
+                        if step > 0 and not last:
+                            @pl.when(has(way, step))
+                            def _(way=way):
+                                line(way, step - 1, i).wait_recv()
+                        if not final and not skip:
+                            @pl.when(has(way, step) & sends(way))
+                            def _(way=way):
+                                line(way, step, i).start()
+
+                if step == 0:
+                    @pl.loop(1, tp_count)
+                    def _(p, m=m):
+                        plane_rest(m, p).wait_recv()
+                for way in range(2):
+                    if step > 0:
+                        @pl.when(has(way, step))
+                        def _(way=way, step=step, m=m):
+                            line_rest(way, step - 1, m).wait_recv()
+                    if not final:
+                        @pl.when(has(way, step) & sends(way))
+                        def _(way=way, step=step, m=m):
+                            line_rest(way, step, m).start()
+
+        for m in range(mats):
+            @pl.loop(1, tp_count)
+            def _(p, m=m):
+                plane(m, p).wait_send()
+                plane_rest(m, p).wait_send()
+        for step in range(count - 1):
+            for way in range(2):
+                @pl.when(has(way, step) & sends(way))
+                def _(way=way, step=step):
+                    sent = main.at[z, pl.ds(0, mats - 1 if step == count - 2 else mats)]
+                    pltpu.make_async_copy(sent, sent, line_send.at[way, step]).wait()
+                    for m in range(mats):
+                        line_rest(way, step, m).wait_send()
+
+    dma = pltpu.SemaphoreType.DMA
+    sent = 2 * (count - 1) * (own_main.size + own_rest.size)
+    return pl.pallas_call(
+        kernel,
+        in_specs=[pl.BlockSpec(memory_space=pl.ANY)] * 2,
+        out_specs=[pl.BlockSpec(memory_space=pl.ANY)] * 2,
+        out_shape=[
+            jax.ShapeDtypeStruct((count,) + own_main.shape, own_main.dtype),
+            jax.ShapeDtypeStruct((count,) + own_rest.shape, own_rest.dtype),
+        ],
+        scratch_shapes=[
+            pltpu.VMEM((mats, units, wide), own_main.dtype),
+            pltpu.VMEM((mats, half, 128), own_rest.dtype),
+            dma((2, mats)),
+            dma((2, mats)),
+            dma((mats, tp_count)),
+            dma((mats, tp_count)),
+            dma((mats, tp_count)),
+            dma((mats, tp_count)),
+            dma((2, count - 1)),
+            dma((2, count - 1, pieces)),
+            dma((2, count - 1, mats)),
+            dma((2, count - 1, mats)),
+        ],
+        compiler_params=pltpu.CompilerParams(has_side_effects=True),
+        cost_estimate=pl.CostEstimate(flops=10**9, bytes_accessed=2 * sent, transcendentals=0),
+    )(own_main, own_rest)
+
+
+def joined(main_ref, rest_ref, out_ref):
+    count, _, _, units, wide = main_ref.shape
+    features = wide + 64
+    half = units // 2
+    for block in range(count):
+        out_ref[:, pl.ds(main_start(block, features), wide)] = main_ref[block, 0, 0]
+    for block in range(0, count, 2):
+        first, second = rest_ref[block, 0, 0], rest_ref[block + 1, 0, 0]
+        place = pl.ds(block * features + wide, 128)
+        out_ref[:half, place] = jnp.concatenate([first[:, :64], second[:, :64]], axis=1)
+        out_ref[half:, place] = jnp.concatenate([first[:, 64:], second[:, 64:]], axis=1)
+
+
+def join_call(main, rest, which, kernel, operand, operand_spec, product_spec, product_shape):
+    count, mats, tp_count, units, wide = main.shape
+    half = rest.shape[3]
+    features = count * (wide + 64)
+    return pl.pallas_call(
+        kernel,
+        grid=(tp_count,),
+        in_specs=[
+            pl.BlockSpec((count, 1, 1, units, wide), lambda i: (0, which, i, 0, 0)),
+            pl.BlockSpec((count, 1, 1, half, 128), lambda i: (0, which, i, 0, 0)),
+            operand_spec,
+        ],
+        out_specs=[pl.BlockSpec((units, features), lambda i: (i, 0)), product_spec],
+        out_shape=[
+            jax.ShapeDtypeStruct((tp_count * units, features), main.dtype),
+            jax.ShapeDtypeStruct(product_shape, jnp.float32),
+        ],
+        cost_estimate=pl.CostEstimate(
+            flops=1000 * tp_count * units * features,
+            bytes_accessed=4 * tp_count * units * features,
+            transcendentals=0,
+        ),
+    )(main, rest, operand)
+
+
+def join_in(main, rest, which, chosen):
+    tp_count, units = main.shape[2:4]
+    slots, features = chosen.shape
+
+    def kernel(main_ref, rest_ref, chosen_ref, new_ref, product_ref):
+        joined(main_ref, rest_ref, new_ref)
+        product_ref[0] = lax.dot_general(
+            chosen_ref[...], new_ref[...], (((1,), (1,)), ((), ())), preferred_element_type=jnp.float32
+        )
+
+    return join_call(
+        main, rest, which, kernel, chosen,
+        pl.BlockSpec((slots, features), lambda i: (0, 0)),
+        pl.BlockSpec((1, slots, units), lambda i: (i, 0, 0)),
+        (tp_count, slots, units),
+    )
+
+
+def join_out(main, rest, which, hidden):
+    tp_count, slots, units = hidden.shape
+    features = main.shape[0] * (main.shape[4] + 64)
+
+    def kernel(main_ref, rest_ref, hidden_ref, new_ref, total_ref):
+        joined(main_ref, rest_ref, new_ref)
+
+        @pl.when(pl.program_id(0) == 0)
+        def _():
+            total_ref[...] = jnp.zeros_like(total_ref)
+
+        total_ref[...] += jnp.dot(hidden_ref[0], new_ref[...], preferred_element_type=jnp.float32)
+
+    return join_call(
+        main, rest, which, kernel, hidden,
+        pl.BlockSpec((1, slots, units), lambda i: (i, 0, 0)),
+        pl.BlockSpec((slots, features), lambda i: (0, 0)),
+        (slots, features),
+    )
+
+
+def join_far(arrived, kept, use_arrived, far_start, last_start, hidden, base):
+    tp_count, units, wide = arrived.shape
+    slots = hidden.shape[1]
+    size = 256 if (wide % 256 == 0 and last_start % 256 == 0) else 128
+
+    def kernel(scalar_ref, arrived_ref, kept_ref, hidden_ref, base_ref, new_ref, total_ref):
+        value = jnp.where(scalar_ref[1] == 1, arrived_ref[0], kept_ref[0])
+        new_ref[...] = value
+
+        @pl.when(pl.program_id(1) == 0)
+        def _():
+            total_ref[...] = jnp.zeros_like(total_ref)
+
+        total_ref[...] += jnp.dot(hidden_ref[0], value, preferred_element_type=jnp.float32)
+
+    scalars = jnp.stack([far_start // size, use_arrived.astype(jnp.int32)])
+    piece = pl.BlockSpec((1, units, size), lambda j, i, s: (i, 0, j))
+    return pl.pallas_call(
+        kernel,
+        grid_spec=pltpu.PrefetchScalarGridSpec(
+            num_scalar_prefetch=1,
+            grid=(wide // size, tp_count),
+            in_specs=[
+                piece, piece,
+                pl.BlockSpec((1, slots, units), lambda j, i, s: (i, 0, 0)),
+                pl.BlockSpec(memory_space=pl.ANY),
+            ],
+            out_specs=[
+                pl.BlockSpec((units, size), lambda j, i, s: (i, s[0] + j)),
+                pl.BlockSpec((slots, size), lambda j, i, s: (0, j)),
+            ],
+        ),
+        out_shape=[
+            jax.ShapeDtypeStruct(base.shape, base.dtype),
+            jax.ShapeDtypeStruct((slots, wide), jnp.float32),
+        ],
+        input_output_aliases={4: 0},
+        cost_estimate=pl.CostEstimate(
+            flops=2 * slots * arrived.size, bytes_accessed=6 * arrived.size, transcendentals=0
+        ),
+    )(scalars, arrived, kept, hidden, base)
+
+
+def pick(tokens, routes, expert):
+    tokens_wide = tokens.astype(jnp.float32)
+    normed = (
+        tokens_wide
+        * lax.rsqrt(jnp.mean(tokens_wide * tokens_wide, axis=1, keepdims=True) + norm_eps)
+    ).astype(jnp.bfloat16)
+    member = jnp.any(routes == expert, axis=1)
+    slot_index = jnp.cumsum(member.astype(jnp.int32)) - 1
+    marked = jnp.where(member, slot_index, -1)
+    picker = (marked[None, :] == jnp.arange(CAP, dtype=jnp.int32)[:, None]).astype(jnp.bfloat16)
+    return jnp.dot(picker, normed, preferred_element_type=jnp.float32).astype(jnp.bfloat16)
+
+
+def mix(partial_value, routes, route_weights, experts):
+    tp_count = lax.axis_size("tp")
+    labels = jnp.arange(experts, dtype=jnp.int32)
+    member_all = jnp.any(routes[:, :, None] == labels[None, None, :], axis=1)
+    slots_all = jnp.cumsum(member_all.astype(jnp.int32), axis=0) - 1
+    slot_pair = jnp.take_along_axis(slots_all, routes, axis=1)
+    flat_index = slot_pair * experts + routes
+    received = lax.all_to_all(
+        partial_value.reshape(CAP, tp_count, -1), "tp", split_axis=1, concat_axis=1, tiled=True
+    )
+    summed = received.astype(jnp.float32).reshape(CAP * experts, -1)
+    picked = jnp.take(summed, flat_index, axis=0)
+    return jnp.sum(route_weights[:, :, None] * picked, axis=1).astype(jnp.bfloat16)
+
+
+def line_shards(tokens, gate_train, up_train, down_train, gain, routes, route_weights):
+    count = lax.axis_size("fs")
+    place = lax.axis_index("fs")
+    experts, features, units = gate_train.shape
+    own_main, own_rest = prepare(
+        gate_train.transpose(0, 2, 1), up_train.transpose(0, 2, 1), down_train.transpose(0, 2, 1), gain[None, :]
+    )
+    main, rest = gather(own_main, own_rest, count)
+    far = jnp.where(place < count // 2, count - 1, 0)
+    kept = lax.dynamic_slice(main, (far, 2, 0, 0, 0), (1, 1) + main.shape[2:])[0, 0]
+    arrived = lax.ppermute(kept, "fs", [(1, 0), (count - 2, count - 1)])
+    main, rest, tokens, routes, route_weights = lax.optimization_barrier(
+        (main, rest, tokens, routes, route_weights)
+    )
+    chosen = pick(tokens, routes, lax.axis_index("tp"))
+    gate_new, gate_pre = join_in(main, rest, 0, chosen)
+    up_new, up_pre = join_in(main, rest, 1, chosen)
+    hidden = (jax.nn.silu(gate_pre) * up_pre).astype(jnp.bfloat16)
+    down_new, total = join_out(main, rest, 2, hidden)
+    at_end = (place == 0) | (place == count - 1)
+    last_start = main_start(count - 1, features)
+    far_start = jnp.where(far == 0, 0, last_start).astype(jnp.int32)
+    down_new, far_total = join_far(arrived, kept, at_end, far_start, last_start, hidden, down_new)
+    total = lax.dynamic_update_slice(total, far_total, (0, far_start))
+    mixed = mix(total.astype(jnp.bfloat16), routes, route_weights, experts)
+    return (gate_new[None], up_new[None], down_new[None], mixed)
+
+
 def solution(mesh):
+    sizes = (mesh.shape["fs"], mesh.shape["tp"])
+
+    def step(*args):
+        return (line_shards if fits(sizes, args[1]) else shards)(*args)
+
     in_specs = (
         P("fs", None),
         P(None, "fs", "tp"),
@@ -282,4 +687,4 @@
         P("fs", None),
     )
     out_specs = (P("tp", None, None), P("tp", None, None), P("tp", None, None), P("fs", "tp"))
-    return jax.shard_map(shards, mesh=mesh, in_specs=in_specs, out_specs=out_specs, check_vma=False)
+    return jax.shard_map(step, mesh=mesh, in_specs=in_specs, out_specs=out_specs, check_vma=False)

time: 607 us -> 579 us (0.954)
  Pallas kernels: 47.1 us -> 534 us
  waiting for transfers between devices: 465 us -> 18.9 us
  local copies, waits for them, and re-layouts: 37.4 us -> 11.9 us
  starting transfers between devices: 19 us -> 4.98 us
  between operations: 13.9 us -> 0.88 us
  other arithmetic: 19.3 us -> 6.33 us
    pallas_call x6, Pallas kernels: 47.1 us -> 534 us  [the longest x1 477 us: gather(): pl.pallas_call(kernel, in_specs=[pl.BlockSpec(memory_space=pl.ANY)] * 2,...]
    all_gather x3 -> x0, waiting for transfers between devices: 290 us -> none  [the longest x1 190 us: shards(): lax.all_gather(jnp.concatenate([up_moved, down_moved[:, :main]], axis=1),...]
    all_to_all x4 -> x1, waiting for transfers between devices: 174 us -> 8.26 us  [mix(): lax.all_to_all(partial_value.reshape(CAP, tp_count, -1), 'tp', split_axis...]
    all_gather x1 -> x0, local copies, waits for them, and re-layouts: 15.6 us -> none  [shards(): lax.all_gather(spread(gate_train, gain), 'fs', axis=0, tiled=True)]
    all_to_all x4 -> x1, starting transfers between devices: 18.8 us -> 3.69 us  [mix(): lax.all_to_all(partial_value.reshape(CAP, tp_count, -1), 'tp', split_axis...]
    ppermute x0 -> x1, waiting for transfers between devices: none -> 10.6 us  [line_shards(): arrived = lax.ppermute(kept, 'fs', [(1, 0), (count - 2, count - 1)])]
    reshape x2 -> x0, other arithmetic: 10.3 us -> none  [arrange(): shaped.transpose(0, 2, 3, 1).reshape(tp_count, piece_width, row_count)]
  transfers between devices with their start and end apart: 7 -> 2, of which waited for: 7 -> 2; matrix products, arithmetic and copies ran while one was open for 8% -> 2% of each run, Pallas kernels for 7% -> 6%
where the time goes in v1:
time: 579 us; the launch traced here: 578 us
  Pallas kernels  534 us (92%)
  waiting for transfers between devices  18.9 us (3%)
  local copies, waits for them, and re-layouts  11.9 us (2%)
  other arithmetic  6.33 us (1%)
    pallas_call x1, Pallas kernels, gather(): pl.pallas_call(kernel, in_specs=[pl.BlockSpec(memory_space=pl.ANY)] * 2,...  477 us
    pallas_call x3, Pallas kernels, join_call(): pl.pallas_call(kernel, grid=(tp_count,), in_specs=[pl.BlockSpec((count, 1...  33.7 us
    pallas_call x1, Pallas kernels, join_far(): pl.pallas_call(kernel, grid_spec=pltpu.PrefetchScalarGridSpec(num_scalar_...  11.8 us
  transfers between devices with their start and end apart: 2, of which 2 were waited for; matrix products, arithmetic and copies ran while one was open for 2% of the time, Pallas kernels for 6%

profile of v1, /device:TPU:0, one launch (start us, length us, event | category | flops | bytes accessed | tf_op | source)
XLA Modules:
  0.0 577.9 jit_solution(12623023863550816794)
XLA Ops:
  0.6 1.3 broadcast_in_dim.36.gain_ref
  1.9 11.3 %shard_map.102 = (bf16[3,8,288,512]{3,2,1,0:T(8,128)(2,1)}, bf16[3,8,144,128]{3,2,1,0:T(8,128)(2,1)}) custom-call(s32[1]{0:T(128)} %bitcast.odd_ref, f32[8,288,576]{2,1,0:T(8,128)} %bitcast.31, f32[8,288,576]{2,1,0:T(8,128)} %bitcast.32, f32[8,288,576]{2,1,0:T(8,128)} %bitcast.33, f32[1,576]{1,0:T(1,128)} %broadcast_in_dim.36.gain_ref), custom_call_target="tpu_custom_call" | custom-call | flops 3981312 | bytes 23887872 | tf_op jit(solution)/shard_map/pallas_call | solution.py:320
  13.2 477.0 %shard_map.103 = (bf16[4,3,8,288,512]{4,3,2,1,0:T(8,128)(2,1)}, bf16[4,3,8,144,128]{4,3,2,1,0:T(8,128)(2,1)}) custom-call(bf16[3,8,288,512]{3,2,1,0:T(8,128)(2,1)} %get-tuple-element.21.own_main, bf16[3,8,144,128]{3,2,1,0:T(8,128)(2,1)} %get-tuple-element.22.own_rest), custom_call_target="tpu_custom_call" | custom-call | flops 1000000000 | bytes 47775744 | tf_op jit(solution)/shard_map/pallas_call | solution.py:471
  490.2 1.9 dynamic-slice_bitcast_fusion.kept_ref
  492.2 1.3 collective-permute-start
  493.8 0.6 reduce-window.19
  494.7 2.7 gather_fusion.1
  497.7 0.3 reduce-window.15
  498.6 0.6 pad_add_fusion.scalar_ref
  499.2 1.1 convolution_convert_fusion.chosen_ref
  500.3 11.5 %shard_map.105 = (bf16[2304,2304]{1,0:T(8,128)(2,1)}, f32[8,72,288]{2,1,0:T(8,128)}) custom-call(bf16[4,3,8,288,512]{4,3,2,1,0:T(8,128)(2,1)} %get-tuple-element.25.main_ref, bf16[4,3,8,144,128]{4,3,2,1,0:T(8,128)(2,1)} %get-tuple-element.26.rest_ref, bf16[72,2304]{1,0:T(8,128)(2,1)} %convolution_convert_fusion.chosen_ref), custom_call_target="tpu_custom_call" | custom-call | flops 5308416000 | bytes 21233664 | tf_op jit(solution)/shard_map/pallas_call | solution.py:515
  511.8 11.6 %shard_map.104 = (bf16[2304,2304]{1,0:T(8,128)(2,1)}, f32[8,72,288]{2,1,0:T(8,128)}) custom-call(bf16[4,3,8,288,512]{4,3,2,1,0:T(8,128)(2,1)} %get-tuple-element.25.main_ref, bf16[4,3,8,144,128]{4,3,2,1,0:T(8,128)(2,1)} %get-tuple-element.26.rest_ref, bf16[72,2304]{1,0:T(8,128)(2,1)} %convolution_convert_fusion.chosen_ref), custom_call_target="tpu_custom_call" | custom-call | flops 5308416000 | bytes 21233664 | tf_op jit(solution)/shard_map/pallas_call | solution.py:515
  523.4 2.2 multiply_convert_fusion.hidden_ref
  525.6 10.6 %shard_map.106 = (bf16[2304,2304]{1,0:T(8,128)(2,1)}, f32[72,2304]{1,0:T(8,128)}) custom-call(bf16[4,3,8,288,512]{4,3,2,1,0:T(8,128)(2,1)} %get-tuple-element.25.main_ref, bf16[4,3,8,144,128]{4,3,2,1,0:T(8,128)(2,1)} %get-tuple-element.26.rest_ref, bf16[8,72,288]{2,1,0:T(8,128)(2,1)} %multiply_convert_fusion.hidden_ref), custom_call_target="tpu_custom_call" | custom-call | flops 5308416000 | bytes 21233664 | tf_op jit(solution)/shard_map/pallas_call | solution.py:515
  536.2 10.6 %collective-permute-done.arrived_ref = bf16[8,288,512]{2,1,0:T(8,128)(2,1)} collective-permute-done((bf16[8,288,512]{2,1,0:T(8,128)(2,1)S(1)}, bf16[8,288,512]{2,1,0:T(8,128)(2,1)}, u32[]{:S(2)}, u32[]{:S(2)}) %collective-permute-start) | collective-permute-done | bytes 2359328 | tf_op jit(solution)/shard_map/ppermute | solution.py:656
  546.8 11.8 %shard_map.107 = (bf16[2304,2304]{1,0:T(8,128)(2,1)}, f32[72,512]{1,0:T(8,128)}) custom-call(s32[2]{0:T(128)} %pad_add_fusion.scalar_ref, bf16[8,288,512]{2,1,0:T(8,128)(2,1)} %collective-permute-done.arrived_ref, bf16[8,288,512]{2,1,0:T(8,128)(2,1)} %copy-done, ...), custom_call_target="tpu_custom_call", output_to_operand_aliasing={{0}: (4, {})} | custom-call | flops 169869312 | bytes 7077888 | tf_op jit(solution)/shard_map/pallas_call | solution.py:592
  558.7 0.9 constant_dynamic-update-slice_fusion
  559.6 0.7 reshape.77
  560.3 0.8 copy.61
  561.2 3.7 all-to-all-start
  565.4 8.3 %all-to-all-done = bf16[72,8,288]{2,0,1:T(8,128)(2,1)S(1)} async-done(((bf16[72,8,288]{2,0,1:T(8,128)(2,1)}), bf16[72,8,288]{2,0,1:T(8,128)(2,1)S(1)}, u32[]{:S(2)}, u32[]{:S(2)}) %all-to-all-start) | async-done | bytes 331808 | tf_op jit(solution)/shard_map/all_to_all | solution.py:638
  573.7 1.7 gather_fusion
  575.5 0.3 reshape.86
  575.8 2.0 multiply_reduce_fusion
  (40 shorter events, 2.1 us)
Async XLA Ops:
  13.2 480.2 %copy-start.4 = (s32[192,2]{0,1:T(2,128)S(1)}, s32[192,2]{0,1:T(2,128)}, u32[]{:S(2)}) copy-start(s32[192,2]{0,1:T(2,128)} %param.12) | copy-start | bytes 4612
  492.2 5.3 copy-start
  492.2 54.7 %collective-permute-start = (bf16[8,288,512]{2,1,0:T(8,128)(2,1)S(1)}, bf16[8,288,512]{2,1,0:T(8,128)(2,1)}, u32[]{:S(2)}, u32[]{:S(2)}) collective-permute-start(bf16[8,288,512]{2,1,0:T(8,128)(2,1)S(1)} %dynamic-slice_bitcast_fusion.kept_ref), channel_id=1, source_target_pairs={{8,0},{16,24},{9,1},{17,25},{10,2},{18,26},{11,3},{19,27},{12,4},{... | collective-permute-start | bytes 7077896 | tf_op jit(solution)/shard_map/ppermute | solution.py:656
  494.7 3.6 copy-start.1
  511.8 11.6 %copy-start.2 = (f32[8,72,288]{2,1,0:T(8,128)S(1)}, f32[8,72,288]{2,1,0:T(8,128)}, u32[]{:S(2)}) copy-start(f32[8,72,288]{2,1,0:T(8,128)} %get-tuple-element.32) | copy-start | bytes 1990660
  546.8 11.8 %copy-start.3 = (f32[72,2304]{1,0:T(8,128)S(1)}, f32[72,2304]{1,0:T(8,128)}, u32[]{:S(2)}) copy-start(f32[72,2304]{1,0:T(8,128)} %get-tuple-element.36) | copy-start | bytes 1990660
  546.8 18.4 %copy-start.5 = (f32[192,2]{0,1:T(2,128)S(1)}, f32[192,2]{0,1:T(2,128)}, u32[]{:S(2)}) copy-start(f32[192,2]{0,1:T(2,128)} %param.13) | copy-start | bytes 4612
  561.2 12.5 %all-to-all-start = ((bf16[72,8,288]{2,0,1:T(8,128)(2,1)}), bf16[72,8,288]{2,0,1:T(8,128)(2,1)S(1)}, u32[]{:S(2)}, u32[]{:S(2)}) async-start(bf16[72,8,288]{2,0,1:T(8,128)(2,1)} %copy.61), calls=%async_computation | async-start | bytes 884736 | tf_op jit(solution)/shard_map/all_to_all | solution.py:638

commit v2 on v1

--- a/solution.py
+++ b/solution.py
@@ -4,6 +4,7 @@
 from jax.experimental import pallas as pl
 from jax.experimental.pallas import tpu as pltpu
 from jax.sharding import PartitionSpec as P
+
 
 CAP = 72
 
@@ -281,6 +282,7 @@
         and count % 2 == 0
         and features % 128 == 64
         and units % 32 == 0
+        and units <= features - 64
     )
 
 
@@ -338,15 +340,15 @@
     )(odd, gate, up, down, gain)
 
 
-def gather(own_main, own_rest, count):
-    mats, tp_count, units, wide = own_main.shape
-    half = own_rest.shape[2]
-    pieces = mats * tp_count
+def gather(own_main, own_rest, tokens, info, count, held):
+    mats, tp_count, half = own_rest.shape[:3]
+    pieces, units, wide = own_main.shape
     bits = tp_count.bit_length() - 1
 
     def kernel(
-        own_main, own_rest, main, rest, hold, hold_rest, load_sem, keep_sem, plane_send, plane_recv,
-        plane_rest_send, plane_rest_recv, line_send, line_recv, line_rest_send, line_rest_recv,
+        own_main, own_rest, tokens, info, main, rest, near_tokens, near_info, early, last, hold, hold_rest, load_sem, keep_sem,
+        plane_send, plane_recv, plane_rest_send, plane_rest_recv, line_send, line_recv, line_rest_send,
+        line_rest_recv, near_send, near_recv, pass_hold, pass_load, pass_keep,
     ):
         z = lax.axis_index("fs")
         t = lax.axis_index("tp")
@@ -361,7 +363,7 @@
         def plane(m, p):
             e = peer(p)
             return pltpu.make_async_remote_copy(
-                own_main.at[m, e], main.at[z, m, t], plane_send.at[m, p], plane_recv.at[m, p],
+                own_main.at[m * tp_count + e], main.at[z, m * tp_count + t], plane_send.at[m, p], plane_recv.at[m, p],
                 device_id={"fs": z, "tp": e}, device_id_type=pl.DeviceIdType.MESH,
             )
 
@@ -375,9 +377,9 @@
         def line(way, step, i):
             block = z + step if way == 0 else z - step
             target = z - 1 if way == 0 else z + 1
-            m, e = i // tp_count, peer(i % tp_count)
+            piece = main.at[block, i // tp_count * tp_count + peer(i % tp_count)]
             return pltpu.make_async_remote_copy(
-                main.at[block, m, e], main.at[block, m, e], line_send.at[way, step], line_recv.at[way, step, i],
+                piece, piece, line_send.at[way, step], line_recv.at[way, step, i],
                 device_id={"fs": target, "tp": t}, device_id_type=pl.DeviceIdType.MESH,
             )
 
@@ -390,7 +392,7 @@
             )
 
         for m in range(mats):
-            pltpu.make_async_copy(own_main.at[m, t], hold.at[m], load_sem.at[0, m]).start()
+            pltpu.make_async_copy(own_main.at[m * tp_count + t], hold.at[m], load_sem.at[0, m]).start()
             pltpu.make_async_copy(own_rest.at[m, t], hold_rest.at[m], load_sem.at[1, m]).start()
 
         for m in range(mats):
@@ -400,8 +402,8 @@
                 plane_rest(m, p).start()
 
         for m in range(mats):
-            pltpu.make_async_copy(own_main.at[m, t], hold.at[m], load_sem.at[0, m]).wait()
-            pltpu.make_async_copy(hold.at[m], main.at[z, m, t], keep_sem.at[0, m]).start()
+            pltpu.make_async_copy(own_main.at[m * tp_count + t], hold.at[m], load_sem.at[0, m]).wait()
+            pltpu.make_async_copy(hold.at[m], main.at[z, m * tp_count + t], keep_sem.at[0, m]).start()
             pltpu.make_async_copy(own_rest.at[m, t], hold_rest.at[m], load_sem.at[1, m]).wait()
             pltpu.make_async_copy(hold_rest.at[m], rest.at[z, m, t], keep_sem.at[1, m]).start()
 
@@ -411,30 +413,48 @@
         def sends(way):
             return z >= 1 if way == 0 else z <= count - 2
 
-        late = pieces - tp_count
+        def near(k):
+            source, target = ((tokens, near_tokens), (info, near_info))[k]
+            inward = jnp.where(z == 0, 1, count - 2)
+            return pltpu.make_async_remote_copy(
+                source, target, near_send.at[k], near_recv.at[k],
+                device_id={"fs": inward, "tp": t}, device_id_type=pl.DeviceIdType.MESH,
+            )
+
+        def into_end(way, step, m, p, sender):
+            if m < mats - 1 or step < count - 3:
+                return True
+            end = sender == 1 if way == 0 else sender == count - 2
+            if step == count - 2:
+                return jnp.logical_not(end)
+            return jnp.logical_not(end & (peer(p) >= tp_count - held))
+
+        def leaves(way, step, m, p):
+            return into_end(way, step, m, p, z)
+
+        def arrives(way, step, m, p):
+            return into_end(way, step, m, p, z + 1 if way == 0 else z - 1)
+
         for step in range(count):
             for m in range(mats):
-                final = step == count - 1
-                last = final and m == mats - 1
-                skip = step == count - 2 and m == mats - 1
                 if step == 0:
-                    pltpu.make_async_copy(hold.at[m], main.at[z, m, t], keep_sem.at[0, m]).wait()
+                    pltpu.make_async_copy(hold.at[m], main.at[z, m * tp_count + t], keep_sem.at[0, m]).wait()
                     pltpu.make_async_copy(hold_rest.at[m], rest.at[z, m, t], keep_sem.at[1, m]).wait()
 
                 @pl.loop(0, tp_count)
-                def _(p, step=step, m=m, last=last, skip=skip, final=final):
+                def _(p, step=step, m=m):
                     i = m * tp_count + p
                     if step == 0:
                         @pl.when(p >= 1)
                         def _():
                             plane(m, p).wait_recv()
                     for way in range(2):
-                        if step > 0 and not last:
-                            @pl.when(has(way, step))
+                        if step > 0:
+                            @pl.when(has(way, step) & arrives(way, step - 1, m, p))
                             def _(way=way):
                                 line(way, step - 1, i).wait_recv()
-                        if not final and not skip:
-                            @pl.when(has(way, step) & sends(way))
+                        if step < count - 1:
+                            @pl.when(has(way, step) & sends(way) & leaves(way, step, m, p))
                             def _(way=way):
                                 line(way, step, i).start()
 
@@ -447,22 +467,67 @@
                         @pl.when(has(way, step))
                         def _(way=way, step=step, m=m):
                             line_rest(way, step - 1, m).wait_recv()
-                    if not final:
+                    if step < count - 1:
                         @pl.when(has(way, step) & sends(way))
                         def _(way=way, step=step, m=m):
                             line_rest(way, step, m).start()
+            if step == 0:
+                @pl.when((z == 0) | (z == count - 1))
+                def _():
+                    near(0).start()
+                    near(1).start()
+
+        @pl.when((z == 1) | (z == count - 2))
+        def _():
+            low = z < count // 2
+            far, after_far = jnp.where(low, count - 1, 0), jnp.where(low, count - 2, 1)
+            first = pieces - held
+            found = [main.at[far, pieces - tp_count + i] for i in range(tp_count)]
+            found += [main.at[after_far, first + i] for i in range(held)]
+            goal = [early.at[i] for i in range(tp_count + held - 1)] + [last.at[0]]
+            loads = [pltpu.make_async_copy(f, pass_hold.at[i], pass_load.at[i]) for i, f in enumerate(found)]
+            keeps = [pltpu.make_async_copy(pass_hold.at[i], g, pass_keep.at[i]) for i, g in enumerate(goal)]
+            for load in loads:
+                load.start()
+            for load, keep in zip(loads, keeps):
+                load.wait()
+                keep.start()
+            for keep in keeps:
+                keep.wait()
 
         for m in range(mats):
             @pl.loop(1, tp_count)
             def _(p, m=m):
                 plane(m, p).wait_send()
                 plane_rest(m, p).wait_send()
+
+        @pl.when((z == 0) | (z == count - 1))
+        def _():
+            near(0).wait_send()
+            near(1).wait_send()
+
+        @pl.when((z == 1) | (z == count - 2))
+        def _():
+            near(0).wait_recv()
+            near(1).wait_recv()
+
         for step in range(count - 1):
             for way in range(2):
                 @pl.when(has(way, step) & sends(way))
                 def _(way=way, step=step):
-                    sent = main.at[z, pl.ds(0, mats - 1 if step == count - 2 else mats)]
-                    pltpu.make_async_copy(sent, sent, line_send.at[way, step]).wait()
+                    end = z == (1 if way == 0 else count - 2)
+
+                    def settle(number, way=way, step=step):
+                        sent = main.at[z, pl.ds(0, number)]
+                        pltpu.make_async_copy(sent, sent, line_send.at[way, step]).wait()
+
+                    if step == count - 2:
+                        settle(pieces - tp_count)
+                    elif step == count - 3:
+                        pl.when(end)(lambda: settle(pieces - held))
+                        pl.when(jnp.logical_not(end))(lambda: settle(pieces))
+                    else:
+                        settle(pieces)
                     for m in range(mats):
                         line_rest(way, step, m).wait_send()
 
@@ -470,11 +535,15 @@
     sent = 2 * (count - 1) * (own_main.size + own_rest.size)
     return pl.pallas_call(
         kernel,
-        in_specs=[pl.BlockSpec(memory_space=pl.ANY)] * 2,
-        out_specs=[pl.BlockSpec(memory_space=pl.ANY)] * 2,
+        in_specs=[pl.BlockSpec(memory_space=pl.ANY)] * 4,
+        out_specs=[pl.BlockSpec(memory_space=pl.ANY)] * 6,
         out_shape=[
             jax.ShapeDtypeStruct((count,) + own_main.shape, own_main.dtype),
             jax.ShapeDtypeStruct((count,) + own_rest.shape, own_rest.dtype),
+            jax.ShapeDtypeStruct(tokens.shape, tokens.dtype),
+            jax.ShapeDtypeStruct(info.shape, info.dtype),
+            jax.ShapeDtypeStruct((tp_count + held - 1, units, wide), own_main.dtype),
+            jax.ShapeDtypeStruct((1, units, wide), own_main.dtype),
         ],
         scratch_shapes=[
             pltpu.VMEM((mats, units, wide), own_main.dtype),
@@ -489,18 +558,23 @@
             dma((2, count - 1, pieces)),
             dma((2, count - 1, mats)),
             dma((2, count - 1, mats)),
+            dma((2,)),
+            dma((2,)),
+            pltpu.VMEM((tp_count + held, units, wide), own_main.dtype),
+            dma((tp_count + held,)),
+            dma((tp_count + held,)),
         ],
         compiler_params=pltpu.CompilerParams(has_side_effects=True),
         cost_estimate=pl.CostEstimate(flops=10**9, bytes_accessed=2 * sent, transcendentals=0),
-    )(own_main, own_rest)
+    )(own_main, own_rest, tokens, info)
 
 
 def joined(main_ref, rest_ref, out_ref):
-    count, _, _, units, wide = main_ref.shape
+    count, _, units, wide = main_ref.shape
     features = wide + 64
     half = units // 2
     for block in range(count):
-        out_ref[:, pl.ds(main_start(block, features), wide)] = main_ref[block, 0, 0]
+        out_ref[:, pl.ds(main_start(block, features), wide)] = main_ref[block, 0]
     for block in range(0, count, 2):
         first, second = rest_ref[block, 0, 0], rest_ref[block + 1, 0, 0]
         place = pl.ds(block * features + wide, 128)
@@ -509,14 +583,14 @@
 
 
 def join_call(main, rest, which, kernel, operand, operand_spec, product_spec, product_shape):
-    count, mats, tp_count, units, wide = main.shape
-    half = rest.shape[3]
+    count, _, tp_count, half = rest.shape[:4]
+    units, wide = main.shape[2:]
     features = count * (wide + 64)
     return pl.pallas_call(
         kernel,
         grid=(tp_count,),
         in_specs=[
-            pl.BlockSpec((count, 1, 1, units, wide), lambda i: (0, which, i, 0, 0)),
+            pl.BlockSpec((count, 1, units, wide), lambda i: (0, which * tp_count + i, 0, 0)),
             pl.BlockSpec((count, 1, 1, half, 128), lambda i: (0, which, i, 0, 0)),
             operand_spec,
         ],
@@ -534,7 +608,7 @@
 
 
 def join_in(main, rest, which, chosen):
-    tp_count, units = main.shape[2:4]
+    tp_count, units = rest.shape[2], main.shape[2]
     slots, features = chosen.shape
 
     def kernel(main_ref, rest_ref, chosen_ref, new_ref, product_ref):
@@ -552,8 +626,8 @@
 
 
 def join_out(main, rest, which, hidden):
-    tp_count, slots, units = hidden.shape
-    features = main.shape[0] * (main.shape[4] + 64)
+    _, slots, units = hidden.shape
+    features = main.shape[0] * (main.shape[3] + 64)
 
     def kernel(main_ref, rest_ref, hidden_ref, new_ref, total_ref):
         joined(main_ref, rest_ref, new_ref)
@@ -572,102 +646,130 @@
     )
 
 
-def join_far(arrived, kept, use_arrived, far_start, last_start, hidden, base):
-    tp_count, units, wide = arrived.shape
-    slots = hidden.shape[1]
-    size = 256 if (wide % 256 == 0 and last_start % 256 == 0) else 128
-
-    def kernel(scalar_ref, arrived_ref, kept_ref, hidden_ref, base_ref, new_ref, total_ref):
-        value = jnp.where(scalar_ref[1] == 1, arrived_ref[0], kept_ref[0])
-        new_ref[...] = value
-
-        @pl.when(pl.program_id(1) == 0)
+def place_late(arrived, places, base, count):
+    pieces, units, wide = arrived.shape
+    start = jnp.stack([column for _, _, column in places])
+
+    def kernel(start_ref, arrived_ref, base_ref, new_ref, hold, load_sem, keep_sem):
+        z = lax.axis_index("fs")
+
+        @pl.when((z == 0) | (z == count - 1))
         def _():
-            total_ref[...] = jnp.zeros_like(total_ref)
-
-        total_ref[...] += jnp.dot(hidden_ref[0], value, preferred_element_type=jnp.float32)
-
-    scalars = jnp.stack([far_start // size, use_arrived.astype(jnp.int32)])
-    piece = pl.BlockSpec((1, units, size), lambda j, i, s: (i, 0, j))
+            loads = [pltpu.make_async_copy(arrived_ref.at[i], hold.at[i], load_sem.at[i]) for i in range(pieces)]
+            keeps = [
+                pltpu.make_async_copy(
+                    hold.at[i],
+                    new_ref.at[
+                        pl.ds(row * units, units), pl.ds(pl.multiple_of(start_ref[i], 128), wide)
+                    ],
+                    keep_sem.at[i],
+                )
+                for i, row, _ in places
+            ]
+            for load in loads:
+                load.start()
+            for load, keep in zip(loads, keeps):
+                load.wait()
+                keep.start()
+            for keep in keeps:
+                keep.wait()
+
     return pl.pallas_call(
         kernel,
         grid_spec=pltpu.PrefetchScalarGridSpec(
             num_scalar_prefetch=1,
-            grid=(wide // size, tp_count),
-            in_specs=[
-                piece, piece,
-                pl.BlockSpec((1, slots, units), lambda j, i, s: (i, 0, 0)),
-                pl.BlockSpec(memory_space=pl.ANY),
+            grid=(1,),
+            in_specs=[pl.BlockSpec(memory_space=pl.ANY)] * 2,
+            out_specs=pl.BlockSpec(memory_space=pl.ANY),
+            scratch_shapes=[
+                pltpu.VMEM(arrived.shape, arrived.dtype),
+                pltpu.SemaphoreType.DMA((pieces,)),
+                pltpu.SemaphoreType.DMA((pieces,)),
             ],
-            out_specs=[
-                pl.BlockSpec((units, size), lambda j, i, s: (i, s[0] + j)),
-                pl.BlockSpec((slots, size), lambda j, i, s: (0, j)),
-            ],
-        ),
-        out_shape=[
-            jax.ShapeDtypeStruct(base.shape, base.dtype),
-            jax.ShapeDtypeStruct((slots, wide), jnp.float32),
-        ],
-        input_output_aliases={4: 0},
+        ),
+        out_shape=jax.ShapeDtypeStruct(base.shape, base.dtype),
+        input_output_aliases={2: 0},
         cost_estimate=pl.CostEstimate(
-            flops=2 * slots * arrived.size, bytes_accessed=6 * arrived.size, transcendentals=0
-        ),
-    )(scalars, arrived, kept, hidden, base)
+            flops=500 * arrived.size, bytes_accessed=4 * arrived.size, transcendentals=0
+        ),
+    )(start, arrived, base)
 
 
 def pick(tokens, routes, expert):
     tokens_wide = tokens.astype(jnp.float32)
     normed = (
         tokens_wide
-        * lax.rsqrt(jnp.mean(tokens_wide * tokens_wide, axis=1, keepdims=True) + norm_eps)
+        * lax.rsqrt(jnp.mean(tokens_wide * tokens_wide, axis=2, keepdims=True) + norm_eps)
     ).astype(jnp.bfloat16)
-    member = jnp.any(routes == expert, axis=1)
-    slot_index = jnp.cumsum(member.astype(jnp.int32)) - 1
+    member = jnp.any(routes == expert, axis=2)
+    slot_index = jnp.cumsum(member.astype(jnp.int32), axis=1) - 1
     marked = jnp.where(member, slot_index, -1)
-    picker = (marked[None, :] == jnp.arange(CAP, dtype=jnp.int32)[:, None]).astype(jnp.bfloat16)
-    return jnp.dot(picker, normed, preferred_element_type=jnp.float32).astype(jnp.bfloat16)
+    picker = (marked[:, None, :] == jnp.arange(CAP, dtype=jnp.int32)[None, :, None]).astype(jnp.bfloat16)
+    chosen = jnp.einsum("gcr,grd->gcd", picker, normed, preferred_element_type=jnp.float32)
+    return chosen.astype(jnp.bfloat16).reshape(-1, tokens.shape[2])
 
 
 def mix(partial_value, routes, route_weights, experts):
     tp_count = lax.axis_size("tp")
+    groups = routes.shape[0]
     labels = jnp.arange(experts, dtype=jnp.int32)
-    member_all = jnp.any(routes[:, :, None] == labels[None, None, :], axis=1)
-    slots_all = jnp.cumsum(member_all.astype(jnp.int32), axis=0) - 1
-    slot_pair = jnp.take_along_axis(slots_all, routes, axis=1)
-    flat_index = slot_pair * experts + routes
+    member_all = jnp.any(routes[:, :, :, None] == labels, axis=2)
+    slots_all = jnp.cumsum(member_all.astype(jnp.int32), axis=1) - 1
+    slot_pair = jnp.take_along_axis(slots_all, routes, axis=2)
+    first = CAP * jnp.arange(groups, dtype=jnp.int32)[:, None, None]
+    flat_index = (first + slot_pair) * experts + routes
     received = lax.all_to_all(
-        partial_value.reshape(CAP, tp_count, -1), "tp", split_axis=1, concat_axis=1, tiled=True
-    )
-    summed = received.astype(jnp.float32).reshape(CAP * experts, -1)
+        partial_value.reshape(groups * CAP, tp_count, -1), "tp", split_axis=1, concat_axis=1, tiled=True
+    )
+    summed = received.astype(jnp.float32).reshape(groups * CAP * experts, -1)
     picked = jnp.take(summed, flat_index, axis=0)
-    return jnp.sum(route_weights[:, :, None] * picked, axis=1).astype(jnp.bfloat16)
+    return jnp.sum(route_weights[:, :, :, None] * picked, axis=2).astype(jnp.bfloat16)
 
 
 def line_shards(tokens, gate_train, up_train, down_train, gain, routes, route_weights):
     count = lax.axis_size("fs")
     place = lax.axis_index("fs")
-    experts, features, units = gate_train.shape
+    experts, features, _ = gate_train.shape
+    held = experts - 3
+    outward = [(1, 0), (count - 2, count - 1)]
     own_main, own_rest = prepare(
         gate_train.transpose(0, 2, 1), up_train.transpose(0, 2, 1), down_train.transpose(0, 2, 1), gain[None, :]
     )
-    main, rest = gather(own_main, own_rest, count)
-    far = jnp.where(place < count // 2, count - 1, 0)
-    kept = lax.dynamic_slice(main, (far, 2, 0, 0, 0), (1, 1) + main.shape[2:])[0, 0]
-    arrived = lax.ppermute(kept, "fs", [(1, 0), (count - 2, count - 1)])
-    main, rest, tokens, routes, route_weights = lax.optimization_barrier(
-        (main, rest, tokens, routes, route_weights)
-    )
-    chosen = pick(tokens, routes, lax.axis_index("tp"))
+    info = jnp.concatenate([routes.T.astype(jnp.float32), route_weights.T])
+    main, rest, near_tokens, near_info, kept_early, kept_last = gather(
+        own_main.reshape((-1,) + own_main.shape[2:]), own_rest, tokens, info, count, held
+    )
+    low = place < count // 2
+    far_start = jnp.where(low, main_start(count - 1, features), main_start(0, features)).astype(jnp.int32)
+    next_start = jnp.where(low, main_start(count - 2, features), main_start(1, features)).astype(jnp.int32)
+    arrived_early = lax.ppermute(kept_early, "fs", outward)
+
+    main, rest, near_tokens, near_info, tokens, info = lax.optimization_barrier(
+        (main, rest, near_tokens, near_info, tokens, info)
+    )
+    both_info = jnp.stack([info, near_info])
+    routed = routes.shape[1]
+    both_routes = both_info[:, :routed].astype(jnp.int32).transpose(0, 2, 1)
+    both_weights = both_info[:, routed:].transpose(0, 2, 1)
+    chosen = pick(jnp.stack([tokens, near_tokens]), both_routes, lax.axis_index("tp"))
     gate_new, gate_pre = join_in(main, rest, 0, chosen)
     up_new, up_pre = join_in(main, rest, 1, chosen)
     hidden = (jax.nn.silu(gate_pre) * up_pre).astype(jnp.bfloat16)
     down_new, total = join_out(main, rest, 2, hidden)
+    both_mixed = mix(total.astype(jnp.bfloat16), both_routes, both_weights, experts)
+    wide = kept_last.shape[2]
+    kept_rows = kept_last.reshape(-1, wide)
+    mixed_rows = jnp.pad(both_mixed[1], ((0, 0), (0, wide - both_mixed.shape[2])))
+    arrived_rows = lax.ppermute(jnp.concatenate([kept_rows, mixed_rows]), "fs", outward)
+    arrived_last = arrived_rows[: kept_rows.shape[0]].reshape(kept_last.shape)
+    near_mixed = arrived_rows[kept_rows.shape[0] :, : both_mixed.shape[2]]
+    first = experts - held
+    early = [(i, i, far_start) for i in range(experts)]
+    early += [(experts + i, first + i, next_start) for i in range(held - 1)]
+    down_new = place_late(arrived_early, early, down_new, count)
+    down_new = place_late(arrived_last, [(0, experts - 1, next_start)], down_new, count)
     at_end = (place == 0) | (place == count - 1)
-    last_start = main_start(count - 1, features)
-    far_start = jnp.where(far == 0, 0, last_start).astype(jnp.int32)
-    down_new, far_total = join_far(arrived, kept, at_end, far_start, last_start, hidden, down_new)
-    total = lax.dynamic_update_slice(total, far_total, (0, far_start))
-    mixed = mix(total.astype(jnp.bfloat16), routes, route_weights, experts)
+    mixed = jnp.where(at_end, near_mixed, both_mixed[0])
     return (gate_new[None], up_new[None], down_new[None], mixed)
 
 
@@ -675,7 +777,9 @@
     sizes = (mesh.shape["fs"], mesh.shape["tp"])
 
     def step(*args):
-        return (line_shards if fits(sizes, args[1]) else shards)(*args)
+        if not fits(sizes, args[1]):
+            return shards(*args)
+        return line_shards(*args)
 
     in_specs = (
         P("fs", None),

time: 579 us -> 562 us (0.971)
  Pallas kernels: 534 us -> 498 us
  other arithmetic: 6.33 us -> 13.1 us
  waiting for transfers between devices: 18.9 us -> 25.1 us
    pallas_call x2 -> x3, Pallas kernels: 489 us -> 451 us  [the longest x1 446 us: gather(): pl.pallas_call(kernel, in_specs=[pl.BlockSpec(memory_space=pl.ANY)] * 4,...]
    ppermute x1 -> x2, waiting for transfers between devices: 10.6 us -> 12.1 us  [the longest x1 12.1 us: line_shards(): lax.ppermute(jnp.concatenate([kept_rows, mixed_rows]), 'fs', outward)]
  transfers between devices with their start and end apart: 2 -> 3, of which waited for: 2 -> 2; matrix products, arithmetic and copies ran while one was open for 2% -> 5% of each run, Pallas kernels for 6% -> 6%
where the time goes in v2:
time: 562 us; the launch traced here: 561 us
  Pallas kernels  498 us (89%)
  waiting for transfers between devices  25.1 us (4%)
  local copies, waits for them, and re-layouts  15.8 us (3%)
  other arithmetic  13.1 us (2%)
  starting transfers between devices  6.33 us (1%)
    pallas_call x1, Pallas kernels, gather(): pl.pallas_call(kernel, in_specs=[pl.BlockSpec(memory_space=pl.ANY)] * 4,...  446 us
    pallas_call x3, Pallas kernels, join_call(): pl.pallas_call(kernel, grid=(tp_count,), in_specs=[pl.BlockSpec((count, 1...  35.5 us
    all_to_all x1, waiting for transfers between devices, mix(): lax.all_to_all(partial_value.reshape(groups * CAP, tp_count, -1), 'tp', s...  13 us
    ppermute x1, waiting for transfers between devices, line_shards(): lax.ppermute(jnp.concatenate([kept_rows, mixed_rows]), 'fs', outward)  12.1 us
    pallas_call x1, Pallas kernels, prepare(): pl.pallas_call(kernel, grid_spec=pltpu.PrefetchScalarGridSpec(num_scalar_...  11.3 us
  transfers between devices with their start and end apart: 3, of which 2 were waited for; matrix products, arithmetic and copies ran while one was open for 5% of the time, Pallas kernels for 6%

profile of v2, /device:TPU:0, one launch (start us, length us, event | category | flops | bytes accessed | tf_op | source)
XLA Modules:
  0.0 560.6 jit_solution(9581331579431028230)
XLA Ops:
  0.6 1.3 broadcast_in_dim.37.gain_ref
  2.6 1.3 pad_maximum_fusion.3.info
  3.9 11.3 %shard_map.102 = (bf16[3,8,288,512]{3,2,1,0:T(8,128)(2,1)}, bf16[3,8,144,128]{3,2,1,0:T(8,128)(2,1)}) custom-call(s32[1]{0:T(128)} %bitcast.odd_ref, f32[8,288,576]{2,1,0:T(8,128)} %bitcast.57, f32[8,288,576]{2,1,0:T(8,128)} %bitcast.58, f32[8,288,576]{2,1,0:T(8,128)} %bitcast.59, f32[1,576]{1,0:T(1,128)} %broadcast_in_dim.37.gain_ref), custom_call_target="tpu_custom_call" | custom-call | flops 3981312 | bytes 23887872 | tf_op jit(solution)/shard_map/pallas_call | solution.py:322
  15.2 445.7 %shard_map.103 = (bf16[4,24,288,512]{3,2,1,0:T(8,128)(2,1)}, bf16[4,3,8,144,128]{4,3,2,1,0:T(8,128)(2,1)}, bf16[192,2304]{1,0:T(8,128)(2,1)}, f32[4,192]{1,0:T(4...) custom-call(bf16[24,288,512]{2,1,0:T(8,128)(2,1)} %bitcast.56, ...), custom_call_target="tpu_custom_call" | custom-call | flops 1000000000 | bytes 47775744 | tf_op jit(solution)/shard_map/pallas_call | solution.py:536
  460.9 1.3 collective-permute-start.1
  463.2 1.2 reduce-window.16
  464.7 6.1 %gather_fusion.1 = s32[768]{0:T(1024)S(1)} fusion(s32[2,192,8]{1,2,0:T(8,128)S(1)} %slice_add_fusion, s32[768]{0:T(1024)S(1)} %reshape.109), kind=kCustom, calls=%fused_computation.1 | custom fusion | bytes 15360 | tf_op jit(solution)/shard_map/jit(take_along_axis)/gather | solution.py:718
  472.8 1.4 convolution_convert_fusion
  474.2 12.0 %shard_map.105 = (bf16[2304,2304]{1,0:T(8,128)(2,1)}, f32[8,144,288]{2,1,0:T(8,128)}) custom-call(bf16[4,24,288,512]{3,2,1,0:T(8,128)(2,1)} %get-tuple-element.30.main_ref, bf16[4,3,8,144,128]{4,3,2,1,0:T(8,128)(2,1)} %get-tuple-element.31.rest_ref, bf16[144,2304]{1,0:T(8,128)(2,1)} %bitcast.62), custom_call_target="tpu_custom_call" | custom-call | flops 5308416000 | bytes 21233664 | tf_op jit(solution)/shard_map/pallas_call | solution.py:589
  486.3 12.3 %shard_map.104 = (bf16[2304,2304]{1,0:T(8,128)(2,1)}, f32[8,144,288]{2,1,0:T(8,128)}) custom-call(bf16[4,24,288,512]{3,2,1,0:T(8,128)(2,1)} %get-tuple-element.30.main_ref, bf16[4,3,8,144,128]{4,3,2,1,0:T(8,128)(2,1)} %get-tuple-element.31.rest_ref, bf16[144,2304]{1,0:T(8,128)(2,1)} %bitcast.63), custom_call_target="tpu_custom_call" | custom-call | flops 5308416000 | bytes 21233664 | tf_op jit(solution)/shard_map/pallas_call | solution.py:589
  498.6 2.9 multiply_convert_fusion.hidden_ref
  501.5 11.1 %shard_map.106 = (bf16[2304,2304]{1,0:T(8,128)(2,1)}, f32[144,2304]{1,0:T(8,128)}) custom-call(bf16[4,24,288,512]{3,2,1,0:T(8,128)(2,1)} %get-tuple-element.30.main_ref, bf16[4,3,8,144,128]{4,3,2,1,0:T(8,128)(2,1)} %get-tuple-element.31.rest_ref, bf16[8,144,288]{2,1,0:T(8,128)(2,1)} %multiply_convert_fusion.hidden_ref), custom_call_target="tpu_custom_call" | custom-call | flops 5308416000 | bytes 21233664 | tf_op jit(solution)/shard_map/pallas_call | solution.py:589
  512.6 1.4 convert_element_type.45
  514.0 1.3 reshape.93
  515.4 1.0 copy.34
  516.4 3.7 all-to-all-start
  520.8 13.0 %all-to-all-done = bf16[144,8,288]{2,0,1:T(8,128)(2,1)S(1)} async-done(((bf16[144,8,288]{2,0,1:T(8,128)(2,1)}), bf16[144,8,288]{2,0,1:T(8,128)(2,1)S(1)}, u32[]{:S(2)}, u32[]{:S(2)}) %all-to-all-start) | async-done | bytes 663584 | tf_op jit(solution)/shard_map/all_to_all | solution.py:721
  533.9 2.1 gather_fusion
  536.8 2.8 multiply_reduce_fusion
  539.6 1.3 collective-permute-start
  541.6 12.1 %collective-permute-done = bf16[480,512]{1,0:T(8,128)(2,1)S(1)} collective-permute-done((bf16[480,512]{1,0:T(8,128)(2,1)S(1)}, bf16[480,512]{1,0:T(8,128)(2,1)S(1)}, u32[]{:S(2)}, u32[]{:S(2)}) %collective-permute-start) | collective-permute-done | bytes 491552 | tf_op jit(solution)/shard_map/ppermute | solution.py:763
  554.4 0.7 slice_bitcast_fusion.arrived_ref
  555.2 3.8 shard_map.107.base_ref
  558.9 1.7 shard_map.108
  (50 shorter events, 6.9 us)
Async XLA Ops:
  15.2 447.0 %copy-start.4 = (f32[4,192]{1,0:T(4,128)S(1)}, f32[4,192]{1,0:T(4,128)}, u32[]{:S(2)}) copy-start(f32[4,192]{1,0:T(4,128)} %pad_maximum_fusion.3.info) | copy-start | bytes 9220
  460.9 94.3 %collective-permute-start.1 = (bf16[12,288,512]{2,1,0:T(8,128)(2,1)}, bf16[12,288,512]{2,1,0:T(8,128)(2,1)}, u32[]{:S(2)}, u32[]{:S(2)}) collective-permute-start(bf16[12,288,512]{2,1,0:T(8,128)(2,1)} %get-tuple-element.42), channel_id=1, source_target_pairs={{8,0},{16,24},{9,1},{17,25},{10,2},{18,26},{11,3},{19,27},{12,4},{... | collective-permute-start | bytes 10616840 | tf_op jit(solution)/shard_map/ppermute | solution.py:745
  464.7 7.7 %copy-start = (bf16[192,2304]{1,0:T(8,128)(2,1)S(1)}, bf16[192,2304]{1,0:T(8,128)(2,1)}, u32[]{:S(2)}) copy-start(bf16[192,2304]{1,0:T(8,128)(2,1)} %tokens.1) | copy-start | bytes 2654212
  464.7 7.7 %copy-start.2 = (bf16[192,2304]{1,0:T(8,128)(2,1)S(1)}, bf16[192,2304]{1,0:T(8,128)(2,1)}, u32[]{:S(2)}) copy-start(bf16[192,2304]{1,0:T(8,128)(2,1)} %get-tuple-element.35) | copy-start | bytes 2654212
  486.3 12.3 %copy-start.1 = (f32[8,144,288]{2,1,0:T(8,128)S(1)}, f32[8,144,288]{2,1,0:T(8,128)}, u32[]{:S(2)}) copy-start(f32[8,144,288]{2,1,0:T(8,128)} %get-tuple-element.40) | copy-start | bytes 3981316
  515.3 5.1 copy-start.5
  516.4 17.4 %all-to-all-start = ((bf16[144,8,288]{2,0,1:T(8,128)(2,1)}), bf16[144,8,288]{2,0,1:T(8,128)(2,1)S(1)}, u32[]{:S(2)}, u32[]{:S(2)}) async-start(bf16[144,8,288]{2,0,1:T(8,128)(2,1)} %copy.34), calls=%async_computation | async-start | bytes 1769472 | tf_op jit(solution)/shard_map/all_to_all | solution.py:721
  536.1 3.5 copy-start.3
  539.6 14.1 %collective-permute-start = (bf16[480,512]{1,0:T(8,128)(2,1)S(1)}, bf16[480,512]{1,0:T(8,128)(2,1)S(1)}, u32[]{:S(2)}, u32[]{:S(2)}) collective-permute-start(bf16[480,512]{1,0:T(8,128)(2,1)S(1)} %fusion.5), channel_id=1, source_target_pairs={{8,0},{16,24},{9,1},{17,25},{10,2},{18,26},{11,3},{19,27},{12,4},{... | collective-permute-start | bytes 1474568 | tf_op jit(solution)/shard_map/ppermute | solution.py:763

commit v3 on v2

--- a/solution.py
+++ b/solution.py
@@ -290,66 +290,25 @@
     return block * features + (64 if block % 2 else 0)
 
 
-def prepare(gate, up, down, gain):
-    experts, units, features = gate.shape
+def gather(trains, gain, near_sources, count, held):
+    mats = len(trains)
+    tp_count, units, features = trains[0].shape
     wide, half = features - 64, units // 2
-    mats = (gate, up, down)
-
-    def kernel(odd_ref, gate_ref, up_ref, down_ref, gain_ref, main_ref, rest_ref):
-        def write(odd):
-            for m, ref in enumerate((gate_ref, up_ref, down_ref)):
-                value = ref[0]
-                if m < 2:
-                    value = value * gain_ref[...]
-                value = value.astype(jnp.bfloat16)
-                if odd:
-                    main, rest = value[:, 64:], value[:, :64]
-                else:
-                    main, rest = value[:, :wide], value[:, wide:]
-                main_ref[m, 0] = main
-                rest_ref[m, 0] = jnp.concatenate([rest[:half], rest[half:]], axis=1)
-
-        @pl.when(odd_ref[0] == 0)
-        def _():
-            write(False)
-
-        @pl.when(odd_ref[0] == 1)
-        def _():
-            write(True)
-
-    odd = (lax.axis_index("fs") % 2).astype(jnp.int32).reshape(1)
-    block = pl.BlockSpec((1, units, features), lambda i, s: (i, 0, 0))
-    return pl.pallas_call(
-        kernel,
-        grid_spec=pltpu.PrefetchScalarGridSpec(
-            num_scalar_prefetch=1,
-            grid=(experts,),
-            in_specs=[block, block, block, pl.BlockSpec((1, features), lambda i, s: (0, 0))],
-            out_specs=[
-                pl.BlockSpec((len(mats), 1, units, wide), lambda i, s: (0, i, 0, 0)),
-                pl.BlockSpec((len(mats), 1, half, 128), lambda i, s: (0, i, 0, 0)),
-            ],
-        ),
-        out_shape=[
-            jax.ShapeDtypeStruct((len(mats), experts, units, wide), jnp.bfloat16),
-            jax.ShapeDtypeStruct((len(mats), experts, half, 128), jnp.bfloat16),
-        ],
-        cost_estimate=pl.CostEstimate(
-            flops=3 * gate.size, bytes_accessed=18 * gate.size, transcendentals=0
-        ),
-    )(odd, gate, up, down, gain)
-
-
-def gather(own_main, own_rest, tokens, info, count, held):
-    mats, tp_count, half = own_rest.shape[:3]
-    pieces, units, wide = own_main.shape
+    pieces = mats * tp_count
     bits = tp_count.bit_length() - 1
-
-    def kernel(
-        own_main, own_rest, tokens, info, main, rest, near_tokens, near_info, early, last, hold, hold_rest, load_sem, keep_sem,
-        plane_send, plane_recv, plane_rest_send, plane_rest_recv, line_send, line_recv, line_rest_send,
-        line_rest_recv, near_send, near_recv, pass_hold, pass_load, pass_keep,
-    ):
+    nears = len(near_sources)
+    depth = 3
+
+    def kernel(*refs):
+        refs = list(refs)
+        take = lambda number: [refs.pop(0) for _ in range(number)]
+        train_refs, (gain_ref,), sources = take(mats), take(1), take(nears)
+        main, rest, own_main, own_rest, early, last = take(6)
+        targets = take(nears)
+        raw, cast, cast_rest, load_sem, keep_sem = take(5)
+        plane_send, plane_recv, plane_rest_send, plane_rest_recv = take(4)
+        line_send, line_recv, line_rest_send, line_rest_recv = take(4)
+        near_send, near_recv, pass_hold, pass_load, pass_keep = take(5)
         z = lax.axis_index("fs")
         t = lax.axis_index("tp")
 
@@ -391,22 +350,6 @@
                 device_id={"fs": target, "tp": t}, device_id_type=pl.DeviceIdType.MESH,
             )
 
-        for m in range(mats):
-            pltpu.make_async_copy(own_main.at[m * tp_count + t], hold.at[m], load_sem.at[0, m]).start()
-            pltpu.make_async_copy(own_rest.at[m, t], hold_rest.at[m], load_sem.at[1, m]).start()
-
-        for m in range(mats):
-            @pl.loop(1, tp_count)
-            def _(p, m=m):
-                plane(m, p).start()
-                plane_rest(m, p).start()
-
-        for m in range(mats):
-            pltpu.make_async_copy(own_main.at[m * tp_count + t], hold.at[m], load_sem.at[0, m]).wait()
-            pltpu.make_async_copy(hold.at[m], main.at[z, m * tp_count + t], keep_sem.at[0, m]).start()
-            pltpu.make_async_copy(own_rest.at[m, t], hold_rest.at[m], load_sem.at[1, m]).wait()
-            pltpu.make_async_copy(hold_rest.at[m], rest.at[z, m, t], keep_sem.at[1, m]).start()
-
         def has(way, step):
             return z + step <= count - 1 if way == 0 else z - step >= 0
 
@@ -414,10 +357,9 @@
             return z >= 1 if way == 0 else z <= count - 2
 
         def near(k):
-            source, target = ((tokens, near_tokens), (info, near_info))[k]
             inward = jnp.where(z == 0, 1, count - 2)
             return pltpu.make_async_remote_copy(
-                source, target, near_send.at[k], near_recv.at[k],
+                sources[k], targets[k], near_send.at[k], near_recv.at[k],
                 device_id={"fs": inward, "tp": t}, device_id_type=pl.DeviceIdType.MESH,
             )
 
@@ -435,47 +377,147 @@
         def arrives(way, step, m, p):
             return into_end(way, step, m, p, z + 1 if way == 0 else z - 1)
 
-        for step in range(count):
+        def load(m, p):
+            slot = (m * tp_count + p) % depth
+            return pltpu.make_async_copy(train_refs[m].at[peer(p)], raw.at[slot], load_sem.at[slot])
+
+        def keep(m, p, own):
+            slot, place = (m * tp_count + p) % depth, m * tp_count + peer(p)
+            goal, goal_rest = (main.at[z], rest.at[z, m]) if own else (own_main, own_rest.at[m])
+            return (
+                pltpu.make_async_copy(cast.at[slot], goal.at[place], keep_sem.at[0, slot]),
+                pltpu.make_async_copy(cast_rest.at[slot], goal_rest.at[peer(p)], keep_sem.at[1, slot]),
+            )
+
+        def load_ahead(m, p):
+            if m < mats:
+                load(m, p).start()
+
+        def convert(m, p, own):
+            slot = (m * tp_count + p) % depth
+            load(m, p).wait()
+
+            def put(odd):
+                value = raw[slot]
+                if m < mats - 1:
+                    value = value * gain_ref[...]
+                value = value.astype(cast.dtype)
+                if odd:
+                    cast[slot], end = value[:, 64:], value[:, :64]
+                else:
+                    cast[slot], end = value[:, :wide], value[:, wide:]
+                cast_rest[slot] = jnp.concatenate([end[:half], end[half:]], axis=1)
+
+            pl.when(z % 2 == 0)(lambda: put(False))
+            pl.when(z % 2 == 1)(lambda: put(True))
+            for copy in keep(m, p, own):
+                copy.start()
+
+        def finish(m, p, own):
+            for copy in keep(m, p, own):
+                copy.wait()
+            if not own:
+                plane(m, p).start()
+                plane_rest(m, p).start()
+
+        def forward(step, m, p, first=False):
+            i = m * tp_count + p
+            if step == 0 and not first:
+                plane(m, p).wait_recv()
+            for way in range(2):
+                if step > 0:
+                    @pl.when(has(way, step) & arrives(way, step - 1, m, p))
+                    def _(way=way):
+                        line(way, step - 1, i).wait_recv()
+                if step < count - 1:
+                    @pl.when(has(way, step) & sends(way) & leaves(way, step, m, p))
+                    def _(way=way):
+                        line(way, step, i).start()
+
+        def forward_rest(step, m):
+            if step == 0:
+                @pl.loop(1, tp_count)
+                def _(p):
+                    plane_rest(m, p).wait_recv()
+            for way in range(2):
+                if step > 0:
+                    @pl.when(has(way, step))
+                    def _(way=way):
+                        line_rest(way, step - 1, m).wait_recv()
+                if step < count - 1:
+                    @pl.when(has(way, step) & sends(way))
+                    def _(way=way):
+                        line_rest(way, step, m).start()
+
+        barrier = pltpu.get_barrier_semaphore()
+        for p in range(1, tp_count):
+            pl.semaphore_signal(
+                barrier, inc=1, device_id={"fs": z, "tp": peer(p)}, device_id_type=pl.DeviceIdType.MESH
+            )
+
+        @pl.when(z >= 1)
+        def _():
+            pl.semaphore_signal(
+                barrier, inc=1, device_id={"fs": z - 1, "tp": t}, device_id_type=pl.DeviceIdType.MESH
+            )
+
+        @pl.when(z <= count - 2)
+        def _():
+            pl.semaphore_signal(
+                barrier, inc=1, device_id={"fs": z + 1, "tp": t}, device_id_type=pl.DeviceIdType.MESH
+            )
+
+        for p in range(depth):
+            load(0, p).start()
+        for m in range(mats):
+            convert(m, 0, True)
+            load_ahead(m, depth)
+            if m == 0:
+                middle = jnp.logical_and(z >= 1, z <= count - 2)
+                pl.semaphore_wait(barrier, tp_count + jnp.where(middle, 1, 0))
+                finish(0, 0, True)
+                forward(0, 0, 0, first=True)
+            else:
+                finish(m - 1, tp_count - 1, False)
+                if m > 1:
+                    forward(0, m - 1, 0, first=True)
+
+            @pl.loop(1, tp_count)
+            def _(p, m=m):
+                convert(m, p, False)
+                pl.when(p + depth < tp_count)(lambda: load(m, p + depth).start())
+                if m + 1 < mats:
+                    pl.when(p + depth >= tp_count)(lambda: load(m + 1, p + depth - tp_count).start())
+                if m == 0:
+                    pl.when(p >= 2)(lambda: finish(m, p - 1, False))
+                else:
+                    pl.when(p == 1)(lambda: finish(m, 0, True))
+                    pl.when(p >= 2)(lambda: finish(m, p - 1, False))
+                    forward(0, m - 1, p)
+
+            if m > 0:
+                forward_rest(0, m - 1)
+        finish(mats - 1, tp_count - 1, False)
+        forward(0, mats - 1, 0, first=True)
+
+        @pl.loop(1, tp_count)
+        def _(p):
+            forward(0, mats - 1, p)
+
+        forward_rest(0, mats - 1)
+
+        @pl.when((z == 0) | (z == count - 1))
+        def _():
+            for k in range(nears):
+                near(k).start()
+
+        for step in range(1, count):
             for m in range(mats):
-                if step == 0:
-                    pltpu.make_async_copy(hold.at[m], main.at[z, m * tp_count + t], keep_sem.at[0, m]).wait()
-                    pltpu.make_async_copy(hold_rest.at[m], rest.at[z, m, t], keep_sem.at[1, m]).wait()
-
                 @pl.loop(0, tp_count)
                 def _(p, step=step, m=m):
-                    i = m * tp_count + p
-                    if step == 0:
-                        @pl.when(p >= 1)
-                        def _():
-                            plane(m, p).wait_recv()
-                    for way in range(2):
-                        if step > 0:
-                            @pl.when(has(way, step) & arrives(way, step - 1, m, p))
-                            def _(way=way):
-                                line(way, step - 1, i).wait_recv()
-                        if step < count - 1:
-                            @pl.when(has(way, step) & sends(way) & leaves(way, step, m, p))
-                            def _(way=way):
-                                line(way, step, i).start()
-
-                if step == 0:
-                    @pl.loop(1, tp_count)
-                    def _(p, m=m):
-                        plane_rest(m, p).wait_recv()
-                for way in range(2):
-                    if step > 0:
-                        @pl.when(has(way, step))
-                        def _(way=way, step=step, m=m):
-                            line_rest(way, step - 1, m).wait_recv()
-                    if step < count - 1:
-                        @pl.when(has(way, step) & sends(way))
-                        def _(way=way, step=step, m=m):
-                            line_rest(way, step, m).start()
-            if step == 0:
-                @pl.when((z == 0) | (z == count - 1))
-                def _():
-                    near(0).start()
-                    near(1).start()
+                    forward(step, m, p)
+
+                forward_rest(step, m)
 
         @pl.when((z == 1) | (z == count - 2))
         def _():
@@ -503,13 +545,13 @@
 
         @pl.when((z == 0) | (z == count - 1))
         def _():
-            near(0).wait_send()
-            near(1).wait_send()
+            for k in range(nears):
+                near(k).wait_send()
 
         @pl.when((z == 1) | (z == count - 2))
         def _():
-            near(0).wait_recv()
-            near(1).wait_recv()
+            for k in range(nears):
+                near(k).wait_recv()
 
         for step in range(count - 1):
             for way in range(2):
@@ -532,24 +574,29 @@
                         line_rest(way, step, m).wait_send()
 
     dma = pltpu.SemaphoreType.DMA
-    sent = 2 * (count - 1) * (own_main.size + own_rest.size)
+    dtype = jnp.bfloat16
+    own = pieces * units * features
+    anywhere = pl.BlockSpec(memory_space=pl.ANY)
+    outs = [
+        (count, pieces, units, wide),
+        (count, mats, tp_count, half, 128),
+        (pieces, units, wide),
+        (mats, tp_count, half, 128),
+        (tp_count + held - 1, units, wide),
+        (1, units, wide),
+    ]
     return pl.pallas_call(
         kernel,
-        in_specs=[pl.BlockSpec(memory_space=pl.ANY)] * 4,
-        out_specs=[pl.BlockSpec(memory_space=pl.ANY)] * 6,
-        out_shape=[
-            jax.ShapeDtypeStruct((count,) + own_main.shape, own_main.dtype),
-            jax.ShapeDtypeStruct((count,) + own_rest.shape, own_rest.dtype),
-            jax.ShapeDtypeStruct(tokens.shape, tokens.dtype),
-            jax.ShapeDtypeStruct(info.shape, info.dtype),
-            jax.ShapeDtypeStruct((tp_count + held - 1, units, wide), own_main.dtype),
-            jax.ShapeDtypeStruct((1, units, wide), own_main.dtype),
-        ],
+        in_specs=[anywhere] * mats + [pl.BlockSpec(memory_space=pltpu.VMEM)] + [anywhere] * nears,
+        out_specs=[anywhere] * (len(outs) + nears),
+        out_shape=[jax.ShapeDtypeStruct(shape, dtype) for shape in outs]
+        + [jax.ShapeDtypeStruct(source.shape, source.dtype) for source in near_sources],
         scratch_shapes=[
-            pltpu.VMEM((mats, units, wide), own_main.dtype),
-            pltpu.VMEM((mats, half, 128), own_rest.dtype),
-            dma((2, mats)),
-            dma((2, mats)),
+            pltpu.VMEM((depth, units, features), jnp.float32),
+            pltpu.VMEM((depth, units, wide), dtype),
+            pltpu.VMEM((depth, half, 128), dtype),
+            dma((depth,)),
+            dma((2, depth)),
             dma((mats, tp_count)),
             dma((mats, tp_count)),
             dma((mats, tp_count)),
@@ -558,15 +605,17 @@
             dma((2, count - 1, pieces)),
             dma((2, count - 1, mats)),
             dma((2, count - 1, mats)),
-            dma((2,)),
-            dma((2,)),
-            pltpu.VMEM((tp_count + held, units, wide), own_main.dtype),
+            dma((nears,)),
+            dma((nears,)),
+            pltpu.VMEM((tp_count + held, units, wide), dtype),
             dma((tp_count + held,)),
             dma((tp_count + held,)),
         ],
-        compiler_params=pltpu.CompilerParams(has_side_effects=True),
-        cost_estimate=pl.CostEstimate(flops=10**9, bytes_accessed=2 * sent, transcendentals=0),
-    )(own_main, own_rest, tokens, info)
+        compiler_params=pltpu.CompilerParams(collective_id=0, has_side_effects=True),
+        cost_estimate=pl.CostEstimate(
+            flops=1000 * own, bytes_accessed=4 * (count + 3) * own, transcendentals=0
+        ),
+    )(*trains, gain, *near_sources)
 
 
 def joined(main_ref, rest_ref, out_ref):
@@ -730,28 +779,22 @@
     count = lax.axis_size("fs")
     place = lax.axis_index("fs")
     experts, features, _ = gate_train.shape
-    held = experts - 3
+    held = experts - 1
     outward = [(1, 0), (count - 2, count - 1)]
-    own_main, own_rest = prepare(
-        gate_train.transpose(0, 2, 1), up_train.transpose(0, 2, 1), down_train.transpose(0, 2, 1), gain[None, :]
-    )
-    info = jnp.concatenate([routes.T.astype(jnp.float32), route_weights.T])
-    main, rest, near_tokens, near_info, kept_early, kept_last = gather(
-        own_main.reshape((-1,) + own_main.shape[2:]), own_rest, tokens, info, count, held
+    near_sources = (tokens, routes.T, route_weights.T)
+    main, rest, _, _, kept_early, kept_last, *near = gather(
+        [train.transpose(0, 2, 1) for train in (gate_train, up_train, down_train)],
+        gain[None, :], near_sources, count, held,
     )
     low = place < count // 2
     far_start = jnp.where(low, main_start(count - 1, features), main_start(0, features)).astype(jnp.int32)
     next_start = jnp.where(low, main_start(count - 2, features), main_start(1, features)).astype(jnp.int32)
     arrived_early = lax.ppermute(kept_early, "fs", outward)
 
-    main, rest, near_tokens, near_info, tokens, info = lax.optimization_barrier(
-        (main, rest, near_tokens, near_info, tokens, info)
-    )
-    both_info = jnp.stack([info, near_info])
-    routed = routes.shape[1]
-    both_routes = both_info[:, :routed].astype(jnp.int32).transpose(0, 2, 1)
-    both_weights = both_info[:, routed:].transpose(0, 2, 1)
-    chosen = pick(jnp.stack([tokens, near_tokens]), both_routes, lax.axis_index("tp"))
+    main, rest, near, near_sources = lax.optimization_barrier((main, rest, near, near_sources))
+    both_tokens, both_routes, both_weights = [jnp.stack(pair) for pair in zip(near_sources, near)]
+    both_routes, both_weights = both_routes.transpose(0, 2, 1), both_weights.transpose(0, 2, 1)
+    chosen = pick(both_tokens, both_routes, lax.axis_index("tp"))
     gate_new, gate_pre = join_in(main, rest, 0, chosen)
     up_new, up_pre = join_in(main, rest, 1, chosen)
     hidden = (jax.nn.silu(gate_pre) * up_pre).astype(jnp.bfloat16)

time: 562 us -> 542 us (0.964)
  Pallas kernels: 498 us -> 469 us
  waiting for transfers between devices: 25.1 us -> 34.7 us
    pallas_call x2 -> x1, Pallas kernels: 457 us -> 428 us  [gather(): pl.pallas_call(kernel, in_specs=[anywhere] * mats + [pl.BlockSpec(memory_...]
    ppermute x1, waiting for transfers between devices: 12.1 us -> 22 us  [line_shards(): lax.ppermute(jnp.concatenate([kept_rows, mixed_rows]), 'fs', outward)]
  transfers between devices with their start and end apart: 3 -> 3, of which waited for: 2 -> 2; matrix products, arithmetic and copies ran while one was open for 5% -> 5% of each run, Pallas kernels for 6% -> 7%
where the time goes in v3:
time: 542 us; the launch traced here: 541 us
  Pallas kernels  469 us (87%)
  waiting for transfers between devices  34.7 us (6%)
  local copies, waits for them, and re-layouts  15.8 us (3%)
  other arithmetic  11.8 us (2%)
  starting transfers between devices  6.31 us (1%)
    pallas_call x1, Pallas kernels, gather(): pl.pallas_call(kernel, in_specs=[anywhere] * mats + [pl.BlockSpec(memory_...  428 us
    pallas_call x3, Pallas kernels, join_call(): pl.pallas_call(kernel, grid=(tp_count,), in_specs=[pl.BlockSpec((count, 1...  35.5 us
    ppermute x1, waiting for transfers between devices, line_shards(): lax.ppermute(jnp.concatenate([kept_rows, mixed_rows]), 'fs', outward)  22 us
    all_to_all x1, waiting for transfers between devices, mix(): lax.all_to_all(partial_value.reshape(groups * CAP, tp_count, -1), 'tp', s...  12.7 us
  transfers between devices with their start and end apart: 3, of which 2 were waited for; matrix products, arithmetic and copies ran while one was open for 5% of the time, Pallas kernels for 7%

profile of v3, /device:TPU:0, one launch (start us, length us, event | category | flops | bytes accessed | tf_op | source)
XLA Modules:
  0.0 540.6 jit_solution(16580616224433425506)
XLA Ops:
  0.6 1.3 broadcast_in_dim.37.refs_3_
  1.9 427.7 %shard_map.102 = (bf16[4,24,288,512]{3,2,1,0:T(8,128)(2,1)}, bf16[4,3,8,144,128]{4,3,2,1,0:T(8,128)(2,1)}, bf16[24,288,512]{2,1,0:T(8,128)(2,1)}, bf16[3,8,144,1...) custom-call(f32[8,288,576]{2,1,0:T(8,128)} %bitcast.61, ...), custom_call_target="tpu_custom_call" | custom-call | flops 3981312000 | bytes 111476736 | tf_op jit(solution)/shard_map/pallas_call | solution.py:588
  429.6 1.3 collective-permute-start.1
  431.6 0.7 bitcast_or_fusion
  432.4 1.2 reduce-window.16
  434.2 6.1 %gather_fusion.1 = s32[768]{0:T(1024)S(1)} fusion(s32[2,192,8]{1,2,0:T(8,128)S(1)} %slice_add_fusion, s32[768]{0:T(1024)S(1)} %reshape.101), kind=kCustom, calls=%fused_computation.1 | custom fusion | bytes 15360 | tf_op jit(solution)/shard_map/jit(take_along_axis)/gather | solution.py:767
  442.3 1.5 convolution_convert_fusion
  443.8 12.0 %shard_map.104 = (bf16[2304,2304]{1,0:T(8,128)(2,1)}, f32[8,144,288]{2,1,0:T(8,128)}) custom-call(bf16[4,24,288,512]{3,2,1,0:T(8,128)(2,1)} %get-tuple-element.30.main_ref, bf16[4,3,8,144,128]{4,3,2,1,0:T(8,128)(2,1)} %get-tuple-element.31.rest_ref, bf16[144,2304]{1,0:T(8,128)(2,1)} %bitcast.66), custom_call_target="tpu_custom_call" | custom-call | flops 5308416000 | bytes 21233664 | tf_op jit(solution)/shard_map/pallas_call | solution.py:638
  455.8 12.3 %shard_map.103 = (bf16[2304,2304]{1,0:T(8,128)(2,1)}, f32[8,144,288]{2,1,0:T(8,128)}) custom-call(bf16[4,24,288,512]{3,2,1,0:T(8,128)(2,1)} %get-tuple-element.30.main_ref, bf16[4,3,8,144,128]{4,3,2,1,0:T(8,128)(2,1)} %get-tuple-element.31.rest_ref, bf16[144,2304]{1,0:T(8,128)(2,1)} %bitcast.67), custom_call_target="tpu_custom_call" | custom-call | flops 5308416000 | bytes 21233664 | tf_op jit(solution)/shard_map/pallas_call | solution.py:638
  468.1 2.9 multiply_convert_fusion.hidden_ref
  471.0 11.1 %shard_map.105 = (bf16[2304,2304]{1,0:T(8,128)(2,1)}, f32[144,2304]{1,0:T(8,128)}) custom-call(bf16[4,24,288,512]{3,2,1,0:T(8,128)(2,1)} %get-tuple-element.30.main_ref, bf16[4,3,8,144,128]{4,3,2,1,0:T(8,128)(2,1)} %get-tuple-element.31.rest_ref, bf16[8,144,288]{2,1,0:T(8,128)(2,1)} %multiply_convert_fusion.hidden_ref), custom_call_target="tpu_custom_call" | custom-call | flops 5308416000 | bytes 21233664 | tf_op jit(solution)/shard_map/pallas_call | solution.py:638
  482.2 1.4 convert_element_type.33
  483.5 1.3 reshape.85
  484.9 1.1 copy.34
  486.0 3.7 all-to-all-start
  490.4 12.7 %all-to-all-done = bf16[144,8,288]{2,0,1:T(8,128)(2,1)S(1)} async-done(((bf16[144,8,288]{2,0,1:T(8,128)(2,1)}), bf16[144,8,288]{2,0,1:T(8,128)(2,1)S(1)}, u32[]{:S(2)}, u32[]{:S(2)}) %all-to-all-start) | async-done | bytes 663584 | tf_op jit(solution)/shard_map/all_to_all | solution.py:770
  503.3 2.1 gather_fusion
  505.4 0.7 reshape.94
  506.1 2.8 multiply_reduce_fusion
  509.0 1.3 collective-permute-start
  510.9 22.0 %collective-permute-done = bf16[480,512]{1,0:T(8,128)(2,1)S(1)} collective-permute-done((bf16[480,512]{1,0:T(8,128)(2,1)S(1)}, bf16[480,512]{1,0:T(8,128)(2,1)S(1)}, u32[]{:S(2)}, u32[]{:S(2)}) %collective-permute-start) | collective-permute-done | bytes 491552 | tf_op jit(solution)/shard_map/ppermute | solution.py:806
  533.6 0.7 slice_bitcast_fusion.arrived_ref
  534.3 4.4 shard_map.106.base_ref
  538.7 1.7 shard_map.107
  (52 shorter events, 5.4 us)
Async XLA Ops:
  1.9 429.0 %copy-start.4 = (s32[192,2]{0,1:T(2,128)S(1)}, s32[192,2]{0,1:T(2,128)}, u32[]{:S(2)}) copy-start(s32[192,2]{0,1:T(2,128)} %param.12) | copy-start | bytes 4612
  429.6 104.7 %collective-permute-start.1 = (bf16[14,288,512]{2,1,0:T(8,128)(2,1)}, bf16[14,288,512]{2,1,0:T(8,128)(2,1)}, u32[]{:S(2)}, u32[]{:S(2)}) collective-permute-start(bf16[14,288,512]{2,1,0:T(8,128)(2,1)} %get-tuple-element.44), channel_id=1, source_target_pairs={{8,0},{16,24},{9,1},{17,25},{10,2},{18,26},{11,3},{19,27},{12,4},{... | collective-permute-start | bytes 12386312 | tf_op jit(solution)/shard_map/ppermute | solution.py:792
  434.2 6.4 %copy-start.5 = (s32[2,192]{1,0:T(2,128)S(1)}, s32[2,192]{1,0:T(2,128)}, u32[]{:S(2)}) copy-start(s32[2,192]{1,0:T(2,128)} %get-tuple-element.33) | copy-start | bytes 4612
  434.2 7.7 %copy-start = (bf16[192,2304]{1,0:T(8,128)(2,1)S(1)}, bf16[192,2304]{1,0:T(8,128)(2,1)}, u32[]{:S(2)}) copy-start(bf16[192,2304]{1,0:T(8,128)(2,1)} %refs_4_.1) | copy-start | bytes 2654212
  434.2 7.7 %copy-start.2 = (bf16[192,2304]{1,0:T(8,128)(2,1)S(1)}, bf16[192,2304]{1,0:T(8,128)(2,1)}, u32[]{:S(2)}) copy-start(bf16[192,2304]{1,0:T(8,128)(2,1)} %get-tuple-element.35) | copy-start | bytes 2654212
  455.8 12.3 %copy-start.1 = (f32[8,144,288]{2,1,0:T(8,128)S(1)}, f32[8,144,288]{2,1,0:T(8,128)}, u32[]{:S(2)}) copy-start(f32[8,144,288]{2,1,0:T(8,128)} %get-tuple-element.42) | copy-start | bytes 3981316
  484.9 5.3 copy-start.6
  484.9 5.3 copy-start.7
  486.0 17.1 %all-to-all-start = ((bf16[144,8,288]{2,0,1:T(8,128)(2,1)}), bf16[144,8,288]{2,0,1:T(8,128)(2,1)S(1)}, u32[]{:S(2)}, u32[]{:S(2)}) async-start(bf16[144,8,288]{2,0,1:T(8,128)(2,1)} %copy.34), calls=%async_computation | async-start | bytes 1769472 | tf_op jit(solution)/shard_map/all_to_all | solution.py:770
  505.4 3.5 copy-start.3
  509.0 23.9 %collective-permute-start = (bf16[480,512]{1,0:T(8,128)(2,1)S(1)}, bf16[480,512]{1,0:T(8,128)(2,1)S(1)}, u32[]{:S(2)}, u32[]{:S(2)}) collective-permute-start(bf16[480,512]{1,0:T(8,128)(2,1)S(1)} %fusion.5), channel_id=1, source_target_pairs={{8,0},{16,24},{9,1},{17,25},{10,2},{18,26},{11,3},{19,27},{12,4},{... | collective-permute-start | bytes 1474568 | tf_op jit(solution)/shard_map/ppermute | solution.py:806

commit v4 on v3

--- a/solution.py
+++ b/solution.py
@@ -400,7 +400,7 @@
             def put(odd):
                 value = raw[slot]
                 if m < mats - 1:
-                    value = value * gain_ref[...]
+                    value = value * gain_ref[...].reshape(1, features)
                 value = value.astype(cast.dtype)
                 if odd:
                     cast[slot], end = value[:, 64:], value[:, :64]
@@ -744,6 +744,33 @@
     )(start, arrived, base)
 
 
+def place_last(arrived, row, column, base, count):
+    units, wide = arrived.shape
+
+    def kernel(start_ref, arrived_ref, base_ref, new_ref, keep_sem):
+        z = lax.axis_index("fs")
+
+        @pl.when((z == 0) | (z == count - 1))
+        def _():
+            goal = new_ref.at[pl.ds(row * units, units), pl.ds(pl.multiple_of(start_ref[0], 128), wide)]
+            keep = pltpu.make_async_copy(arrived_ref, goal, keep_sem)
+            keep.start()
+            keep.wait()
+
+    return pl.pallas_call(
+        kernel,
+        in_specs=[pl.BlockSpec(memory_space=space) for space in (pltpu.SMEM, pltpu.VMEM, pl.ANY)],
+        out_specs=pl.BlockSpec(memory_space=pl.ANY),
+        out_shape=jax.ShapeDtypeStruct(base.shape, base.dtype),
+        scratch_shapes=[pltpu.SemaphoreType.DMA],
+        input_output_aliases={2: 0},
+        compiler_params=pltpu.CompilerParams(vmem_limit_bytes=4 * arrived.size),
+        cost_estimate=pl.CostEstimate(
+            flops=500 * arrived.size, bytes_accessed=4 * arrived.size, transcendentals=0
+        ),
+    )(column.reshape(1), arrived, base)
+
+
 def pick(tokens, routes, expert):
     tokens_wide = tokens.astype(jnp.float32)
     normed = (
@@ -764,7 +791,8 @@
     labels = jnp.arange(experts, dtype=jnp.int32)
     member_all = jnp.any(routes[:, :, :, None] == labels, axis=2)
     slots_all = jnp.cumsum(member_all.astype(jnp.int32), axis=1) - 1
-    slot_pair = jnp.take_along_axis(slots_all, routes, axis=2)
+    named = routes[:, :, :, None] == labels
+    slot_pair = jnp.sum(jnp.where(named, slots_all[:, :, None, :], 0), axis=3)
     first = CAP * jnp.arange(groups, dtype=jnp.int32)[:, None, None]
     flat_index = (first + slot_pair) * experts + routes
     received = lax.all_to_all(
@@ -784,7 +812,7 @@
     near_sources = (tokens, routes.T, route_weights.T)
     main, rest, _, _, kept_early, kept_last, *near = gather(
         [train.transpose(0, 2, 1) for train in (gate_train, up_train, down_train)],
-        gain[None, :], near_sources, count, held,
+        gain, near_sources, count, held,
     )
     low = place < count // 2
     far_start = jnp.where(low, main_start(count - 1, features), main_start(0, features)).astype(jnp.int32)
@@ -800,17 +828,14 @@
     hidden = (jax.nn.silu(gate_pre) * up_pre).astype(jnp.bfloat16)
     down_new, total = join_out(main, rest, 2, hidden)
     both_mixed = mix(total.astype(jnp.bfloat16), both_routes, both_weights, experts)
-    wide = kept_last.shape[2]
-    kept_rows = kept_last.reshape(-1, wide)
-    mixed_rows = jnp.pad(both_mixed[1], ((0, 0), (0, wide - both_mixed.shape[2])))
-    arrived_rows = lax.ppermute(jnp.concatenate([kept_rows, mixed_rows]), "fs", outward)
-    arrived_last = arrived_rows[: kept_rows.shape[0]].reshape(kept_last.shape)
-    near_mixed = arrived_rows[kept_rows.shape[0] :, : both_mixed.shape[2]]
+    near_mixed = lax.ppermute(both_mixed[1], "fs", outward)
+    kept_last, _ = lax.optimization_barrier((kept_last, both_mixed))
+    arrived_last = lax.ppermute(kept_last, "fs", outward)
     first = experts - held
     early = [(i, i, far_start) for i in range(experts)]
     early += [(experts + i, first + i, next_start) for i in range(held - 1)]
     down_new = place_late(arrived_early, early, down_new, count)
-    down_new = place_late(arrived_last, [(0, experts - 1, next_start)], down_new, count)
+    down_new = place_last(arrived_last[0], experts - 1, next_start, down_new, count)
     at_end = (place == 0) | (place == count - 1)
     mixed = jnp.where(at_end, near_mixed, both_mixed[0])
     return (gate_new[None], up_new[None], down_new[None], mixed)

time: 542 us -> 533 us (0.983)
  local copies, waits for them, and re-layouts: 15.8 us -> 7.11 us
    gather x5 -> x0, local copies, waits for them, and re-layouts: 6.69 us -> none  [mix(): slot_pair = jnp.take_along_axis(slots_all, routes, axis=2)]
    ppermute x1 -> x2, waiting for transfers between devices: 22 us -> 20.4 us  [the longest x1 20.4 us: line_shards(): near_mixed = lax.ppermute(both_mixed[1], 'fs', outward)]
  transfers between devices with their start and end apart: 3 -> 4, of which waited for: 2 -> 2; matrix products, arithmetic and copies ran while one was open for 5% -> 4% of each run, Pallas kernels for 7% -> 8%
where the time goes in v4:
time: 533 us; the launch traced here: 532 us
  Pallas kernels  468 us (88%)
  waiting for transfers between devices  33.3 us (6%)
  other arithmetic  13 us (2%)
  starting transfers between devices  7.55 us (1%)
  local copies, waits for them, and re-layouts  7.11 us (1%)
    pallas_call x1, Pallas kernels, gather(): pl.pallas_call(kernel, in_specs=[anywhere] * mats + [pl.BlockSpec(memory_...  428 us
    pallas_call x3, Pallas kernels, join_call(): pl.pallas_call(kernel, grid=(tp_count,), in_specs=[pl.BlockSpec((count, 1...  35.5 us
    ppermute x1, waiting for transfers between devices, line_shards(): near_mixed = lax.ppermute(both_mixed[1], 'fs', outward)  20.4 us
    all_to_all x1, waiting for transfers between devices, mix(): lax.all_to_all(partial_value.reshape(groups * CAP, tp_count, -1), 'tp', s...  12.9 us
  transfers between devices with their start and end apart: 4, of which 2 were waited for; matrix products, arithmetic and copies ran while one was open for 4% of the time, Pallas kernels for 8%

profile of v4, /device:TPU:0, one launch (start us, length us, event | category | flops | bytes accessed | tf_op | source)
XLA Modules:
  0.0 531.8 jit_solution(11465740544998552545)
XLA Ops:
  0.7 427.8 %shard_map.102 = (bf16[4,24,288,512]{3,2,1,0:T(8,128)(2,1)}, bf16[4,3,8,144,128]{4,3,2,1,0:T(8,128)(2,1)}, bf16[24,288,512]{2,1,0:T(8,128)(2,1)}, bf16[3,8,144,1...) custom-call(f32[8,288,576]{2,1,0:T(8,128)} %bitcast.52, ...), custom_call_target="tpu_custom_call" | custom-call | flops 3981312000 | bytes 111476736 | tf_op jit(solution)/shard_map/pallas_call | solution.py:588
  428.5 1.4 collective-permute-start.1
  429.9 0.7 add_bitcast_fusion.1
  430.6 1.2 reduce-window.16
  432.2 0.8 compare_and_fusion
  434.1 1.6 fusion
  435.7 1.4 convolution_convert_fusion
  437.1 12.0 %shard_map.104 = (bf16[2304,2304]{1,0:T(8,128)(2,1)}, f32[8,144,288]{2,1,0:T(8,128)}) custom-call(bf16[4,24,288,512]{3,2,1,0:T(8,128)(2,1)} %get-tuple-element.31.main_ref, bf16[4,3,8,144,128]{4,3,2,1,0:T(8,128)(2,1)} %get-tuple-element.32.rest_ref, bf16[144,2304]{1,0:T(8,128)(2,1)} %bitcast.57), custom_call_target="tpu_custom_call" | custom-call | flops 5308416000 | bytes 21233664 | tf_op jit(solution)/shard_map/pallas_call | solution.py:638
  449.2 12.3 %shard_map.103 = (bf16[2304,2304]{1,0:T(8,128)(2,1)}, f32[8,144,288]{2,1,0:T(8,128)}) custom-call(bf16[4,24,288,512]{3,2,1,0:T(8,128)(2,1)} %get-tuple-element.31.main_ref, bf16[4,3,8,144,128]{4,3,2,1,0:T(8,128)(2,1)} %get-tuple-element.32.rest_ref, bf16[144,2304]{1,0:T(8,128)(2,1)} %bitcast.58), custom_call_target="tpu_custom_call" | custom-call | flops 5308416000 | bytes 21233664 | tf_op jit(solution)/shard_map/pallas_call | solution.py:638
  461.5 2.9 multiply_convert_fusion.hidden_ref
  464.4 11.1 %shard_map.105 = (bf16[2304,2304]{1,0:T(8,128)(2,1)}, f32[144,2304]{1,0:T(8,128)}) custom-call(bf16[4,24,288,512]{3,2,1,0:T(8,128)(2,1)} %get-tuple-element.31.main_ref, bf16[4,3,8,144,128]{4,3,2,1,0:T(8,128)(2,1)} %get-tuple-element.32.rest_ref, bf16[8,144,288]{2,1,0:T(8,128)(2,1)} %multiply_convert_fusion.hidden_ref), custom_call_target="tpu_custom_call" | custom-call | flops 5308416000 | bytes 21233664 | tf_op jit(solution)/shard_map/pallas_call | solution.py:638
  475.5 1.4 convert_element_type.31
  476.9 1.3 reshape.73
  478.3 1.1 copy.30
  479.3 3.5 all-to-all-start
  483.6 12.9 %all-to-all-done = bf16[144,8,288]{2,0,1:T(8,128)(2,1)S(1)} async-done(((bf16[144,8,288]{2,0,1:T(8,128)(2,1)}), bf16[144,8,288]{2,0,1:T(8,128)(2,1)S(1)}, u32[]{:S(2)}, u32[]{:S(2)}) %all-to-all-start) | async-done | bytes 663584 | tf_op jit(solution)/shard_map/all_to_all | solution.py:798
  496.6 2.1 gather_fusion
  498.8 0.7 reshape.81
  499.5 2.8 multiply_reduce_fusion
  502.3 1.3 collective-permute-start.2
  504.2 1.3 collective-permute-start
  505.5 20.4 %collective-permute-done.2 = bf16[192,288]{1,0:T(8,128)(2,1)S(1)} collective-permute-done((bf16[192,288]{1,0:T(8,128)(2,1)S(1)}, bf16[192,288]{1,0:T(8,128)(2,1)S(1)}, u32[]{:S(2)}, u32[]{:S(2)}) %collective-permute-start.2) | collective-permute-done | bytes 110624 | tf_op jit(solution)/shard_map/ppermute | solution.py:831
  526.6 4.4 shard_map.106.base_ref
  531.0 0.7 shard_map.107
  (44 shorter events, 3.7 us)
Async XLA Ops:
  0.6 429.3 %copy-start.3 = (s32[192,2]{0,1:T(2,128)S(1)}, s32[192,2]{0,1:T(2,128)}, u32[]{:S(2)}) copy-start(s32[192,2]{0,1:T(2,128)} %param.12) | copy-start | bytes 4612
  0.6 433.4 %copy-start = (bf16[192,2304]{1,0:T(8,128)(2,1)S(1)}, bf16[192,2304]{1,0:T(8,128)(2,1)}, u32[]{:S(2)}) copy-start(bf16[192,2304]{1,0:T(8,128)(2,1)} %refs_4_.1) | copy-start | bytes 2654212
  428.4 7.2 %copy-start.2 = (bf16[192,2304]{1,0:T(8,128)(2,1)S(1)}, bf16[192,2304]{1,0:T(8,128)(2,1)}, u32[]{:S(2)}) copy-start(bf16[192,2304]{1,0:T(8,128)(2,1)} %get-tuple-element.36) | copy-start | bytes 2654212
  428.5 98.1 %collective-permute-start.1 = (bf16[14,288,512]{2,1,0:T(8,128)(2,1)}, bf16[14,288,512]{2,1,0:T(8,128)(2,1)}, u32[]{:S(2)}, u32[]{:S(2)}) collective-permute-start(bf16[14,288,512]{2,1,0:T(8,128)(2,1)} %get-tuple-element.46), channel_id=1, source_target_pairs={{8,0},{16,24},{9,1},{17,25},{10,2},{18,26},{11,3},{19,27},{12,4},{... | collective-permute-start | bytes 12386312 | tf_op jit(solution)/shard_map/ppermute | solution.py:820
  449.2 12.3 %copy-start.1 = (f32[8,144,288]{2,1,0:T(8,128)S(1)}, f32[8,144,288]{2,1,0:T(8,128)}, u32[]{:S(2)}) copy-start(f32[8,144,288]{2,1,0:T(8,128)} %get-tuple-element.43) | copy-start | bytes 3981316
  478.2 5.1 copy-start.4
  478.3 5.1 copy-start.5
  479.3 17.1 %all-to-all-start = ((bf16[144,8,288]{2,0,1:T(8,128)(2,1)}), bf16[144,8,288]{2,0,1:T(8,128)(2,1)S(1)}, u32[]{:S(2)}, u32[]{:S(2)}) async-start(bf16[144,8,288]{2,0,1:T(8,128)(2,1)} %copy.30), calls=%async_computation | async-start | bytes 1769472 | tf_op jit(solution)/shard_map/all_to_all | solution.py:798
  498.8 5.4 %copy-start.6 = (bf16[1,288,512]{2,1,0:T(8,128)(2,1)S(1)}, bf16[1,288,512]{2,1,0:T(8,128)(2,1)}, u32[]{:S(2)}) copy-start(bf16[1,288,512]{2,1,0:T(8,128)(2,1)} %get-tuple-element.45) | copy-start | bytes 884740
  502.3 23.6 %collective-permute-start.2 = (bf16[192,288]{1,0:T(8,128)(2,1)S(1)}, bf16[192,288]{1,0:T(8,128)(2,1)S(1)}, u32[]{:S(2)}, u32[]{:S(2)}) collective-permute-start(bf16[192,288]{1,0:T(8,128)(2,1)S(1)} %slice_bitcast_fusion.1), channel_id=1, source_target_pairs={{8,0},{16,24},{9,1},{17,25},{10,2},{18,26},{11,3},{19,27},{12,4},{... | collective-permute-start | bytes 331784 | tf_op jit(solution)/shard_map/ppermute | solution.py:831
  504.2 26.8 %collective-permute-start = (bf16[1,288,512]{2,1,0:T(8,128)(2,1)S(1)}, bf16[1,288,512]{2,1,0:T(8,128)(2,1)S(1)}, u32[]{:S(2)}, u32[]{:S(2)}) collective-permute-start(bf16[1,288,512]{2,1,0:T(8,128)(2,1)S(1)} %copy-done.6), channel_id=1, source_target_pairs={{8,0},{16,24},{9,1},{17,25},{10,2},{18,26},{11,3},{19,27},{12,4},{... | collective-permute-start | bytes 884744 | tf_op jit(solution)/shard_map/ppermute | solution.py:833

commit v5 on v4

--- a/solution.py
+++ b/solution.py
@@ -278,6 +278,7 @@
     return (
         experts == tp_count
         and tp_count & (tp_count - 1) == 0
+        and tp_count >= 4
         and count >= 4
         and count % 2 == 0
         and features % 128 == 64
@@ -290,7 +291,7 @@
     return block * features + (64 if block % 2 else 0)
 
 
-def gather(trains, gain, near_sources, count, held):
+def gather(trains, gain, near_sources, count, held, lead):
     mats = len(trains)
     tp_count, units, features = trains[0].shape
     wide, half = features - 64, units // 2
@@ -303,7 +304,7 @@
         refs = list(refs)
         take = lambda number: [refs.pop(0) for _ in range(number)]
         train_refs, (gain_ref,), sources = take(mats), take(1), take(nears)
-        main, rest, own_main, own_rest, early, last = take(6)
+        main, rest, own_main, own_rest, early, extra, last = take(7)
         targets = take(nears)
         raw, cast, cast_rest, load_sem, keep_sem = take(5)
         plane_send, plane_recv, plane_rest_send, plane_rest_recv = take(4)
@@ -369,7 +370,7 @@
             end = sender == 1 if way == 0 else sender == count - 2
             if step == count - 2:
                 return jnp.logical_not(end)
-            return jnp.logical_not(end & (peer(p) >= tp_count - held))
+            return jnp.logical_not(end & (peer(p) >= tp_count - held - lead * (1 - t % 2)))
 
         def leaves(way, step, m, p):
             return into_end(way, step, m, p, z)
@@ -523,10 +524,11 @@
         def _():
             low = z < count // 2
             far, after_far = jnp.where(low, count - 1, 0), jnp.where(low, count - 2, 1)
-            first = pieces - held
+            first = pieces - held - lead
             found = [main.at[far, pieces - tp_count + i] for i in range(tp_count)]
-            found += [main.at[after_far, first + i] for i in range(held)]
-            goal = [early.at[i] for i in range(tp_count + held - 1)] + [last.at[0]]
+            found += [main.at[after_far, first + i] for i in range(lead + held)]
+            goal = [early.at[i] for i in range(tp_count)] + [extra.at[i] for i in range(lead)]
+            goal += [early.at[tp_count + i] for i in range(held - 1)] + [last.at[0]]
             loads = [pltpu.make_async_copy(f, pass_hold.at[i], pass_load.at[i]) for i, f in enumerate(found)]
             keeps = [pltpu.make_async_copy(pass_hold.at[i], g, pass_keep.at[i]) for i, g in enumerate(goal)]
             for load in loads:
@@ -566,7 +568,8 @@
                     if step == count - 2:
                         settle(pieces - tp_count)
                     elif step == count - 3:
-                        pl.when(end)(lambda: settle(pieces - held))
+                        pl.when(end & (t % 2 == 0))(lambda: settle(pieces - held - lead))
+                        pl.when(end & (t % 2 == 1))(lambda: settle(pieces - held))
                         pl.when(jnp.logical_not(end))(lambda: settle(pieces))
                     else:
                         settle(pieces)
@@ -583,6 +586,7 @@
         (pieces, units, wide),
         (mats, tp_count, half, 128),
         (tp_count + held - 1, units, wide),
+        (lead, units, wide),
         (1, units, wide),
     ]
     return pl.pallas_call(
@@ -607,9 +611,9 @@
             dma((2, count - 1, mats)),
             dma((nears,)),
             dma((nears,)),
-            pltpu.VMEM((tp_count + held, units, wide), dtype),
-            dma((tp_count + held,)),
-            dma((tp_count + held,)),
+            pltpu.VMEM((tp_count + held + lead, units, wide), dtype),
+            dma((tp_count + held + lead,)),
+            dma((tp_count + held + lead,)),
         ],
         compiler_params=pltpu.CompilerParams(collective_id=0, has_side_effects=True),
         cost_estimate=pl.CostEstimate(
@@ -695,26 +699,24 @@
     )
 
 
-def place_late(arrived, places, base, count):
-    pieces, units, wide = arrived.shape
-    start = jnp.stack([column for _, _, column in places])
-
-    def kernel(start_ref, arrived_ref, base_ref, new_ref, hold, load_sem, keep_sem):
-        z = lax.axis_index("fs")
-
-        @pl.when((z == 0) | (z == count - 1))
-        def _():
-            loads = [pltpu.make_async_copy(arrived_ref.at[i], hold.at[i], load_sem.at[i]) for i in range(pieces)]
-            keeps = [
-                pltpu.make_async_copy(
-                    hold.at[i],
-                    new_ref.at[
-                        pl.ds(row * units, units), pl.ds(pl.multiple_of(start_ref[i], 128), wide)
-                    ],
-                    keep_sem.at[i],
-                )
-                for i, row, _ in places
-            ]
+def place_late(arrived, places, extra, extra_places, base, count):
+    units, wide = arrived.shape[1:]
+    places, extra_places = list(places), list(extra_places)
+    total = len(places) + len(extra_places)
+    start = jnp.stack([column for _, column in places + extra_places])
+
+    def kernel(start_ref, arrived_ref, extra_ref, base_ref, new_ref, hold, load_sem, keep_sem):
+        z, t = lax.axis_index("fs"), lax.axis_index("tp")
+
+        def move(source, number, first, rows):
+            loads, keeps = [], []
+            for i in range(number):
+                k = first + i
+                goal = new_ref.at[
+                    pl.ds(rows[i][0] * units, units), pl.ds(pl.multiple_of(start_ref[k], 128), wide)
+                ]
+                loads.append(pltpu.make_async_copy(source.at[i], hold.at[k], load_sem.at[k]))
+                keeps.append(pltpu.make_async_copy(hold.at[k], goal, keep_sem.at[k]))
             for load in loads:
                 load.start()
             for load, keep in zip(loads, keeps):
@@ -723,25 +725,27 @@
             for keep in keeps:
                 keep.wait()
 
-    return pl.pallas_call(
-        kernel,
-        grid_spec=pltpu.PrefetchScalarGridSpec(
-            num_scalar_prefetch=1,
-            grid=(1,),
-            in_specs=[pl.BlockSpec(memory_space=pl.ANY)] * 2,
-            out_specs=pl.BlockSpec(memory_space=pl.ANY),
-            scratch_shapes=[
-                pltpu.VMEM(arrived.shape, arrived.dtype),
-                pltpu.SemaphoreType.DMA((pieces,)),
-                pltpu.SemaphoreType.DMA((pieces,)),
-            ],
-        ),
+        at_end = (z == 0) | (z == count - 1)
+        pl.when(at_end)(lambda: move(arrived_ref, len(places), 0, places))
+        pl.when(at_end & (t % 2 == 0))(
+            lambda: move(extra_ref, len(extra_places), len(places), extra_places)
+        )
+
+    return pl.pallas_call(
+        kernel,
+        in_specs=[pl.BlockSpec(memory_space=pltpu.SMEM)] + [pl.BlockSpec(memory_space=pl.ANY)] * 3,
+        out_specs=pl.BlockSpec(memory_space=pl.ANY),
+        scratch_shapes=[
+            pltpu.VMEM((total, units, wide), arrived.dtype),
+            pltpu.SemaphoreType.DMA((total,)),
+            pltpu.SemaphoreType.DMA((total,)),
+        ],
         out_shape=jax.ShapeDtypeStruct(base.shape, base.dtype),
-        input_output_aliases={2: 0},
+        input_output_aliases={3: 0},
         cost_estimate=pl.CostEstimate(
             flops=500 * arrived.size, bytes_accessed=4 * arrived.size, transcendentals=0
         ),
-    )(start, arrived, base)
+    )(start, arrived, extra, base)
 
 
 def place_last(arrived, row, column, base, count):
@@ -807,16 +811,19 @@
     count = lax.axis_size("fs")
     place = lax.axis_index("fs")
     experts, features, _ = gate_train.shape
-    held = experts - 1
+    lead = 2
+    held = experts - lead
     outward = [(1, 0), (count - 2, count - 1)]
     near_sources = (tokens, routes.T, route_weights.T)
-    main, rest, _, _, kept_early, kept_last, *near = gather(
+    main, rest, _, _, kept_early, kept_extra, kept_last, *near = gather(
         [train.transpose(0, 2, 1) for train in (gate_train, up_train, down_train)],
-        gain, near_sources, count, held,
+        gain, near_sources, count, held, lead,
     )
     low = place < count // 2
     far_start = jnp.where(low, main_start(count - 1, features), main_start(0, features)).astype(jnp.int32)
     next_start = jnp.where(low, main_start(count - 2, features), main_start(1, features)).astype(jnp.int32)
+    pairs = [(a * experts + t, b * experts + t) for a, b in outward for t in range(0, experts, 2)]
+    arrived_extra = lax.ppermute(kept_extra, ("fs", "tp"), pairs)
     arrived_early = lax.ppermute(kept_early, "fs", outward)
 
     main, rest, near, near_sources = lax.optimization_barrier((main, rest, near, near_sources))
@@ -831,10 +838,10 @@
     near_mixed = lax.ppermute(both_mixed[1], "fs", outward)
     kept_last, _ = lax.optimization_barrier((kept_last, both_mixed))
     arrived_last = lax.ppermute(kept_last, "fs", outward)
-    first = experts - held
-    early = [(i, i, far_start) for i in range(experts)]
-    early += [(experts + i, first + i, next_start) for i in range(held - 1)]
-    down_new = place_late(arrived_early, early, down_new, count)
+    early = [(i, far_start) for i in range(experts)]
+    early += [(i, next_start) for i in range(experts - held, experts - 1)]
+    extra = [(i, next_start) for i in range(experts - held - lead, experts - held)]
+    down_new = place_late(arrived_early, early, arrived_extra, extra, down_new, count)
     down_new = place_last(arrived_last[0], experts - 1, next_start, down_new, count)
     at_end = (place == 0) | (place == count - 1)
     mixed = jnp.where(at_end, near_mixed, both_mixed[0])

time: 533 us -> 530 us (level)
  starting transfers between devices: 7.55 us -> 13.5 us
    pallas_call x1, Pallas kernels: 428 us -> 422 us  [gather(): pl.pallas_call(kernel, in_specs=[anywhere] * mats + [pl.BlockSpec(memory_...]
  transfers between devices with their start and end apart: 4 -> 5, of which waited for: 2 -> 2; matrix products, arithmetic and copies ran while one was open for 4% -> 4% of each run, Pallas kernels for 8% -> 8%
where the time goes in v5:
time: 530 us; the launch traced here: 529 us
  Pallas kernels  464 us (88%)
  waiting for transfers between devices  29 us (5%)
  starting transfers between devices  13.5 us (3%)
  other arithmetic  13 us (2%)
  local copies, waits for them, and re-layouts  7.15 us (1%)
    pallas_call x1, Pallas kernels, gather(): pl.pallas_call(kernel, in_specs=[anywhere] * mats + [pl.BlockSpec(memory_...  422 us
    pallas_call x3, Pallas kernels, join_call(): pl.pallas_call(kernel, grid=(tp_count,), in_specs=[pl.BlockSpec((count, 1...  35.5 us
    ppermute x1, waiting for transfers between devices, line_shards(): near_mixed = lax.ppermute(both_mixed[1], 'fs', outward)  17.3 us
    all_to_all x1, waiting for transfers between devices, mix(): lax.all_to_all(partial_value.reshape(groups * CAP, tp_count, -1), 'tp', s...  11.7 us
  transfers between devices with their start and end apart: 5, of which 2 were waited for; matrix products, arithmetic and copies ran while one was open for 4% of the time, Pallas kernels for 8%

profile of v5, /device:TPU:0, one launch (start us, length us, event | category | flops | bytes accessed | tf_op | source)
XLA Modules:
  0.0 529.2 jit_solution(14119011762515723130)
XLA Ops:
  0.7 422.1 %shard_map.102 = (bf16[4,24,288,512]{3,2,1,0:T(8,128)(2,1)}, bf16[4,3,8,144,128]{4,3,2,1,0:T(8,128)(2,1)}, bf16[24,288,512]{2,1,0:T(8,128)(2,1)}, bf16[3,8,144,1...) custom-call(f32[8,288,576]{2,1,0:T(8,128)} %bitcast.52, ...), custom_call_target="tpu_custom_call" | custom-call | flops 3981312000 | bytes 111476736 | tf_op jit(solution)/shard_map/pallas_call | solution.py:592
  422.7 1.4 collective-permute-start.1
  424.9 1.2 reduce-window.16
  426.4 0.8 compare_and_fusion
  428.3 1.6 fusion
  430.0 1.4 convolution_convert_fusion
  431.4 12.0 %shard_map.104 = (bf16[2304,2304]{1,0:T(8,128)(2,1)}, f32[8,144,288]{2,1,0:T(8,128)}) custom-call(bf16[4,24,288,512]{3,2,1,0:T(8,128)(2,1)} %get-tuple-element.32.main_ref, bf16[4,3,8,144,128]{4,3,2,1,0:T(8,128)(2,1)} %get-tuple-element.33.rest_ref, bf16[144,2304]{1,0:T(8,128)(2,1)} %bitcast.57), custom_call_target="tpu_custom_call" | custom-call | flops 5308416000 | bytes 21233664 | tf_op jit(solution)/shard_map/pallas_call | solution.py:642
  443.4 12.3 %shard_map.103 = (bf16[2304,2304]{1,0:T(8,128)(2,1)}, f32[8,144,288]{2,1,0:T(8,128)}) custom-call(bf16[4,24,288,512]{3,2,1,0:T(8,128)(2,1)} %get-tuple-element.32.main_ref, bf16[4,3,8,144,128]{4,3,2,1,0:T(8,128)(2,1)} %get-tuple-element.33.rest_ref, bf16[144,2304]{1,0:T(8,128)(2,1)} %bitcast.58), custom_call_target="tpu_custom_call" | custom-call | flops 5308416000 | bytes 21233664 | tf_op jit(solution)/shard_map/pallas_call | solution.py:642
  455.7 2.9 multiply_convert_fusion.hidden_ref
  458.7 11.2 %shard_map.105 = (bf16[2304,2304]{1,0:T(8,128)(2,1)}, f32[144,2304]{1,0:T(8,128)}) custom-call(bf16[4,24,288,512]{3,2,1,0:T(8,128)(2,1)} %get-tuple-element.32.main_ref, bf16[4,3,8,144,128]{4,3,2,1,0:T(8,128)(2,1)} %get-tuple-element.33.rest_ref, bf16[8,144,288]{2,1,0:T(8,128)(2,1)} %multiply_convert_fusion.hidden_ref), custom_call_target="tpu_custom_call" | custom-call | flops 5308416000 | bytes 21233664 | tf_op jit(solution)/shard_map/pallas_call | solution.py:642
  469.8 1.4 convert_element_type.31
  471.2 1.3 reshape.73
  472.6 1.0 copy.30
  473.6 8.2 %all-to-all-start = ((bf16[144,8,288]{2,0,1:T(8,128)(2,1)}), bf16[144,8,288]{2,0,1:T(8,128)(2,1)S(1)}, u32[]{:S(2)}, u32[]{:S(2)}) async-start(bf16[144,8,288]{2,0,1:T(8,128)(2,1)} %copy.30), calls=%async_computation | async-start | bytes 1769472 | tf_op jit(solution)/shard_map/all_to_all | solution.py:802
  481.8 1.3 collective-permute-start.2
  483.8 11.7 %all-to-all-done = bf16[144,8,288]{2,0,1:T(8,128)(2,1)S(1)} async-done(((bf16[144,8,288]{2,0,1:T(8,128)(2,1)}), bf16[144,8,288]{2,0,1:T(8,128)(2,1)S(1)}, u32[]{:S(2)}, u32[]{:S(2)}) %all-to-all-start) | async-done | bytes 663584 | tf_op jit(solution)/shard_map/all_to_all | solution.py:802
  495.6 2.1 gather_fusion
  497.8 0.7 reshape.81
  498.5 2.8 multiply_reduce_fusion
  501.3 1.3 collective-permute-start.3
  503.3 1.3 collective-permute-start
  504.6 17.3 %collective-permute-done.3 = bf16[192,288]{1,0:T(8,128)(2,1)S(1)} collective-permute-done((bf16[192,288]{1,0:T(8,128)(2,1)S(1)}, bf16[192,288]{1,0:T(8,128)(2,1)S(1)}, u32[]{:S(2)}, u32[]{:S(2)}) %collective-permute-start.3) | collective-permute-done | bytes 110624 | tf_op jit(solution)/shard_map/ppermute | solution.py:838
  522.6 5.9 %shard_map.106.base_ref = bf16[2304,2304]{1,0:T(8,128)(2,1)} custom-call(s32[15]{0:T(128)} %stack.57.start_ref, bf16[13,288,512]{2,1,0:T(8,128)(2,1)} %collective-permute-done.1.arrived_ref, bf16[2,288,512]{2,1,0:T(8,128)(2,1)} %collective-permute-done.2.extra_ref, bf16[2304,2304]{1,0:T(8,128)(2,1)} %get-tuple-element.49.base_ref), custom_call_target="tpu_custom_call", output_to_operand_aliasing={{}: (3, {})} | custom-call | flops 958464000 | bytes 7667712 | tf_op jit(solution)/shard_map/pallas_call | solution.py:734
  528.5 0.7 shard_map.107
  (46 shorter events, 4.4 us)
Async XLA Ops:
  0.6 423.6 %copy-start.3 = (s32[192,2]{0,1:T(2,128)S(1)}, s32[192,2]{0,1:T(2,128)}, u32[]{:S(2)}) copy-start(s32[192,2]{0,1:T(2,128)} %param.12) | copy-start | bytes 4612
  0.6 427.7 %copy-start = (bf16[192,2304]{1,0:T(8,128)(2,1)S(1)}, bf16[192,2304]{1,0:T(8,128)(2,1)}, u32[]{:S(2)}) copy-start(bf16[192,2304]{1,0:T(8,128)(2,1)} %refs_4_.1) | copy-start | bytes 2654212
  422.7 7.2 %copy-start.2 = (bf16[192,2304]{1,0:T(8,128)(2,1)S(1)}, bf16[192,2304]{1,0:T(8,128)(2,1)}, u32[]{:S(2)}) copy-start(bf16[192,2304]{1,0:T(8,128)(2,1)} %get-tuple-element.37) | copy-start | bytes 2654212
  422.7 99.8 %collective-permute-start.1 = (bf16[13,288,512]{2,1,0:T(8,128)(2,1)}, bf16[13,288,512]{2,1,0:T(8,128)(2,1)}, u32[]{:S(2)}, u32[]{:S(2)}) collective-permute-start(bf16[13,288,512]{2,1,0:T(8,128)(2,1)} %get-tuple-element.47), channel_id=1, source_target_pairs={{8,0},{16,24},{9,1},{17,25},{10,2},{18,26},{11,3},{19,27},{12,4},{... | collective-permute-start | bytes 11501576 | tf_op jit(solution)/shard_map/ppermute | solution.py:827
  443.4 12.3 %copy-start.1 = (f32[8,144,288]{2,1,0:T(8,128)S(1)}, f32[8,144,288]{2,1,0:T(8,128)}, u32[]{:S(2)}) copy-start(f32[8,144,288]{2,1,0:T(8,128)} %get-tuple-element.44) | copy-start | bytes 3981316
  472.6 11.0 %copy-start.4 = (f32[192,2]{0,1:T(2,128)S(1)}, f32[192,2]{0,1:T(2,128)}, u32[]{:S(2)}) copy-start(f32[192,2]{0,1:T(2,128)} %param.13) | copy-start | bytes 4612
  472.6 11.0 %copy-start.5 = (f32[2,192]{1,0:T(2,128)S(1)}, f32[2,192]{1,0:T(2,128)}, u32[]{:S(2)}) copy-start(f32[2,192]{1,0:T(2,128)} %get-tuple-element.42) | copy-start | bytes 4612
  473.6 21.8 %all-to-all-start = ((bf16[144,8,288]{2,0,1:T(8,128)(2,1)}), bf16[144,8,288]{2,0,1:T(8,128)(2,1)S(1)}, u32[]{:S(2)}, u32[]{:S(2)}) async-start(bf16[144,8,288]{2,0,1:T(8,128)(2,1)} %copy.30), calls=%async_computation | async-start | bytes 1769472 | tf_op jit(solution)/shard_map/all_to_all | solution.py:802
  481.8 40.8 %collective-permute-start.2 = (bf16[2,288,512]{2,1,0:T(8,128)(2,1)}, bf16[2,288,512]{2,1,0:T(8,128)(2,1)}, u32[]{:S(2)}, u32[]{:S(2)}) collective-permute-start(bf16[2,288,512]{2,1,0:T(8,128)(2,1)} %get-tuple-element.48), channel_id=1, source_target_pairs={{8,0},{10,2},{12,4},{14,6},{16,24},{18,26},{20,28},{22,30}} | collective-permute-start | bytes 1769480 | tf_op jit(solution)/shard_map/ppermute | solution.py:826
  497.8 5.5 %copy-start.6 = (bf16[1,288,512]{2,1,0:T(8,128)(2,1)S(1)}, bf16[1,288,512]{2,1,0:T(8,128)(2,1)}, u32[]{:S(2)}) copy-start(bf16[1,288,512]{2,1,0:T(8,128)(2,1)} %get-tuple-element.46) | copy-start | bytes 884740
  501.3 20.6 %collective-permute-start.3 = (bf16[192,288]{1,0:T(8,128)(2,1)S(1)}, bf16[192,288]{1,0:T(8,128)(2,1)S(1)}, u32[]{:S(2)}, u32[]{:S(2)}) collective-permute-start(bf16[192,288]{1,0:T(8,128)(2,1)S(1)} %slice_bitcast_fusion.1), channel_id=1, source_target_pairs={{8,0},{16,24},{9,1},{17,25},{10,2},{18,26},{11,3},{19,27},{12,4},{... | collective-permute-start | bytes 331784 | tf_op jit(solution)/shard_map/ppermute | solution.py:838
  503.3 25.2 %collective-permute-start = (bf16[1,288,512]{2,1,0:T(8,128)(2,1)S(1)}, bf16[1,288,512]{2,1,0:T(8,128)(2,1)S(1)}, u32[]{:S(2)}, u32[]{:S(2)}) collective-permute-start(bf16[1,288,512]{2,1,0:T(8,128)(2,1)S(1)} %copy-done.6), channel_id=1, source_target_pairs={{8,0},{16,24},{9,1},{17,25},{10,2},{18,26},{11,3},{19,27},{12,4},{... | collective-permute-start | bytes 884744 | tf_op jit(solution)/shard_map/ppermute | solution.py:840

commit v6 on v5

--- a/solution.py
+++ b/solution.py
@@ -334,12 +334,12 @@
                 device_id={"fs": z, "tp": e}, device_id_type=pl.DeviceIdType.MESH,
             )
 
-        def line(way, step, i):
+        def line(way, step, i, source=True):
             block = z + step if way == 0 else z - step
             target = z - 1 if way == 0 else z + 1
             piece = main.at[block, i // tp_count * tp_count + peer(i % tp_count)]
             return pltpu.make_async_remote_copy(
-                piece, piece, line_send.at[way, step], line_recv.at[way, step, i],
+                cast.at[depth] if source is None else piece, piece, line_send.at[way, step], line_recv.at[way, step, i],
                 device_id={"fs": target, "tp": t}, device_id_type=pl.DeviceIdType.MESH,
             )
 
@@ -383,23 +383,22 @@
             return pltpu.make_async_copy(train_refs[m].at[peer(p)], raw.at[slot], load_sem.at[slot])
 
         def keep(m, p, own):
-            slot, place = (m * tp_count + p) % depth, m * tp_count + peer(p)
+            slot, place = cast_slot(m, p), m * tp_count + peer(p)
             goal, goal_rest = (main.at[z], rest.at[z, m]) if own else (own_main, own_rest.at[m])
             return (
                 pltpu.make_async_copy(cast.at[slot], goal.at[place], keep_sem.at[0, slot]),
                 pltpu.make_async_copy(cast_rest.at[slot], goal_rest.at[peer(p)], keep_sem.at[1, slot]),
             )
 
-        def load_ahead(m, p):
-            if m < mats:
-                load(m, p).start()
+        def cast_slot(m, p):
+            return depth if m == 0 and isinstance(p, int) and p == 0 else (m * tp_count + p) % depth
 
         def convert(m, p, own):
-            slot = (m * tp_count + p) % depth
+            slot = cast_slot(m, p)
             load(m, p).wait()
 
             def put(odd):
-                value = raw[slot]
+                value = raw[(m * tp_count + p) % depth]
                 if m < mats - 1:
                     value = value * gain_ref[...].reshape(1, features)
                 value = value.astype(cast.dtype)
@@ -472,12 +471,13 @@
             load(0, p).start()
         for m in range(mats):
             convert(m, 0, True)
-            load_ahead(m, depth)
+            load(m, depth).start()
             if m == 0:
                 middle = jnp.logical_and(z >= 1, z <= count - 2)
                 pl.semaphore_wait(barrier, tp_count + jnp.where(middle, 1, 0))
+                for way in range(2):
+                    pl.when(sends(way))(lambda way=way: line(way, 0, 0, None).start())
                 finish(0, 0, True)
-                forward(0, 0, 0, first=True)
             else:
                 finish(m - 1, tp_count - 1, False)
                 if m > 1:
@@ -491,10 +491,14 @@
                     pl.when(p + depth >= tp_count)(lambda: load(m + 1, p + depth - tp_count).start())
                 if m == 0:
                     pl.when(p >= 2)(lambda: finish(m, p - 1, False))
+                    pl.when(p == tp_count // 2)(lambda: forward(0, 0, 1))
                 else:
                     pl.when(p == 1)(lambda: finish(m, 0, True))
                     pl.when(p >= 2)(lambda: finish(m, p - 1, False))
-                    forward(0, m - 1, p)
+                    if m == 1:
+                        pl.when(p >= 2)(lambda: forward(0, 0, p))
+                    else:
+                        forward(0, m - 1, p)
 
             if m > 0:
                 forward_rest(0, m - 1)
@@ -597,10 +601,10 @@
         + [jax.ShapeDtypeStruct(source.shape, source.dtype) for source in near_sources],
         scratch_shapes=[
             pltpu.VMEM((depth, units, features), jnp.float32),
-            pltpu.VMEM((depth, units, wide), dtype),
-            pltpu.VMEM((depth, half, 128), dtype),
+            pltpu.VMEM((depth + 1, units, wide), dtype),
+            pltpu.VMEM((depth + 1, half, 128), dtype),
             dma((depth,)),
-            dma((2, depth)),
+            dma((2, depth + 1)),
             dma((mats, tp_count)),
             dma((mats, tp_count)),
             dma((mats, tp_count)),

time: 530 us -> 531 us (level)
  no operation moved by 1% of the time
where the time goes in v6:
time: 531 us; the launch traced here: 530 us
  Pallas kernels  465 us (88%)
  waiting for transfers between devices  28.1 us (5%)
  starting transfers between devices  14 us (3%)
  other arithmetic  13 us (2%)
  local copies, waits for them, and re-layouts  7.15 us (1%)
    pallas_call x1, Pallas kernels, gather(): pl.pallas_call(kernel, in_specs=[anywhere] * mats + [pl.BlockSpec(memory_...  423 us
    pallas_call x3, Pallas kernels, join_call(): pl.pallas_call(kernel, grid=(tp_count,), in_specs=[pl.BlockSpec((count, 1...  35.6 us
    ppermute x1, waiting for transfers between devices, line_shards(): near_mixed = lax.ppermute(both_mixed[1], 'fs', outward)  16.4 us
    all_to_all x1, waiting for transfers between devices, mix(): lax.all_to_all(partial_value.reshape(groups * CAP, tp_count, -1), 'tp', s...  11.7 us
  transfers between devices with their start and end apart: 5, of which 2 were waited for; matrix products, arithmetic and copies ran while one was open for 4% of the time, Pallas kernels for 8%

profile of v6, /device:TPU:0, one launch (start us, length us, event | category | flops | bytes accessed | tf_op | source)
XLA Modules:
  0.0 529.7 jit_solution(7947343018443357579)
XLA Ops:
  0.7 422.9 %shard_map.102 = (bf16[4,24,288,512]{3,2,1,0:T(8,128)(2,1)}, bf16[4,3,8,144,128]{4,3,2,1,0:T(8,128)(2,1)}, bf16[24,288,512]{2,1,0:T(8,128)(2,1)}, bf16[3,8,144,1...) custom-call(f32[8,288,576]{2,1,0:T(8,128)} %bitcast.52, ...), custom_call_target="tpu_custom_call" | custom-call | flops 3981312000 | bytes 111476736 | tf_op jit(solution)/shard_map/pallas_call | solution.py:596
  423.5 1.4 collective-permute-start.1
  425.7 1.2 reduce-window.16
  427.2 0.8 compare_and_fusion
  429.1 1.6 fusion
  430.7 1.4 convolution_convert_fusion
  432.2 12.1 %shard_map.104 = (bf16[2304,2304]{1,0:T(8,128)(2,1)}, f32[8,144,288]{2,1,0:T(8,128)}) custom-call(bf16[4,24,288,512]{3,2,1,0:T(8,128)(2,1)} %get-tuple-element.32.main_ref, bf16[4,3,8,144,128]{4,3,2,1,0:T(8,128)(2,1)} %get-tuple-element.33.rest_ref, bf16[144,2304]{1,0:T(8,128)(2,1)} %bitcast.57), custom_call_target="tpu_custom_call" | custom-call | flops 5308416000 | bytes 21233664 | tf_op jit(solution)/shard_map/pallas_call | solution.py:646
  444.3 12.3 %shard_map.103 = (bf16[2304,2304]{1,0:T(8,128)(2,1)}, f32[8,144,288]{2,1,0:T(8,128)}) custom-call(bf16[4,24,288,512]{3,2,1,0:T(8,128)(2,1)} %get-tuple-element.32.main_ref, bf16[4,3,8,144,128]{4,3,2,1,0:T(8,128)(2,1)} %get-tuple-element.33.rest_ref, bf16[144,2304]{1,0:T(8,128)(2,1)} %bitcast.58), custom_call_target="tpu_custom_call" | custom-call | flops 5308416000 | bytes 21233664 | tf_op jit(solution)/shard_map/pallas_call | solution.py:646
  456.6 2.9 multiply_convert_fusion.hidden_ref
  459.5 11.2 %shard_map.105 = (bf16[2304,2304]{1,0:T(8,128)(2,1)}, f32[144,2304]{1,0:T(8,128)}) custom-call(bf16[4,24,288,512]{3,2,1,0:T(8,128)(2,1)} %get-tuple-element.32.main_ref, bf16[4,3,8,144,128]{4,3,2,1,0:T(8,128)(2,1)} %get-tuple-element.33.rest_ref, bf16[8,144,288]{2,1,0:T(8,128)(2,1)} %multiply_convert_fusion.hidden_ref), custom_call_target="tpu_custom_call" | custom-call | flops 5308416000 | bytes 21233664 | tf_op jit(solution)/shard_map/pallas_call | solution.py:646
  470.7 1.4 convert_element_type.31
  472.1 1.3 reshape.73
  473.4 1.0 copy.30
  474.5 8.7 %all-to-all-start = ((bf16[144,8,288]{2,0,1:T(8,128)(2,1)}), bf16[144,8,288]{2,0,1:T(8,128)(2,1)S(1)}, u32[]{:S(2)}, u32[]{:S(2)}) async-start(bf16[144,8,288]{2,0,1:T(8,128)(2,1)} %copy.30), calls=%async_computation | async-start | bytes 1769472 | tf_op jit(solution)/shard_map/all_to_all | solution.py:806
  483.2 1.3 collective-permute-start.2
  485.2 11.7 %all-to-all-done = bf16[144,8,288]{2,0,1:T(8,128)(2,1)S(1)} async-done(((bf16[144,8,288]{2,0,1:T(8,128)(2,1)}), bf16[144,8,288]{2,0,1:T(8,128)(2,1)S(1)}, u32[]{:S(2)}, u32[]{:S(2)}) %all-to-all-start) | async-done | bytes 663584 | tf_op jit(solution)/shard_map/all_to_all | solution.py:806
  497.0 2.1 gather_fusion
  499.2 0.7 reshape.81
  499.9 2.8 multiply_reduce_fusion
  502.7 1.3 collective-permute-start.3
  504.7 1.3 collective-permute-start
  505.9 16.4 %collective-permute-done.3 = bf16[192,288]{1,0:T(8,128)(2,1)S(1)} collective-permute-done((bf16[192,288]{1,0:T(8,128)(2,1)S(1)}, bf16[192,288]{1,0:T(8,128)(2,1)S(1)}, u32[]{:S(2)}, u32[]{:S(2)}) %collective-permute-start.3) | collective-permute-done | bytes 110624 | tf_op jit(solution)/shard_map/ppermute | solution.py:842
  523.0 5.9 %shard_map.106.base_ref = bf16[2304,2304]{1,0:T(8,128)(2,1)} custom-call(s32[15]{0:T(128)} %stack.57.start_ref, bf16[13,288,512]{2,1,0:T(8,128)(2,1)} %collective-permute-done.1.arrived_ref, bf16[2,288,512]{2,1,0:T(8,128)(2,1)} %collective-permute-done.2.extra_ref, bf16[2304,2304]{1,0:T(8,128)(2,1)} %get-tuple-element.49.base_ref), custom_call_target="tpu_custom_call", output_to_operand_aliasing={{}: (3, {})} | custom-call | flops 958464000 | bytes 7667712 | tf_op jit(solution)/shard_map/pallas_call | solution.py:738
  528.9 0.7 shard_map.107
  (46 shorter events, 4.4 us)
Async XLA Ops:
  0.6 424.3 %copy-start.3 = (s32[192,2]{0,1:T(2,128)S(1)}, s32[192,2]{0,1:T(2,128)}, u32[]{:S(2)}) copy-start(s32[192,2]{0,1:T(2,128)} %param.12) | copy-start | bytes 4612
  0.6 428.5 %copy-start = (bf16[192,2304]{1,0:T(8,128)(2,1)S(1)}, bf16[192,2304]{1,0:T(8,128)(2,1)}, u32[]{:S(2)}) copy-start(bf16[192,2304]{1,0:T(8,128)(2,1)} %refs_4_.1) | copy-start | bytes 2654212
  423.5 7.2 %copy-start.2 = (bf16[192,2304]{1,0:T(8,128)(2,1)S(1)}, bf16[192,2304]{1,0:T(8,128)(2,1)}, u32[]{:S(2)}) copy-start(bf16[192,2304]{1,0:T(8,128)(2,1)} %get-tuple-element.37) | copy-start | bytes 2654212
  423.5 99.5 %collective-permute-start.1 = (bf16[13,288,512]{2,1,0:T(8,128)(2,1)}, bf16[13,288,512]{2,1,0:T(8,128)(2,1)}, u32[]{:S(2)}, u32[]{:S(2)}) collective-permute-start(bf16[13,288,512]{2,1,0:T(8,128)(2,1)} %get-tuple-element.47), channel_id=1, source_target_pairs={{8,0},{16,24},{9,1},{17,25},{10,2},{18,26},{11,3},{19,27},{12,4},{... | collective-permute-start | bytes 11501576 | tf_op jit(solution)/shard_map/ppermute | solution.py:831
  444.3 12.3 %copy-start.1 = (f32[8,144,288]{2,1,0:T(8,128)S(1)}, f32[8,144,288]{2,1,0:T(8,128)}, u32[]{:S(2)}) copy-start(f32[8,144,288]{2,1,0:T(8,128)} %get-tuple-element.44) | copy-start | bytes 3981316
  473.4 11.6 %copy-start.4 = (f32[192,2]{0,1:T(2,128)S(1)}, f32[192,2]{0,1:T(2,128)}, u32[]{:S(2)}) copy-start(f32[192,2]{0,1:T(2,128)} %param.13) | copy-start | bytes 4612
  473.4 11.6 %copy-start.5 = (f32[2,192]{1,0:T(2,128)S(1)}, f32[2,192]{1,0:T(2,128)}, u32[]{:S(2)}) copy-start(f32[2,192]{1,0:T(2,128)} %get-tuple-element.42) | copy-start | bytes 4612
  474.5 22.4 %all-to-all-start = ((bf16[144,8,288]{2,0,1:T(8,128)(2,1)}), bf16[144,8,288]{2,0,1:T(8,128)(2,1)S(1)}, u32[]{:S(2)}, u32[]{:S(2)}) async-start(bf16[144,8,288]{2,0,1:T(8,128)(2,1)} %copy.30), calls=%async_computation | async-start | bytes 1769472 | tf_op jit(solution)/shard_map/all_to_all | solution.py:806
  483.2 39.8 %collective-permute-start.2 = (bf16[2,288,512]{2,1,0:T(8,128)(2,1)}, bf16[2,288,512]{2,1,0:T(8,128)(2,1)}, u32[]{:S(2)}, u32[]{:S(2)}) collective-permute-start(bf16[2,288,512]{2,1,0:T(8,128)(2,1)} %get-tuple-element.48), channel_id=1, source_target_pairs={{8,0},{10,2},{12,4},{14,6},{16,24},{18,26},{20,28},{22,30}} | collective-permute-start | bytes 1769480 | tf_op jit(solution)/shard_map/ppermute | solution.py:830
  499.2 5.5 %copy-start.6 = (bf16[1,288,512]{2,1,0:T(8,128)(2,1)S(1)}, bf16[1,288,512]{2,1,0:T(8,128)(2,1)}, u32[]{:S(2)}) copy-start(bf16[1,288,512]{2,1,0:T(8,128)(2,1)} %get-tuple-element.46) | copy-start | bytes 884740
  502.7 19.7 %collective-permute-start.3 = (bf16[192,288]{1,0:T(8,128)(2,1)S(1)}, bf16[192,288]{1,0:T(8,128)(2,1)S(1)}, u32[]{:S(2)}, u32[]{:S(2)}) collective-permute-start(bf16[192,288]{1,0:T(8,128)(2,1)S(1)} %slice_bitcast_fusion.1), channel_id=1, source_target_pairs={{8,0},{16,24},{9,1},{17,25},{10,2},{18,26},{11,3},{19,27},{12,4},{... | collective-permute-start | bytes 331784 | tf_op jit(solution)/shard_map/ppermute | solution.py:842
  504.7 24.3 %collective-permute-start = (bf16[1,288,512]{2,1,0:T(8,128)(2,1)S(1)}, bf16[1,288,512]{2,1,0:T(8,128)(2,1)S(1)}, u32[]{:S(2)}, u32[]{:S(2)}) collective-permute-start(bf16[1,288,512]{2,1,0:T(8,128)(2,1)S(1)} %copy-done.6), channel_id=1, source_target_pairs={{8,0},{16,24},{9,1},{17,25},{10,2},{18,26},{11,3},{19,27},{12,4},{... | collective-permute-start | bytes 884744 | tf_op jit(solution)/shard_map/ppermute | solution.py:844

commit v7 on v5

--- a/solution.py
+++ b/solution.py
@@ -272,7 +272,7 @@
     return (gate_new[None], up_new[None], down_new[None], mixed.astype(jnp.bfloat16))
 
 
-def fits(mesh_sizes, train):
+def fits(mesh_sizes, rows, train):
     count, tp_count = mesh_sizes
     experts, features, units = train.shape
     return (
@@ -280,6 +280,7 @@
         and tp_count & (tp_count - 1) == 0
         and tp_count >= 4
         and count >= 4
+        and rows % 32 == 0
         and count % 2 == 0
         and features % 128 == 64
         and units % 32 == 0
@@ -699,24 +700,29 @@
     )
 
 
-def place_late(arrived, places, extra, extra_places, base, count):
-    units, wide = arrived.shape[1:]
-    places, extra_places = list(places), list(extra_places)
-    total = len(places) + len(extra_places)
-    start = jnp.stack([column for _, column in places + extra_places])
-
-    def kernel(start_ref, arrived_ref, extra_ref, base_ref, new_ref, hold, load_sem, keep_sem):
+def place_late(arrived, places, even_only, base, count):
+    pieces, units, wide = arrived.shape
+    start = jnp.stack([column for _, column in places])
+
+    def kernel(start_ref, arrived_ref, base_ref, new_ref, hold, load_sem, keep_sem):
         z, t = lax.axis_index("fs"), lax.axis_index("tp")
-
-        def move(source, number, first, rows):
-            loads, keeps = [], []
-            for i in range(number):
-                k = first + i
-                goal = new_ref.at[
-                    pl.ds(rows[i][0] * units, units), pl.ds(pl.multiple_of(start_ref[k], 128), wide)
-                ]
-                loads.append(pltpu.make_async_copy(source.at[i], hold.at[k], load_sem.at[k]))
-                keeps.append(pltpu.make_async_copy(hold.at[k], goal, keep_sem.at[k]))
+        wanted = (z == 0) | (z == count - 1)
+        if even_only:
+            wanted = wanted & (t % 2 == 0)
+
+        @pl.when(wanted)
+        def _():
+            loads = [pltpu.make_async_copy(arrived_ref.at[i], hold.at[i], load_sem.at[i]) for i in range(pieces)]
+            keeps = [
+                pltpu.make_async_copy(
+                    hold.at[i],
+                    new_ref.at[
+                        pl.ds(row * units, units), pl.ds(pl.multiple_of(start_ref[i], 128), wide)
+                    ],
+                    keep_sem.at[i],
+                )
+                for i, (row, _) in enumerate(places)
+            ]
             for load in loads:
                 load.start()
             for load, keep in zip(loads, keeps):
@@ -725,27 +731,21 @@
             for keep in keeps:
                 keep.wait()
 
-        at_end = (z == 0) | (z == count - 1)
-        pl.when(at_end)(lambda: move(arrived_ref, len(places), 0, places))
-        pl.when(at_end & (t % 2 == 0))(
-            lambda: move(extra_ref, len(extra_places), len(places), extra_places)
-        )
-
-    return pl.pallas_call(
-        kernel,
-        in_specs=[pl.BlockSpec(memory_space=pltpu.SMEM)] + [pl.BlockSpec(memory_space=pl.ANY)] * 3,
+    return pl.pallas_call(
+        kernel,
+        in_specs=[pl.BlockSpec(memory_space=pltpu.SMEM)] + [pl.BlockSpec(memory_space=pl.ANY)] * 2,
         out_specs=pl.BlockSpec(memory_space=pl.ANY),
         scratch_shapes=[
-            pltpu.VMEM((total, units, wide), arrived.dtype),
-            pltpu.SemaphoreType.DMA((total,)),
-            pltpu.SemaphoreType.DMA((total,)),
+            pltpu.VMEM(arrived.shape, arrived.dtype),
+            pltpu.SemaphoreType.DMA((pieces,)),
+            pltpu.SemaphoreType.DMA((pieces,)),
         ],
         out_shape=jax.ShapeDtypeStruct(base.shape, base.dtype),
-        input_output_aliases={3: 0},
+        input_output_aliases={2: 0},
         cost_estimate=pl.CostEstimate(
             flops=500 * arrived.size, bytes_accessed=4 * arrived.size, transcendentals=0
         ),
-    )(start, arrived, extra, base)
+    )(start, arrived, base)
 
 
 def place_last(arrived, row, column, base, count):
@@ -835,13 +835,17 @@
     hidden = (jax.nn.silu(gate_pre) * up_pre).astype(jnp.bfloat16)
     down_new, total = join_out(main, rest, 2, hidden)
     both_mixed = mix(total.astype(jnp.bfloat16), both_routes, both_weights, experts)
-    near_mixed = lax.ppermute(both_mixed[1], "fs", outward)
+    half, width = both_mixed.shape[1] // 2, both_mixed.shape[2]
+    packed = jnp.concatenate([both_mixed[1, :half], both_mixed[1, half:]], axis=1)
+    packed = lax.ppermute(packed, "fs", outward)
+    near_mixed = jnp.concatenate([packed[:, :width], packed[:, width:]])
     kept_last, _ = lax.optimization_barrier((kept_last, both_mixed))
     arrived_last = lax.ppermute(kept_last, "fs", outward)
     early = [(i, far_start) for i in range(experts)]
     early += [(i, next_start) for i in range(experts - held, experts - 1)]
     extra = [(i, next_start) for i in range(experts - held - lead, experts - held)]
-    down_new = place_late(arrived_early, early, arrived_extra, extra, down_new, count)
+    down_new = place_late(arrived_extra, extra, True, down_new, count)
+    down_new = place_late(arrived_early, early, False, down_new, count)
     down_new = place_last(arrived_last[0], experts - 1, next_start, down_new, count)
     at_end = (place == 0) | (place == count - 1)
     mixed = jnp.where(at_end, near_mixed, both_mixed[0])
@@ -852,7 +856,7 @@
     sizes = (mesh.shape["fs"], mesh.shape["tp"])
 
     def step(*args):
-        if not fits(sizes, args[1]):
+        if not fits(sizes, args[0].shape[0], args[1]):
             return shards(*args)
         return line_shards(*args)
 

time: 530 us -> 528 us (level)
    ppermute x1, waiting for transfers between devices: 17.3 us -> 0.04 us  [line_shards(): packed = lax.ppermute(packed, 'fs', outward)]
    ppermute x1, waiting for transfers between devices: 0.01 us -> 14.2 us  [line_shards(): arrived_extra = lax.ppermute(kept_extra, ('fs', 'tp'), pairs)]
where the time goes in v7:
time: 528 us; the launch traced here: 527 us
  Pallas kernels  465 us (88%)
  waiting for transfers between devices  25.1 us (5%)
  starting transfers between devices  13.8 us (3%)
  other arithmetic  13.7 us (3%)
  local copies, waits for them, and re-layouts  7.2 us (1%)
    pallas_call x1, Pallas kernels, gather(): pl.pallas_call(kernel, in_specs=[anywhere] * mats + [pl.BlockSpec(memory_...  422 us
    pallas_call x3, Pallas kernels, join_call(): pl.pallas_call(kernel, grid=(tp_count,), in_specs=[pl.BlockSpec((count, 1...  35.5 us
    ppermute x1, waiting for transfers between devices, line_shards(): arrived_extra = lax.ppermute(kept_extra, ('fs', 'tp'), pairs)  14.2 us
    all_to_all x1, waiting for transfers between devices, mix(): lax.all_to_all(partial_value.reshape(groups * CAP, tp_count, -1), 'tp', s...  10.8 us
  transfers between devices with their start and end apart: 5, of which 2 were waited for; matrix products, arithmetic and copies ran while one was open for 4% of the time, Pallas kernels for 8%

profile of v7, /device:TPU:0, one launch (start us, length us, event | category | flops | bytes accessed | tf_op | source)
XLA Modules:
  0.0 527.2 jit_solution(1902685612588266388)
XLA Ops:
  0.7 422.1 %shard_map.102 = (bf16[4,24,288,512]{3,2,1,0:T(8,128)(2,1)}, bf16[4,3,8,144,128]{4,3,2,1,0:T(8,128)(2,1)}, bf16[24,288,512]{2,1,0:T(8,128)(2,1)}, bf16[3,8,144,1...) custom-call(f32[8,288,576]{2,1,0:T(8,128)} %bitcast.54, ...), custom_call_target="tpu_custom_call" | custom-call | flops 3981312000 | bytes 111476736 | tf_op jit(solution)/shard_map/pallas_call | solution.py:593
  422.7 1.4 collective-permute-start.1
  424.9 1.2 reduce-window.16
  426.4 0.8 compare_and_fusion
  428.3 1.6 fusion
  429.9 1.4 convolution_convert_fusion
  431.4 12.0 %shard_map.104 = (bf16[2304,2304]{1,0:T(8,128)(2,1)}, f32[8,144,288]{2,1,0:T(8,128)}) custom-call(bf16[4,24,288,512]{3,2,1,0:T(8,128)(2,1)} %get-tuple-element.32.main_ref, bf16[4,3,8,144,128]{4,3,2,1,0:T(8,128)(2,1)} %get-tuple-element.33.rest_ref, bf16[144,2304]{1,0:T(8,128)(2,1)} %bitcast.59), custom_call_target="tpu_custom_call" | custom-call | flops 5308416000 | bytes 21233664 | tf_op jit(solution)/shard_map/pallas_call | solution.py:643
  443.4 12.3 %shard_map.103 = (bf16[2304,2304]{1,0:T(8,128)(2,1)}, f32[8,144,288]{2,1,0:T(8,128)}) custom-call(bf16[4,24,288,512]{3,2,1,0:T(8,128)(2,1)} %get-tuple-element.32.main_ref, bf16[4,3,8,144,128]{4,3,2,1,0:T(8,128)(2,1)} %get-tuple-element.33.rest_ref, bf16[144,2304]{1,0:T(8,128)(2,1)} %bitcast.60), custom_call_target="tpu_custom_call" | custom-call | flops 5308416000 | bytes 21233664 | tf_op jit(solution)/shard_map/pallas_call | solution.py:643
  455.7 2.9 multiply_convert_fusion.hidden_ref
  458.6 11.2 %shard_map.105 = (bf16[2304,2304]{1,0:T(8,128)(2,1)}, f32[144,2304]{1,0:T(8,128)}) custom-call(bf16[4,24,288,512]{3,2,1,0:T(8,128)(2,1)} %get-tuple-element.32.main_ref, bf16[4,3,8,144,128]{4,3,2,1,0:T(8,128)(2,1)} %get-tuple-element.33.rest_ref, bf16[8,144,288]{2,1,0:T(8,128)(2,1)} %multiply_convert_fusion.hidden_ref), custom_call_target="tpu_custom_call" | custom-call | flops 5308416000 | bytes 21233664 | tf_op jit(solution)/shard_map/pallas_call | solution.py:643
  469.8 1.4 convert_element_type.31
  471.2 1.3 reshape.73
  472.6 1.0 copy.31
  473.6 8.3 %all-to-all-start = ((bf16[144,8,288]{2,0,1:T(8,128)(2,1)}), bf16[144,8,288]{2,0,1:T(8,128)(2,1)S(1)}, u32[]{:S(2)}, u32[]{:S(2)}) async-start(bf16[144,8,288]{2,0,1:T(8,128)(2,1)} %copy.31), calls=%async_computation | async-start | bytes 1769472 | tf_op jit(solution)/shard_map/all_to_all | solution.py:802
  481.9 1.5 collective-permute-start.2
  484.7 10.8 %all-to-all-done = bf16[144,8,288]{2,0,1:T(8,128)(2,1)S(1)} async-done(((bf16[144,8,288]{2,0,1:T(8,128)(2,1)}), bf16[144,8,288]{2,0,1:T(8,128)(2,1)S(1)}, u32[]{:S(2)}, u32[]{:S(2)}) %all-to-all-start) | async-done | bytes 663584 | tf_op jit(solution)/shard_map/all_to_all | solution.py:802
  495.7 2.1 gather_fusion
  498.6 2.8 multiply_reduce_fusion
  501.4 1.3 collective-permute-start.3
  503.3 1.3 collective-permute-start
  504.6 14.2 %collective-permute-done.2.arrived_ref = bf16[2,288,512]{2,1,0:T(8,128)(2,1)} collective-permute-done((bf16[2,288,512]{2,1,0:T(8,128)(2,1)}, bf16[2,288,512]{2,1,0:T(8,128)(2,1)}, u32[]{:S(2)}, u32[]{:S(2)}) %collective-permute-start.2) | collective-permute-done | bytes 589856 | tf_op jit(solution)/shard_map/ppermute | solution.py:826
  518.8 2.5 shard_map.106.base_ref
  522.2 4.1 shard_map.107.base_ref
  526.3 0.7 shard_map.108
  (50 shorter events, 5.9 us)
Async XLA Ops:
  0.6 423.6 %copy-start.3 = (s32[192,2]{0,1:T(2,128)S(1)}, s32[192,2]{0,1:T(2,128)}, u32[]{:S(2)}) copy-start(s32[192,2]{0,1:T(2,128)} %param.12) | copy-start | bytes 4612
  0.6 427.7 %copy-start = (bf16[192,2304]{1,0:T(8,128)(2,1)S(1)}, bf16[192,2304]{1,0:T(8,128)(2,1)}, u32[]{:S(2)}) copy-start(bf16[192,2304]{1,0:T(8,128)(2,1)} %refs_4_.1) | copy-start | bytes 2654212
  422.7 7.2 %copy-start.2 = (bf16[192,2304]{1,0:T(8,128)(2,1)S(1)}, bf16[192,2304]{1,0:T(8,128)(2,1)}, u32[]{:S(2)}) copy-start(bf16[192,2304]{1,0:T(8,128)(2,1)} %get-tuple-element.37) | copy-start | bytes 2654212
  422.7 99.4 %collective-permute-start.1 = (bf16[13,288,512]{2,1,0:T(8,128)(2,1)}, bf16[13,288,512]{2,1,0:T(8,128)(2,1)}, u32[]{:S(2)}, u32[]{:S(2)}) collective-permute-start(bf16[13,288,512]{2,1,0:T(8,128)(2,1)} %get-tuple-element.47), channel_id=1, source_target_pairs={{8,0},{16,24},{9,1},{17,25},{10,2},{18,26},{11,3},{19,27},{12,4},{... | collective-permute-start | bytes 11501576 | tf_op jit(solution)/shard_map/ppermute | solution.py:827
  443.4 12.3 %copy-start.1 = (f32[8,144,288]{2,1,0:T(8,128)S(1)}, f32[8,144,288]{2,1,0:T(8,128)}, u32[]{:S(2)}) copy-start(f32[8,144,288]{2,1,0:T(8,128)} %get-tuple-element.44) | copy-start | bytes 3981316
  472.5 11.3 %copy-start.4 = (f32[192,2]{0,1:T(2,128)S(1)}, f32[192,2]{0,1:T(2,128)}, u32[]{:S(2)}) copy-start(f32[192,2]{0,1:T(2,128)} %param.13) | copy-start | bytes 4612
  472.6 11.3 %copy-start.5 = (f32[2,192]{1,0:T(2,128)S(1)}, f32[2,192]{1,0:T(2,128)}, u32[]{:S(2)}) copy-start(f32[2,192]{1,0:T(2,128)} %get-tuple-element.42) | copy-start | bytes 4612
  473.6 21.9 %all-to-all-start = ((bf16[144,8,288]{2,0,1:T(8,128)(2,1)}), bf16[144,8,288]{2,0,1:T(8,128)(2,1)S(1)}, u32[]{:S(2)}, u32[]{:S(2)}) async-start(bf16[144,8,288]{2,0,1:T(8,128)(2,1)} %copy.31), calls=%async_computation | async-start | bytes 1769472 | tf_op jit(solution)/shard_map/all_to_all | solution.py:802
  481.9 36.9 %collective-permute-start.2 = (bf16[2,288,512]{2,1,0:T(8,128)(2,1)}, bf16[2,288,512]{2,1,0:T(8,128)(2,1)}, u32[]{:S(2)}, u32[]{:S(2)}) collective-permute-start(bf16[2,288,512]{2,1,0:T(8,128)(2,1)} %get-tuple-element.48), channel_id=1, source_target_pairs={{8,0},{10,2},{12,4},{14,6},{16,24},{18,26},{20,28},{22,30}} | collective-permute-start | bytes 1769480 | tf_op jit(solution)/shard_map/ppermute | solution.py:826
  497.8 5.5 %copy-start.6 = (bf16[1,288,512]{2,1,0:T(8,128)(2,1)S(1)}, bf16[1,288,512]{2,1,0:T(8,128)(2,1)}, u32[]{:S(2)}) copy-start(bf16[1,288,512]{2,1,0:T(8,128)(2,1)} %get-tuple-element.46) | copy-start | bytes 884740
  501.4 19.9 %collective-permute-start.3 = (bf16[96,576]{1,0:T(8,128)(2,1)S(1)}, bf16[96,576]{1,0:T(8,128)(2,1)S(1)}, u32[]{:S(2)}, u32[]{:S(2)}) collective-permute-start(bf16[96,576]{1,0:T(8,128)(2,1)S(1)} %pad_maximum_fusion.2), channel_id=1, source_target_pairs={{8,0},{16,24},{9,1},{17,25},{10,2},{18,26},{11,3},{19,27},{12,4},{... | collective-permute-start | bytes 331784 | tf_op jit(solution)/shard_map/ppermute | solution.py:840
  503.3 22.9 %collective-permute-start = (bf16[1,288,512]{2,1,0:T(8,128)(2,1)S(1)}, bf16[1,288,512]{2,1,0:T(8,128)(2,1)S(1)}, u32[]{:S(2)}, u32[]{:S(2)}) collective-permute-start(bf16[1,288,512]{2,1,0:T(8,128)(2,1)S(1)} %copy-done.6), channel_id=1, source_target_pairs={{8,0},{16,24},{9,1},{17,25},{10,2},{18,26},{11,3},{19,27},{12,4},{... | collective-permute-start | bytes 884744 | tf_op jit(solution)/shard_map/ppermute | solution.py:843

commit v8 on v7

--- a/solution.py
+++ b/solution.py
@@ -280,7 +280,7 @@
         and tp_count & (tp_count - 1) == 0
         and tp_count >= 4
         and count >= 4
-        and rows % 32 == 0
+        and rows % 64 == 0
         and count % 2 == 0
         and features % 128 == 64
         and units % 32 == 0
@@ -311,6 +311,7 @@
         plane_send, plane_recv, plane_rest_send, plane_rest_recv = take(4)
         line_send, line_recv, line_rest_send, line_rest_recv = take(4)
         near_send, near_recv, pass_hold, pass_load, pass_keep = take(5)
+        scale, scale_sem = take(2)
         z = lax.axis_index("fs")
         t = lax.axis_index("tp")
 
@@ -402,7 +403,7 @@
             def put(odd):
                 value = raw[slot]
                 if m < mats - 1:
-                    value = value * gain_ref[...].reshape(1, features)
+                    value = value * scale[...].reshape(1, features)
                 value = value.astype(cast.dtype)
                 if odd:
                     cast[slot], end = value[:, 64:], value[:, :64]
@@ -469,8 +470,11 @@
                 barrier, inc=1, device_id={"fs": z + 1, "tp": t}, device_id_type=pl.DeviceIdType.MESH
             )
 
+        scale_copy = pltpu.make_async_copy(gain_ref, scale, scale_sem)
+        scale_copy.start()
         for p in range(depth):
             load(0, p).start()
+        scale_copy.wait()
         for m in range(mats):
             convert(m, 0, True)
             load_ahead(m, depth)
@@ -492,10 +496,14 @@
                     pl.when(p + depth >= tp_count)(lambda: load(m + 1, p + depth - tp_count).start())
                 if m == 0:
                     pl.when(p >= 2)(lambda: finish(m, p - 1, False))
+                    pl.when(p == tp_count // 2)(lambda: forward(0, 0, 1))
                 else:
                     pl.when(p == 1)(lambda: finish(m, 0, True))
                     pl.when(p >= 2)(lambda: finish(m, p - 1, False))
-                    forward(0, m - 1, p)
+                    if m == 1:
+                        pl.when(p >= 2)(lambda: forward(0, 0, p))
+                    else:
+                        forward(0, m - 1, p)
 
             if m > 0:
                 forward_rest(0, m - 1)
@@ -592,7 +600,7 @@
     ]
     return pl.pallas_call(
         kernel,
-        in_specs=[anywhere] * mats + [pl.BlockSpec(memory_space=pltpu.VMEM)] + [anywhere] * nears,
+        in_specs=[anywhere] * (mats + 1 + nears),
         out_specs=[anywhere] * (len(outs) + nears),
         out_shape=[jax.ShapeDtypeStruct(shape, dtype) for shape in outs]
         + [jax.ShapeDtypeStruct(source.shape, source.dtype) for source in near_sources],
@@ -615,6 +623,8 @@
             pltpu.VMEM((tp_count + held + lead, units, wide), dtype),
             dma((tp_count + held + lead,)),
             dma((tp_count + held + lead,)),
+            pltpu.VMEM(gain.shape, gain.dtype),
+            dma,
         ],
         compiler_params=pltpu.CompilerParams(collective_id=0, has_side_effects=True),
         cost_estimate=pl.CostEstimate(
@@ -835,10 +845,10 @@
     hidden = (jax.nn.silu(gate_pre) * up_pre).astype(jnp.bfloat16)
     down_new, total = join_out(main, rest, 2, hidden)
     both_mixed = mix(total.astype(jnp.bfloat16), both_routes, both_weights, experts)
-    half, width = both_mixed.shape[1] // 2, both_mixed.shape[2]
-    packed = jnp.concatenate([both_mixed[1, :half], both_mixed[1, half:]], axis=1)
+    width = both_mixed.shape[2]
+    packed = jnp.concatenate(jnp.split(both_mixed[1], 4), axis=1)
     packed = lax.ppermute(packed, "fs", outward)
-    near_mixed = jnp.concatenate([packed[:, :width], packed[:, width:]])
+    near_mixed = jnp.concatenate([packed[:, i * width : (i + 1) * width] for i in range(4)])
     kept_last, _ = lax.optimization_barrier((kept_last, both_mixed))
     arrived_last = lax.ppermute(kept_last, "fs", outward)
     early = [(i, far_start) for i in range(experts)]

time: 528 us -> 528 us (level)
  no operation moved by 1% of the time
where the time goes in v8:
time: 528 us; the launch traced here: 527 us
  Pallas kernels  465 us (88%)
  waiting for transfers between devices  24.2 us (5%)
  starting transfers between devices  14.2 us (3%)
  other arithmetic  13.6 us (3%)
  local copies, waits for them, and re-layouts  7.35 us (1%)
    pallas_call x1, Pallas kernels, gather(): pl.pallas_call(kernel, in_specs=[anywhere] * (mats + 1 + nears), out_spec...  422 us
    pallas_call x3, Pallas kernels, join_call(): pl.pallas_call(kernel, grid=(tp_count,), in_specs=[pl.BlockSpec((count, 1...  35.6 us
    ppermute x1, waiting for transfers between devices, line_shards(): arrived_extra = lax.ppermute(kept_extra, ('fs', 'tp'), pairs)  13.3 us
    all_to_all x1, waiting for transfers between devices, mix(): lax.all_to_all(partial_value.reshape(groups * CAP, tp_count, -1), 'tp', s...  10.8 us
  transfers between devices with their start and end apart: 5, of which 2 were waited for; matrix products, arithmetic and copies ran while one was open for 4% of the time, Pallas kernels for 8%

profile of v8, /device:TPU:0, one launch (start us, length us, event | category | flops | bytes accessed | tf_op | source)
XLA Modules:
  0.0 527.0 jit_solution(12459955425660521504)
XLA Ops:
  0.7 422.2 %shard_map.102 = (bf16[4,24,288,512]{3,2,1,0:T(8,128)(2,1)}, bf16[4,3,8,144,128]{4,3,2,1,0:T(8,128)(2,1)}, bf16[24,288,512]{2,1,0:T(8,128)(2,1)}, bf16[3,8,144,1...) custom-call(f32[8,288,576]{2,1,0:T(8,128)} %bitcast.58, ...), custom_call_target="tpu_custom_call" | custom-call | flops 3981312000 | bytes 111476736 | tf_op jit(solution)/shard_map/pallas_call | solution.py:601
  422.9 1.4 collective-permute-start.1
  425.1 1.2 reduce-window.16
  426.6 0.8 compare_and_fusion
  428.5 1.6 fusion
  430.1 1.4 convolution_convert_fusion
  431.5 12.1 %shard_map.104 = (bf16[2304,2304]{1,0:T(8,128)(2,1)}, f32[8,144,288]{2,1,0:T(8,128)}) custom-call(bf16[4,24,288,512]{3,2,1,0:T(8,128)(2,1)} %get-tuple-element.32.main_ref, bf16[4,3,8,144,128]{4,3,2,1,0:T(8,128)(2,1)} %get-tuple-element.33.rest_ref, bf16[144,2304]{1,0:T(8,128)(2,1)} %bitcast.63), custom_call_target="tpu_custom_call" | custom-call | flops 5308416000 | bytes 21233664 | tf_op jit(solution)/shard_map/pallas_call | solution.py:653
  443.6 12.3 %shard_map.103 = (bf16[2304,2304]{1,0:T(8,128)(2,1)}, f32[8,144,288]{2,1,0:T(8,128)}) custom-call(bf16[4,24,288,512]{3,2,1,0:T(8,128)(2,1)} %get-tuple-element.32.main_ref, bf16[4,3,8,144,128]{4,3,2,1,0:T(8,128)(2,1)} %get-tuple-element.33.rest_ref, bf16[144,2304]{1,0:T(8,128)(2,1)} %bitcast.64), custom_call_target="tpu_custom_call" | custom-call | flops 5308416000 | bytes 21233664 | tf_op jit(solution)/shard_map/pallas_call | solution.py:653
  456.0 2.9 multiply_convert_fusion.hidden_ref
  458.9 11.2 %shard_map.105 = (bf16[2304,2304]{1,0:T(8,128)(2,1)}, f32[144,2304]{1,0:T(8,128)}) custom-call(bf16[4,24,288,512]{3,2,1,0:T(8,128)(2,1)} %get-tuple-element.32.main_ref, bf16[4,3,8,144,128]{4,3,2,1,0:T(8,128)(2,1)} %get-tuple-element.33.rest_ref, bf16[8,144,288]{2,1,0:T(8,128)(2,1)} %multiply_convert_fusion.hidden_ref), custom_call_target="tpu_custom_call" | custom-call | flops 5308416000 | bytes 21233664 | tf_op jit(solution)/shard_map/pallas_call | solution.py:653
  470.0 1.4 convert_element_type.31
  471.4 1.3 reshape.77
  472.8 1.0 copy.31
  473.8 8.7 %all-to-all-start = ((bf16[144,8,288]{2,0,1:T(8,128)(2,1)}), bf16[144,8,288]{2,0,1:T(8,128)(2,1)S(1)}, u32[]{:S(2)}, u32[]{:S(2)}) async-start(bf16[144,8,288]{2,0,1:T(8,128)(2,1)} %copy.31), calls=%async_computation | async-start | bytes 1769472 | tf_op jit(solution)/shard_map/all_to_all | solution.py:812
  482.6 1.5 collective-permute-start.2
  485.3 10.8 %all-to-all-done = bf16[144,8,288]{2,0,1:T(8,128)(2,1)S(1)} async-done(((bf16[144,8,288]{2,0,1:T(8,128)(2,1)}), bf16[144,8,288]{2,0,1:T(8,128)(2,1)S(1)}, u32[]{:S(2)}, u32[]{:S(2)}) %all-to-all-start) | async-done | bytes 663584 | tf_op jit(solution)/shard_map/all_to_all | solution.py:812
  496.4 2.1 gather_fusion
  499.2 2.8 multiply_reduce_fusion
  502.1 1.3 collective-permute-start.3
  504.0 1.3 collective-permute-start
  505.3 13.3 %collective-permute-done.2.arrived_ref = bf16[2,288,512]{2,1,0:T(8,128)(2,1)} collective-permute-done((bf16[2,288,512]{2,1,0:T(8,128)(2,1)}, bf16[2,288,512]{2,1,0:T(8,128)(2,1)}, u32[]{:S(2)}, u32[]{:S(2)}) %collective-permute-start.2) | collective-permute-done | bytes 589856 | tf_op jit(solution)/shard_map/ppermute | solution.py:836
  518.7 2.5 shard_map.106.base_ref
  522.0 4.1 shard_map.107.base_ref
  526.1 0.7 shard_map.108
  (50 shorter events, 5.9 us)
Async XLA Ops:
  0.6 423.7 %copy-start.3 = (s32[192,2]{0,1:T(2,128)S(1)}, s32[192,2]{0,1:T(2,128)}, u32[]{:S(2)}) copy-start(s32[192,2]{0,1:T(2,128)} %param.12) | copy-start | bytes 4612
  0.6 427.9 %copy-start = (bf16[192,2304]{1,0:T(8,128)(2,1)S(1)}, bf16[192,2304]{1,0:T(8,128)(2,1)}, u32[]{:S(2)}) copy-start(bf16[192,2304]{1,0:T(8,128)(2,1)} %refs_4_.1) | copy-start | bytes 2654212
  422.9 7.2 %copy-start.2 = (bf16[192,2304]{1,0:T(8,128)(2,1)S(1)}, bf16[192,2304]{1,0:T(8,128)(2,1)}, u32[]{:S(2)}) copy-start(bf16[192,2304]{1,0:T(8,128)(2,1)} %get-tuple-element.37) | copy-start | bytes 2654212
  422.9 99.1 %collective-permute-start.1 = (bf16[13,288,512]{2,1,0:T(8,128)(2,1)}, bf16[13,288,512]{2,1,0:T(8,128)(2,1)}, u32[]{:S(2)}, u32[]{:S(2)}) collective-permute-start(bf16[13,288,512]{2,1,0:T(8,128)(2,1)} %get-tuple-element.47), channel_id=1, source_target_pairs={{8,0},{16,24},{9,1},{17,25},{10,2},{18,26},{11,3},{19,27},{12,4},{... | collective-permute-start | bytes 11501576 | tf_op jit(solution)/shard_map/ppermute | solution.py:837
  443.6 12.3 %copy-start.1 = (f32[8,144,288]{2,1,0:T(8,128)S(1)}, f32[8,144,288]{2,1,0:T(8,128)}, u32[]{:S(2)}) copy-start(f32[8,144,288]{2,1,0:T(8,128)} %get-tuple-element.44) | copy-start | bytes 3981316
  472.8 11.7 %copy-start.4 = (f32[192,2]{0,1:T(2,128)S(1)}, f32[192,2]{0,1:T(2,128)}, u32[]{:S(2)}) copy-start(f32[192,2]{0,1:T(2,128)} %param.13) | copy-start | bytes 4612
  472.8 11.7 %copy-start.5 = (f32[2,192]{1,0:T(2,128)S(1)}, f32[2,192]{1,0:T(2,128)}, u32[]{:S(2)}) copy-start(f32[2,192]{1,0:T(2,128)} %get-tuple-element.42) | copy-start | bytes 4612
  473.8 22.3 %all-to-all-start = ((bf16[144,8,288]{2,0,1:T(8,128)(2,1)}), bf16[144,8,288]{2,0,1:T(8,128)(2,1)S(1)}, u32[]{:S(2)}, u32[]{:S(2)}) async-start(bf16[144,8,288]{2,0,1:T(8,128)(2,1)} %copy.31), calls=%async_computation | async-start | bytes 1769472 | tf_op jit(solution)/shard_map/all_to_all | solution.py:812
  482.6 36.1 %collective-permute-start.2 = (bf16[2,288,512]{2,1,0:T(8,128)(2,1)}, bf16[2,288,512]{2,1,0:T(8,128)(2,1)}, u32[]{:S(2)}, u32[]{:S(2)}) collective-permute-start(bf16[2,288,512]{2,1,0:T(8,128)(2,1)} %get-tuple-element.48), channel_id=1, source_target_pairs={{8,0},{10,2},{12,4},{14,6},{16,24},{18,26},{20,28},{22,30}} | collective-permute-start | bytes 1769480 | tf_op jit(solution)/shard_map/ppermute | solution.py:836
  498.5 5.5 %copy-start.6 = (bf16[1,288,512]{2,1,0:T(8,128)(2,1)S(1)}, bf16[1,288,512]{2,1,0:T(8,128)(2,1)}, u32[]{:S(2)}) copy-start(bf16[1,288,512]{2,1,0:T(8,128)(2,1)} %get-tuple-element.46) | copy-start | bytes 884740
  502.1 19.0 %collective-permute-start.3 = (bf16[48,1152]{1,0:T(8,128)(2,1)S(1)}, bf16[48,1152]{1,0:T(8,128)(2,1)S(1)}, u32[]{:S(2)}, u32[]{:S(2)}) collective-permute-start(bf16[48,1152]{1,0:T(8,128)(2,1)S(1)} %concatenate.6), channel_id=1, source_target_pairs={{8,0},{16,24},{9,1},{17,25},{10,2},{18,26},{11,3},{19,27},{12,4},{... | collective-permute-start | bytes 331784 | tf_op jit(solution)/shard_map/ppermute | solution.py:850
  504.0 22.0 %collective-permute-start = (bf16[1,288,512]{2,1,0:T(8,128)(2,1)S(1)}, bf16[1,288,512]{2,1,0:T(8,128)(2,1)S(1)}, u32[]{:S(2)}, u32[]{:S(2)}) collective-permute-start(bf16[1,288,512]{2,1,0:T(8,128)(2,1)S(1)} %copy-done.6), channel_id=1, source_target_pairs={{8,0},{16,24},{9,1},{17,25},{10,2},{18,26},{11,3},{19,27},{12,4},{... | collective-permute-start | bytes 884744 | tf_op jit(solution)/shard_map/ppermute | solution.py:853
